TPU v7x, 32 devices: a whole 2x2x4 slice. The times are simulated.
32 devices in a mesh: sp: 16 (over z, y, core), tp: 2 (over x).
Axes of the slice: x: 2, y: 2, z: 4, core: 2. Of those that a mesh axis runs over, the one named last changes fastest.
Arguments:
- activations: bfloat16 [4096, 2048], P('sp', 'tp'), may hold values from -8 to 8
- norm_gain: float32 [2048], replicated, may hold values from 0.1 to 1.9
- win_query: bfloat16 [2048, 1024], P(None, 'tp'), may hold values from -1 to 1
- win_key: bfloat16 [2048, 512], P(None, 'tp'), may hold values from -1 to 1
- win_value: bfloat16 [2048, 512], P(None, 'tp'), may hold values from -0.125 to 0.125
- sink_logit: float32 [16], P('tp'), may hold values from 1 to 6
- lat_query: bfloat16 [2048, 1536], P(None, 'tp'), may hold values from -1 to 1
- key_value_down_weight: bfloat16 [2048, 128], replicated, may hold values from -0.125 to 0.125
- rope_key: bfloat16 [2048, 64], replicated, may hold values from -1 to 1
- latent_norm_gain: float32 [128], replicated, may hold values from 0.1 to 1.9
- key_up_weight: bfloat16 [128, 1024], P(None, 'tp'), may hold values from -0.5 to 0.5
- value_up_weight: bfloat16 [128, 1024], P(None, 'tp'), may hold values from -0.5 to 0.5
- out_win: bfloat16 [1024, 2048], P('tp'), may hold values from -0.359375 to 0.359375
- out_lat: bfloat16 [1024, 2048], P('tp'), may hold values from -0.59765625 to 0.59765625
Outputs:
- mixed: bfloat16 [4096, 2048], P('sp', 'tp')
All inputs are finite; a program needn't handle non-finite values.
Results may differ from a plain program's by a relative error of at most 0.025.
Values may be sent and summed in bfloat16 or wider, within the bound.
No kernel may reach another device: no remote copies, remote signals or barrier semaphores. Data moves between devices by JAX's collectives and lax.ppermute only.
A program may use at most 64 MiB of HBM per device.

v0:
```python
from functools import partial

import jax
import jax.numpy as jnp
from jax import lax
from jax.sharding import PartitionSpec as P

HEADS_A = 16
DH = 64
WINDOW = 128
UNROTATED_WIDTH = 128
D_ROPE = 64
VALUE_WIDTH = 128


EPSILON = 1e-06
ROPE_BASE = 10000.0


def padded_2(cells, sides, width):
    for axis, dim in sides:
        count = lax.axis_size(axis)
        ends = count - 1
        head = lax.slice_in_dim(cells, 0, width, axis=dim)
        tail = lax.slice_in_dim(cells, cells.shape[dim] - width, cells.shape[dim], axis=dim)
        cells = jnp.concatenate(
            [
                lax.ppermute(tail, axis, [(i, (i + 1) % count) for i in range(ends)]),
                cells,
                lax.ppermute(head, axis, [((i + 1) % count, i) for i in range(ends)]),
            ],
            axis=dim,
        )
    return cells


def rotate(vectors, angles):
    half_width = vectors.shape[-1] // 2
    cosine_table = jnp.cos(angles)
    sine_table = jnp.sin(angles)
    lower_half = vectors[..., :half_width]
    upper_half = vectors[..., half_width:]
    return jnp.concatenate(
        [
            lower_half * cosine_table - upper_half * sine_table,
            lower_half * sine_table + upper_half * cosine_table,
        ],
        axis=-1,
    )


def rotary_angles(places, width):
    frequency = 1.0 / ROPE_BASE ** (jnp.arange(0, width, 2).astype(jnp.float32) / width)
    return places[:, None] * frequency[None, :]


def window_attention(queries, padded, sinks, offset, seq_total, head_start):
    tok_rows = queries.shape[0]
    key_heads = padded.shape[1] // (2 * DH)
    groups = queries.shape[1] // (DH * key_heads)
    key_rows = padded[:, : key_heads * DH].reshape(-1, key_heads, DH)
    value_rows = padded[:, key_heads * DH :].reshape(-1, key_heads, DH)
    grouped = queries.reshape(tok_rows, key_heads, groups, DH)
    scores = jnp.einsum(
        "qhgd,khd->hgqk", grouped, key_rows, preferred_element_type=jnp.float32
    ) * DH ** (-0.5)
    query_pos = offset + jnp.arange(tok_rows, dtype=jnp.int32)
    key_pos = offset - WINDOW + jnp.arange(tok_rows + 2 * WINDOW, dtype=jnp.int32)
    distance = jnp.abs(query_pos[:, None] - key_pos[None, :])
    in_window = (distance <= WINDOW) & (key_pos[None, :] >= 0) & (key_pos[None, :] < seq_total)
    head_ids = head_start + jnp.arange(key_heads * groups, dtype=jnp.int32)
    slopes = jnp.exp2(-8.0 * (head_ids + 1).astype(jnp.float32) / HEADS_A).reshape(
        key_heads, groups
    )
    scores = scores - slopes[:, :, None, None] * distance.astype(jnp.float32)[None, None]
    scores = jnp.where(in_window[None, None], scores, -jnp.inf)
    sink_table = sinks.reshape(key_heads, groups)
    row_peak = jnp.maximum(jnp.max(scores, axis=3), sink_table[:, :, None])
    weights = jnp.exp(scores - row_peak[..., None])
    denominator = jnp.sum(weights, axis=3) + jnp.exp(sink_table[:, :, None] - row_peak)
    blended = jnp.einsum(
        "hgqk,khd->qhgd",
        weights.astype(jnp.bfloat16),
        value_rows,
        preferred_element_type=jnp.float32,
    )
    blended = blended / jnp.transpose(denominator, (2, 0, 1))[..., None]
    return blended.reshape(tok_rows, key_heads * groups * DH).astype(jnp.bfloat16)


def latent_step(running, key_block, query_plain, query_turned):
    row_peak, totals, weighted = running
    keys_plain, values_plain, keys_turned = key_block
    key_count = keys_plain.shape[0]
    head_count = query_plain.shape[1]
    scores = jnp.einsum(
        "qhd,khd->hqk",
        query_plain,
        keys_plain.reshape(key_count, head_count, UNROTATED_WIDTH),
        preferred_element_type=jnp.float32,
    )
    scores = scores + jnp.einsum(
        "qhd,kd->hqk", query_turned, keys_turned, preferred_element_type=jnp.float32
    )
    scores = scores * (UNROTATED_WIDTH + D_ROPE) ** (-0.5)
    new_peak = jnp.maximum(row_peak, jnp.max(scores, axis=2))
    factor = jnp.exp(row_peak - new_peak)
    weights = jnp.exp(scores - new_peak[..., None])
    totals = totals * factor + jnp.sum(weights, axis=2)
    weighted = weighted * factor[..., None] + jnp.einsum(
        "hqk,khd->hqd",
        weights.astype(jnp.bfloat16),
        values_plain.reshape(key_count, head_count, VALUE_WIDTH),
        preferred_element_type=jnp.float32,
    )
    return (new_peak, totals, weighted)


def over_blocks(running, pieces, prepare, attend, block_rows):
    key_count = pieces[0].shape[0]
    stacked = tuple(
        (
            piece_part.reshape((key_count // block_rows, block_rows) + piece_part.shape[1:])
            for piece_part in pieces
        )
    )

    def one_block(state_now, key_block):
        return (attend(state_now, prepare(key_block)), None)

    return lax.scan(one_block, running, stacked)[0]


def per_device(
    activations,
    norm_gain,
    win_query,
    win_key,
    win_value,
    sink_logit,
    lat_query,
    key_value_down_weight,
    rope_key,
    latent_norm_gain,
    key_up_weight,
    value_up_weight,
    out_win,
    out_lat,
):
    tok_rows = activations.shape[0]
    weights_all = (win_query, win_key, win_value, lat_query, key_value_down_weight, rope_key)
    widened = lax.all_gather(activations, "tp", axis=1, tiled=True).astype(jnp.float32)
    normalized = (widened * norm_gain[None, :]).astype(jnp.bfloat16)
    squares = jnp.sum(widened * widened, axis=1)
    totals = tuple(
        (jnp.dot(normalized, weight, preferred_element_type=jnp.float32) for weight in weights_all)
    )
    squares, totals = (squares, totals)
    win_proj, key_proj, value_proj, latq_proj, compressed, rope_proj = totals
    row_scale = lax.rsqrt(squares / norm_gain.shape[0] + EPSILON)[:, None]
    offset = lax.axis_index("sp") * tok_rows
    seq_total = tok_rows * lax.axis_size("sp")
    places = (offset + jnp.arange(tok_rows, dtype=jnp.int32)).astype(jnp.float32)
    angles = rotary_angles(places, D_ROPE)
    win_queries = (win_proj * row_scale).astype(jnp.bfloat16)
    key_value = jnp.concatenate(
        [
            (key_proj * row_scale).astype(jnp.bfloat16),
            (value_proj * row_scale).astype(jnp.bfloat16),
        ],
        axis=1,
    )
    padded = padded_2(key_value, (("sp", 0),), WINDOW)
    head_start = lax.axis_index("tp") * sink_logit.shape[0]
    win_out = window_attention(win_queries, padded, sink_logit, offset, seq_total, head_start)
    head_count = lat_query.shape[1] // (UNROTATED_WIDTH + D_ROPE)
    query_all = (latq_proj * row_scale).reshape(tok_rows, head_count, UNROTATED_WIDTH + D_ROPE)
    query_plain = query_all[..., :UNROTATED_WIDTH].astype(jnp.bfloat16)
    query_turned = rotate(query_all[..., UNROTATED_WIDTH:], angles[:, None, :]).astype(jnp.bfloat16)
    latent = (
        compressed
        * lax.rsqrt(jnp.mean(compressed * compressed, axis=1, keepdims=True) + EPSILON)
        * latent_norm_gain[None, :]
    ).astype(jnp.bfloat16)
    key_rotary = rotate(rope_proj * row_scale, angles).astype(jnp.bfloat16)
    attend = partial(latent_step, query_plain=query_plain, query_turned=query_turned)

    def expand(key_block):
        return (
            jnp.dot(key_block[0], key_up_weight, preferred_element_type=jnp.float32).astype(
                jnp.bfloat16
            ),
            jnp.dot(key_block[0], value_up_weight, preferred_element_type=jnp.float32).astype(
                jnp.bfloat16
            ),
            key_block[1],
        )

    row_peak, totals_lat, weighted = over_blocks(
        (
            jnp.full((head_count, tok_rows), -jnp.inf, jnp.float32),
            jnp.zeros((head_count, tok_rows), jnp.float32),
            jnp.zeros((head_count, tok_rows, VALUE_WIDTH), jnp.float32),
        ),
        (
            lax.all_gather(latent, "sp", axis=0, tiled=True),
            lax.all_gather(key_rotary, "sp", axis=0, tiled=True),
        ),
        expand,
        attend,
        2048,
    )
    lat_out = (
        (weighted / totals_lat[..., None])
        .transpose(1, 0, 2)
        .reshape(tok_rows, head_count * VALUE_WIDTH)
    )
    lat_out = lat_out.astype(jnp.bfloat16)
    terms = jnp.dot(win_out, out_win, preferred_element_type=jnp.float32) + jnp.dot(
        lat_out, out_lat, preferred_element_type=jnp.float32
    )
    return lax.psum_scatter(terms.astype(jnp.bfloat16), "tp", scatter_dimension=1, tiled=True)


def solution(mesh):
    return jax.shard_map(
        per_device,
        mesh=mesh,
        in_specs=(
            P("sp", "tp"),
            P(),
            P(None, "tp"),
            P(None, "tp"),
            P(None, "tp"),
            P("tp"),
            P(None, "tp"),
            P(),
            P(),
            P(),
            P(None, "tp"),
            P(None, "tp"),
            P("tp", None),
            P("tp", None),
        ),
        out_specs=P("sp", "tp"),
        check_vma=False,
    )
```

profile of v0, /device:TPU:0, one launch (start us, length us, event | category | flops | bytes accessed | tf_op | source)
XLA Modules:
  0.0 175.6 jit_solution(10355702871223245682)
XLA Ops:
  6.5 0.7 all-gather.3.cloned.1.call-update
  7.3 0.0 all-gather.5.cloned.1.call-start
  7.3 0.9 max.19
  8.3 0.6 multiply_exponential_fusion
  8.9 0.9 fusion.44
  9.8 0.9 fusion.41
  10.7 22.2 %all-gather.3.cloned.1.call-done = bf16[256,2048]{1,0:T(8,128)(2,1)} async-done(((bf16[256,1024]{1,0:T(8,128)(2,1)}), bf16[256,2048]{1,0:T(8,128)(2,1)}) %all-gather.3.cloned.1.call-update) | async-done | bytes 1048592 | tf_op jit(solution)/shard_map/all_gather | solution.py:152
  32.9 1.5 fusion.25
  34.5 3.1 %convolution_multiply_fusion = f32[256,768]{1,0:T(8,128)} fusion(bf16[2048,768]{1,0:T(8,128)(2,1)S(1)} %copy-done, bf16[256,2048]{1,0:T(8,128)(2,1)} %all-gather.3.cloned.1.call-done, f32[2048]{0:T(1024)} %param.17, f32[256]{0:T(256)S(1)} %add_rsqrt_fusion.1), kind=kOutput, calls=%fused_computation.38 | convolution fusion | flops 807075840 | bytes 4989952 | tf_op jit(solution)/shard_map/dot_general | solution.py:156
  37.6 2.3 %copy.30 = f32[256,768]{0,1:T(8,128)} copy(f32[256,768]{1,0:T(8,128)} %convolution_multiply_fusion) | data formatting | bytes 1572864 | tf_op jit(solution)/shard_map/mul | solution.py:177
  39.9 1.7 convolution_multiply_fusion.4
  41.6 0.2 multiply_cosine_fusion
  41.8 22.9 %all_gather.11 = bf16[4096,64]{0,1:T(8,128)(2,1)S(1)} all-gather(bf16[256,64]{0,1:T(8,128)(2,1)S(1)} %pad_maximum_fusion.3), channel_id=1, replica_groups=mesh['sp'=16,'tp'=2] {'sp'}, dimensions={0}, use_global_device_ids=true | all-gather | bytes 557056 | tf_op jit(solution)/shard_map/all_gather | solution.py:207
  64.7 0.8 copy.44
  65.5 1.8 %slice.64 = bf16[256,4,128]{0,2,1:T(8,128)(2,1)} slice(f32[256,4,192]{0,2,1:T(8,128)} %bitcast.110), slice={[0:256], [0:4], [0:128]} | slice | bytes 524288 | tf_op jit(solution)/shard_map/slice | solution.py:178
  67.3 1.1 copy.32
  68.4 1.9 %multiply_reduce_fusion = (f32[256]{0:T(256)S(1)}, f32[256,128]{0,1:T(8,128)S(1)}) fusion(bf16[2048,128]{1,0:T(8,128)(2,1)} %param.23, bf16[256,2048]{1,0:T(8,128)(2,1)} %all-gather.3.cloned.1.call-done, f32[2048]{0:T(1024)} %param.17), kind=kOutput, calls=%fused_computation.67 | convolution fusion | flops 135855872 | bytes 1713152 | tf_op jit(solution)/shard_map/dot_general | solution.py:156
  70.3 1.4 multiply_convert_fusion
  71.7 0.0 all-gather.5.cloned.1.call-update
  71.7 0.0 reduce-scatter.2.cloned.1.call-start
  71.8 0.0 copy-start.14
  71.8 2.3 %fusion.34 = bf16[256,256]{0,1:T(8,128)(2,1)S(1)} fusion(bf16[2048,256]{1,0:T(8,128)(2,1)} %param.20, bf16[256,2048]{1,0:T(8,128)(2,1)} %all-gather.3.cloned.1.call-done, f32[2048]{0:T(1024)} %param.17, f32[256]{0:T(256)S(1)} %copy-done.13), kind=kOutput, calls=%fused_computation.45 | convolution fusion | flops 270139392 | bytes 2237440 | tf_op jit(solution)/shard_map/dot_general | solution.py:156
  74.1 2.2 %fusion.33 = bf16[256,256]{0,1:T(8,128)(2,1)S(1)} fusion(bf16[2048,256]{1,0:T(8,128)(2,1)} %param.19, bf16[256,2048]{1,0:T(8,128)(2,1)} %all-gather.3.cloned.1.call-done, f32[2048]{0:T(1024)} %param.17, f32[256]{0:T(256)S(1)} %copy-done.13), kind=kOutput, calls=%fused_computation.44 | convolution fusion | flops 270139392 | bytes 2237440 | tf_op jit(solution)/shard_map/dot_general | solution.py:156
  76.3 0.7 fusion.52
  77.0 2.9 %collective-permute-start = (bf16[128,512]{0,1:T(8,128)(2,1)}, bf16[128,512]{0,1:T(8,128)(2,1)}, u32[]{:S(2)}, u32[]{:S(2)}) collective-permute-start(bf16[128,512]{0,1:T(8,128)(2,1)} %get-tuple-element.141), channel_id=1, source_target_pairs={{0,2},{2,4},{4,6},{6,8},{8,10},{10,12},{12,14},{14,16},{16,18},{18... | collective-permute-start | bytes 393224 | tf_op jit(solution)/shard_map/ppermute | solution.py:28
  79.9 1.3 collective-permute-start.1
  81.2 1.4 fusion.32
  82.7 1.7 subtract_convert_fusion
  84.3 1.8 %copy.28 = bf16[256,512]{0,1:T(8,128)(2,1)} copy(bf16[256,512]{1,0:T(8,128)(2,1)} %fusion.32) | data formatting | bytes 524288 | tf_op jit(solution)/shard_map/convert_element_type | solution.py:165
  86.1 0.9 pad_maximum_fusion.2
  87.0 0.0 copy-start.5
  87.0 0.0 collective-permute-done
  87.0 0.0 collective-permute-done.1
  87.0 1.2 pad_maximum_fusion
  88.3 2.5 %fusion.23 = (f32[4,2,256]{2,1,0:T(2,128)S(1)}, f32[4,512,256,2]{2,1,3,0:T(8,128)S(1)}) fusion(f32[256,512]{0,1:T(8,128)} %fusion.41, f32[4,2]{1,0:T(4,128)S(1)} %copy-done.11, pred[256,512]{0,1:T(8,128)(4,1)} %fusion.44, bf16[512,4,64,1]{0,2,3,1:T(8,128)(2,1)S(1)} %bitcast.117, bf16[256,4,2,64]{0,3,2,1:T(8,128)(2,1)} %bitcast.115), kind=kOutput, calls=%fused_computation.33 | convolution fusion | flops 139458560 | bytes 5382176 | tf_op jit(solution)/shard_map/qhgd,khd->hgqk/dot_general | solution.py:64
  90.8 0.1 broadcast_maximum_fusion
  90.9 1.2 fusion.20
  92.1 0.1 add_bitcast_fusion
  92.2 0.0 copy-start.6
  92.2 1.4 fusion.38
  93.6 0.2 copy-done.6
  93.8 2.1 %fusion.61 = f32[256,2048]{1,0:T(8,128)} fusion(bf16[256,512]{0,1:T(8,128)(2,1)S(1)} %bitcast.114, bf16[512,2048]{1,0:T(8,128)(2,1)S(1)} %copy-done.6), kind=kOutput, calls=%fused_computation.89 | convolution fusion | flops 536870912 | bytes 4456448 | tf_op jit(solution)/shard_map/dot_general | solution.py:219
  95.9 9.1 %all-gather.5.cloned.1.call-done = bf16[4096,128]{0,1:T(8,128)(2,1)} async-done(((bf16[256,128]{0,1:T(8,128)(2,1)}), bf16[4096,128]{0,1:T(8,128)(2,1)}) %all-gather.5.cloned.1.call-update) | async-done | bytes 1048592 | tf_op jit(solution)/shard_map/all_gather | solution.py:206
  105.0 2.3 %copy.41 = bf16[4096,128]{1,0:T(8,128)(2,1)} copy(bf16[4096,128]{0,1:T(8,128)(2,1)} %all-gather.5.cloned.1.call-done) | data formatting | bytes 2097152
  107.3 34.6 %while.15 = (s32[]{:T(128)}, f32[4,256]{1,0:T(4,128)S(1)}, f32[4,256]{1,0:T(4,128)S(1)}, f32[4,256,128]{2,1,0:T(8,128)}, bf16[2,2048,128]{2,1,0:T(8,128)(2,1)}, ...) while((s32[]{:T(128)}, f32[4,256]{1,0:T(4,128)S(1)}, ...), condition=%wide.region_7.8_spmd.clone, body=%wide.region_4.7_spmd.clone.sunk | while | flops 1896223744 | bytes 93258992 | solution.py:131
  107.3 1.8 %convolution_convert_fusion.4 = bf16[2048,512]{0,1:T(8,128)(2,1)S(1)} fusion(bf16[128,512]{1,0:T(8,128)(2,1)} %get-tuple-element.255, bf16[2,2048,128]{2,1,0:T(8,128)(2,1)} %get-tuple-element.254, s32[]{:T(128)} %get-tuple-element.238), kind=kOutput, calls=%fused_computation.8.clone.1 | convolution fusion | flops 269484032 | bytes 2753024 | tf_op jit(solution)/shard_map/while/body/eval_jaxpr/dot_general | solution.py:190
  109.1 1.3 fusion.104
  110.4 4.5 %fusion.105 = (f32[4,256]{1,0:T(4,128)S(1)}, f32[4,256,2048]{1,2,0:T(8,128)}) fusion(bf16[256,4,64]{0,2,1:T(8,128)(2,1)S(1)} %get-tuple-element.258, bf16[2,2048,64]{1,2,0:T(8,128)(2,1)S(1)} %copy-done.4, s32[]{:T(128)} %get-tuple-element.238, f32[4,2048,256]{2,1,0:T(8,128)S(1)} %fusion.104), kind=kOutput, calls=%fused_computation.86.clone.1 | convolution fusion | flops 274725888 | bytes 17174532 | tf_op jit(solution)/shard_map/while/body/eval_jaxpr/qhd,kd->hqk/dot_general | solution.py:102
  114.9 4.6 %fusion.106 = f32[4,256]{1,0:T(4,128)S(1)} fusion(f32[4,256,2048]{1,2,0:T(8,128)} %get-tuple-element.223, f32[4,256]{1,0:T(4,128)S(1)} %select_maximum_fusion.2), kind=kLoop, calls=%fused_computation.4.clone.1 | loop fusion | flops 4193280 | bytes 8396800 | tf_op jit(solution)/shard_map/while/body/eval_jaxpr/reduce_sum | solution.py:109
  119.6 2.1 %convolution_convert_fusion.5 = bf16[2048,512]{0,1:T(8,128)(2,1)S(1)} fusion(bf16[128,512]{1,0:T(8,128)(2,1)} %get-tuple-element.259, bf16[2,2048,128]{2,1,0:T(8,128)(2,1)} %get-tuple-element.254, s32[]{:T(128)} %get-tuple-element.238), kind=kOutput, calls=%fused_computation.7.clone.1 | convolution fusion | flops 269484032 | bytes 2753024 | tf_op jit(solution)/shard_map/while/body/eval_jaxpr/dot_general | solution.py:193
  121.7 2.1 %fusion.108 = f32[4,256,128]{2,1,0:T(8,128)S(1)} fusion(bf16[2048,4,128]{0,2,1:T(8,128)(2,1)S(1)} %bitcast.106, f32[4,256,2048]{1,2,0:T(8,128)S(1)} %copy-done.1, f32[4,256]{1,0:T(4,128)S(1)} %select_maximum_fusion.2, f32[4,256,128]{2,1,0:T(8,128)S(1)} %copy-done.2, f32[4,256]{1,0:T(4,128)S(1)} %get-tuple-element.225, pred[]{:T(512)S(6)} %compare.3), kind=kOutput, calls=%fused_computation.9.clone.1 | convolution fusion | flops 541458432 | bytes 11542529 | tf_op jit(solution)/shard_map/while/body/eval_jaxpr/hqk,khd->hqd/dot_general | solution.py:110
  123.8 0.8 copy-done.3
  124.6 1.8 %convolution_convert_fusion.4 = bf16[2048,512]{0,1:T(8,128)(2,1)S(1)} fusion(bf16[128,512]{1,0:T(8,128)(2,1)} %get-tuple-element.255, bf16[2,2048,128]{2,1,0:T(8,128)(2,1)} %get-tuple-element.254, s32[]{:T(128)} %get-tuple-element.238), kind=kOutput, calls=%fused_computation.8.clone.1 | convolution fusion | flops 269484032 | bytes 2753024 | tf_op jit(solution)/shard_map/while/body/eval_jaxpr/dot_general | solution.py:190
  126.4 1.3 fusion.104
  127.7 4.5 %fusion.105 = (f32[4,256]{1,0:T(4,128)S(1)}, f32[4,256,2048]{1,2,0:T(8,128)}) fusion(bf16[256,4,64]{0,2,1:T(8,128)(2,1)S(1)} %get-tuple-element.258, bf16[2,2048,64]{1,2,0:T(8,128)(2,1)S(1)} %copy-done.4, s32[]{:T(128)} %get-tuple-element.238, f32[4,2048,256]{2,1,0:T(8,128)S(1)} %fusion.104), kind=kOutput, calls=%fused_computation.86.clone.1 | convolution fusion | flops 274725888 | bytes 17174532 | tf_op jit(solution)/shard_map/while/body/eval_jaxpr/qhd,kd->hqk/dot_general | solution.py:102
  132.2 4.6 %fusion.106 = f32[4,256]{1,0:T(4,128)S(1)} fusion(f32[4,256,2048]{1,2,0:T(8,128)} %get-tuple-element.223, f32[4,256]{1,0:T(4,128)S(1)} %select_maximum_fusion.2), kind=kLoop, calls=%fused_computation.4.clone.1 | loop fusion | flops 4193280 | bytes 8396800 | tf_op jit(solution)/shard_map/while/body/eval_jaxpr/reduce_sum | solution.py:109
  136.9 2.1 %convolution_convert_fusion.5 = bf16[2048,512]{0,1:T(8,128)(2,1)S(1)} fusion(bf16[128,512]{1,0:T(8,128)(2,1)} %get-tuple-element.259, bf16[2,2048,128]{2,1,0:T(8,128)(2,1)} %get-tuple-element.254, s32[]{:T(128)} %get-tuple-element.238), kind=kOutput, calls=%fused_computation.7.clone.1 | convolution fusion | flops 269484032 | bytes 2753024 | tf_op jit(solution)/shard_map/while/body/eval_jaxpr/dot_general | solution.py:193
  139.0 2.1 %fusion.108 = f32[4,256,128]{2,1,0:T(8,128)S(1)} fusion(bf16[2048,4,128]{0,2,1:T(8,128)(2,1)S(1)} %bitcast.106, f32[4,256,2048]{1,2,0:T(8,128)S(1)} %copy-done.1, f32[4,256]{1,0:T(4,128)S(1)} %select_maximum_fusion.2, f32[4,256,128]{2,1,0:T(8,128)S(1)} %copy-done.2, f32[4,256]{1,0:T(4,128)S(1)} %get-tuple-element.225, pred[]{:T(512)S(6)} %compare.3), kind=kOutput, calls=%fused_computation.9.clone.1 | convolution fusion | flops 541458432 | bytes 11542529 | tf_op jit(solution)/shard_map/while/body/eval_jaxpr/hqk,khd->hqd/dot_general | solution.py:110
  141.1 0.8 copy-done.3
  141.9 2.0 %copy.34 = f32[4,256,128]{1,2,0:T(8,128)} copy(f32[4,256,128]{2,1,0:T(8,128)} %get-tuple-element.58) | data formatting | bytes 1048576 | tf_op jit(solution)/shard_map/while | solution.py:131
  143.9 1.1 divide_convert_fusion
  145.0 3.9 %fusion.22 = bf16[256,2048]{1,0:T(8,128)(2,1)} fusion(f32[256,2048]{1,0:T(8,128)} %fusion.61, bf16[256,512]{0,1:T(8,128)(2,1)S(1)} %bitcast.113, bf16[512,2048]{1,0:T(8,128)(2,1)} %param.29), kind=kOutput, calls=%fused_computation.32 | convolution fusion | flops 537919488 | bytes 5505024 | tf_op jit(solution)/shard_map/dot_general | solution.py:219
  148.9 0.0 reduce-scatter.2.cloned.1.call-update
  149.0 20.1 %reduce-scatter.2.cloned.1.call-done = bf16[256,1024]{1,0:T(8,128)(2,1)} async-done(((bf16[256,2048]{1,0:T(8,128)(2,1)}), bf16[256,1024]{1,0:T(8,128)(2,1)}) %reduce-scatter.2.cloned.1.call-update) | async-done | bytes 524304 | tf_op jit(solution)/shard_map/reduce_scatter | solution.py:222
  (54 shorter events, 0.2 us)
Async XLA Ops:
  6.5 27.9 %copy-start = (bf16[2048,768]{1,0:T(8,128)(2,1)S(1)}, bf16[2048,768]{1,0:T(8,128)(2,1)}, u32[]{:S(2)}) copy-start(bf16[2048,768]{1,0:T(8,128)(2,1)} %param.22) | copy-start | bytes 9437188
  6.5 26.4 %all-gather.3.cloned.1.call-start = ((), (), s32[]{:S(2)}) async-start(), calls=%async_computation.1 | async-start | bytes 1572864 | tf_op jit(solution)/shard_map/all_gather | solution.py:152
  7.3 97.8 %all-gather.5.cloned.1.call-start = ((), (), s32[]{:S(2)}) async-start(), calls=%async_computation.2 | async-start | bytes 1114112 | tf_op jit(solution)/shard_map/all_gather | solution.py:206
  10.7 29.1 %copy-start.15 = (f32[2048]{0:T(1024)S(1)}, f32[2048]{0:T(1024)}, u32[]{:S(2)}) copy-start(f32[2048]{0:T(1024)} %param.17) | copy-start | bytes 24580
  34.4 7.1 %copy-start.12 = (f32[256]{0:T(256)}, f32[256]{0:T(256)S(1)}, u32[]{:S(2)}) copy-start(f32[256]{0:T(256)S(1)} %add_rsqrt_fusion.1) | copy-start | bytes 3076
  41.8 30.0 %copy-start.13 = (f32[256]{0:T(256)S(1)}, f32[256]{0:T(256)}, u32[]{:S(2)}) copy-start(f32[256]{0:T(256)} %copy-done.12) | copy-start | bytes 3076
  65.5 15.7 %copy-start.16 = (f32[2048]{0:T(1024)S(1)}, f32[2048]{0:T(1024)}, u32[]{:S(2)}) copy-start(f32[2048]{0:T(1024)} %param.17) | copy-start | bytes 24580
  71.7 97.4 %reduce-scatter.2.cloned.1.call-start = ((), (), s32[]{:S(2)}) async-start(), calls=%async_computation.3 | async-start | bytes 1572864 | tf_op jit(solution)/shard_map/reduce_scatter | solution.py:222
  71.7 9.5 %copy-start.7 = (bf16[256,2048]{1,0:T(8,128)(2,1)S(1)}, bf16[256,2048]{1,0:T(8,128)(2,1)}, u32[]{:S(2)}) copy-start(bf16[256,2048]{1,0:T(8,128)(2,1)} %all-gather.3.cloned.1.call-done) | copy-start | bytes 3145732
  71.8 9.5 %copy-start.14 = (bf16[2048,512]{1,0:T(8,128)(2,1)S(1)}, bf16[2048,512]{1,0:T(8,128)(2,1)}, u32[]{:S(2)}) copy-start(bf16[2048,512]{1,0:T(8,128)(2,1)} %param.18) | copy-start | bytes 6291460
  74.0 8.6 %copy-start.9 = (bf16[256,256]{0,1:T(8,128)(2,1)}, bf16[256,256]{0,1:T(8,128)(2,1)S(1)}, u32[]{:S(2)}) copy-start(bf16[256,256]{0,1:T(8,128)(2,1)S(1)} %fusion.34) | copy-start | bytes 393220
  76.2 6.4 %copy-start.10 = (bf16[256,256]{0,1:T(8,128)(2,1)}, bf16[256,256]{0,1:T(8,128)(2,1)S(1)}, u32[]{:S(2)}) copy-start(bf16[256,256]{0,1:T(8,128)(2,1)S(1)} %fusion.33) | copy-start | bytes 393220
  76.3 12.0 %copy-start.11 = (f32[4,2]{1,0:T(4,128)S(1)}, f32[4,2]{1,0:T(4,128)}, u32[]{:S(2)}) copy-start(f32[4,2]{1,0:T(4,128)} %multiply_exponential_fusion) | copy-start | bytes 100
  77.0 10.0 %collective-permute-start = (bf16[128,512]{0,1:T(8,128)(2,1)}, bf16[128,512]{0,1:T(8,128)(2,1)}, u32[]{:S(2)}, u32[]{:S(2)}) collective-permute-start(bf16[128,512]{0,1:T(8,128)(2,1)} %get-tuple-element.141), channel_id=1, source_target_pairs={{0,2},{2,4},{4,6},{6,8},{8,10},{10,12},{12,14},{14,16},{16,18},{18... | collective-permute-start | bytes 393224 | tf_op jit(solution)/shard_map/ppermute | solution.py:28
  79.9 7.1 %collective-permute-start.1 = (bf16[128,512]{0,1:T(8,128)(2,1)}, bf16[128,512]{0,1:T(8,128)(2,1)}, u32[]{:S(2)}, u32[]{:S(2)}) collective-permute-start(bf16[128,512]{0,1:T(8,128)(2,1)} %get-tuple-element.142), channel_id=1, source_target_pairs={{2,0},{4,2},{6,4},{8,6},{10,8},{12,10},{14,12},{16,14},{18,16},{20... | collective-permute-start | bytes 393224 | tf_op jit(solution)/shard_map/ppermute | solution.py:30
  87.0 3.9 %copy-start.5 = (f32[256,512]{0,1:T(8,128)S(1)}, f32[256,512]{0,1:T(8,128)}, u32[]{:S(2)}) copy-start(f32[256,512]{0,1:T(8,128)} %fusion.41) | copy-start | bytes 1572868
  87.0 3.9 %copy-start.8 = (pred[256,512]{0,1:T(8,128)(4,1)S(1)}, pred[256,512]{0,1:T(8,128)(4,1)}, u32[]{:S(2)}) copy-start(pred[256,512]{0,1:T(8,128)(4,1)} %fusion.44) | copy-start | bytes 393220
  92.2 1.6 copy-start.6
  109.1 1.3 copy-start.4
  114.9 6.7 %copy-start.1 = (f32[4,256,2048]{1,2,0:T(8,128)S(1)}, f32[4,256,2048]{1,2,0:T(8,128)}, u32[]{:S(2)}) copy-start(f32[4,256,2048]{1,2,0:T(8,128)} %get-tuple-element.223) | copy-start | bytes 25165828 | tf_op jit(solution)/shard_map/while
  114.9 6.7 %copy-start.2 = (f32[4,256,128]{2,1,0:T(8,128)S(1)}, f32[4,256,128]{2,1,0:T(8,128)}, u32[]{:S(2)}) copy-start(f32[4,256,128]{2,1,0:T(8,128)} %get-tuple-element.241) | copy-start | bytes 1572868 | tf_op jit(solution)/shard_map/while
  123.8 0.8 copy-start.3
  126.4 1.3 copy-start.4
  132.2 6.7 %copy-start.1 = (f32[4,256,2048]{1,2,0:T(8,128)S(1)}, f32[4,256,2048]{1,2,0:T(8,128)}, u32[]{:S(2)}) copy-start(f32[4,256,2048]{1,2,0:T(8,128)} %get-tuple-element.223) | copy-start | bytes 25165828 | tf_op jit(solution)/shard_map/while
  132.2 6.7 %copy-start.2 = (f32[4,256,128]{2,1,0:T(8,128)S(1)}, f32[4,256,128]{2,1,0:T(8,128)}, u32[]{:S(2)}) copy-start(f32[4,256,128]{2,1,0:T(8,128)} %get-tuple-element.241) | copy-start | bytes 1572868 | tf_op jit(solution)/shard_map/while
  141.1 0.8 copy-start.3
Sparse Core Ops, SparseCore 0:
  8.9 23.9 all-gather.2
  71.8 33.1 all-gather.4
  149.1 19.9 reduce-scatter.1
where the time goes:
time: 176 us
  waiting for transfers between devices  52.2 us (30%)
  matrix products  46 us (26%)
  blocking collectives  22.9 us (13%)
  other arithmetic  21.9 us (12%)
  local copies, waits for them, and re-layouts  14.9 us (8%)
  between operations  13.4 us (8%)
  starting transfers between devices  4.27 us (2%)
    all_gather x1, blocking collectives, per_device(): lax.all_gather(key_rotary, 'sp', axis=0, tiled=True)  22.9 us
    all_gather x1, waiting for transfers between devices, per_device(): lax.all_gather(activations, 'tp', axis=1, tiled=True).astype(jnp.float32)  22.2 us
    reduce_scatter x1, waiting for transfers between devices, per_device(): lax.psum_scatter(terms.astype(jnp.bfloat16), 'tp', scatter_dimension=1, t...  20.1 us
    dot_general x6, matrix products, per_device(): jnp.dot(normalized, weight, preferred_element_type=jnp.float32)  12.6 us
    reduce_sum x2, other arithmetic, latent_step(): totals = totals * factor + jnp.sum(weights, axis=2)  9.28 us
    all_gather x1, waiting for transfers between devices, per_device(): lax.all_gather(latent, 'sp', axis=0, tiled=True)  9.12 us
    dot_general x2, matrix products, latent_step(): jnp.einsum('qhd,kd->hqk', query_turned, keys_turned, preferred_element_ty...  9.05 us
    dot_general x2, matrix products, latent_step(): jnp.einsum('hqk,khd->hqd', weights.astype(jnp.bfloat16), values_plain.res...  4.13 us
  transfers between devices with their start and end apart: 5, of which 3 were waited for; matrix products, arithmetic and copies ran while one was open for 13% of the time, Pallas kernels for 0%

commit v1 on v0

--- a/solution.py
+++ b/solution.py
@@ -3,6 +3,8 @@
 import jax
 import jax.numpy as jnp
 from jax import lax
+from jax.experimental import pallas as pl
+from jax.experimental.pallas import tpu as pltpu
 from jax.sharding import PartitionSpec as P
 
 HEADS_A = 16
@@ -15,6 +17,13 @@
 
 EPSILON = 1e-06
 ROPE_BASE = 10000.0
+LOG2E = 1.4426950408889634
+LANES = 128
+MASKED = -1e30
+
+
+F32 = jnp.float32
+BF16 = jnp.bfloat16
 
 
 def padded_2(cells, sides, width):
@@ -131,7 +140,7 @@
     return lax.scan(one_block, running, stacked)[0]
 
 
-def per_device(
+def per_device_wide(
     activations,
     norm_gain,
     win_query,
@@ -196,7 +205,7 @@
             key_block[1],
         )
 
-    row_peak, totals_lat, weighted = over_blocks(
+    _, totals_lat, weighted = over_blocks(
         (
             jnp.full((head_count, tok_rows), -jnp.inf, jnp.float32),
             jnp.zeros((head_count, tok_rows), jnp.float32),
@@ -222,9 +231,321 @@
     return lax.psum_scatter(terms.astype(jnp.bfloat16), "tp", scatter_dimension=1, tiled=True)
 
 
+def dot(a, b, dims=((1,), (0,))):
+    return lax.dot_general(a, b, (dims, ((), ())), preferred_element_type=F32)
+
+
+def whole(count):
+    return [pl.BlockSpec(memory_space=pltpu.VMEM)] * count
+
+
+def scalars(count):
+    return [pl.BlockSpec(memory_space=pltpu.SMEM)] * count
+
+
+def call(body, shapes, smem, operands, flops, mib):
+    single = not isinstance(shapes, (list, tuple))
+    outs = [shapes] if single else list(shapes)
+    result = pl.pallas_call(
+        body,
+        out_shape=outs,
+        in_specs=scalars(len(smem)) + whole(len(operands)),
+        out_specs=whole(len(outs)),
+        cost_estimate=pl.CostEstimate(
+            flops=int(flops),
+            bytes_accessed=sum(x.size * x.dtype.itemsize for x in operands),
+            transcendentals=0,
+        ),
+        compiler_params=pltpu.CompilerParams(vmem_limit_bytes=mib * 2**20),
+    )(*smem, *operands)
+    return result[0] if single else result
+
+
+def compress_body(part_ref, x_ref, gain_ref, down_ref, rope_ref, norm_ref, own_ref, send_ref):
+    rows, half = x_ref.shape
+    start = pl.multiple_of(part_ref[0] * half, half)
+    wide = x_ref[...].astype(F32)
+    normalized = (wide * gain_ref[:, pl.ds(start, half)]).astype(BF16)
+    norm_ref[...] = normalized
+    compressed = dot(normalized, down_ref[pl.ds(start, half), :])
+    rope = dot(normalized, rope_ref[pl.ds(start, half), :])
+    squares = jnp.sum(wide * wide, axis=1, keepdims=True)
+    high = squares.astype(BF16).astype(F32)
+    lane = lax.broadcasted_iota(jnp.int32, (rows, LANES), 1)
+    rope = jnp.concatenate([rope, jnp.zeros((rows, LANES - rope.shape[1]), F32)], axis=1)
+    width = compressed.shape[1]
+    own_ref[:, :width] = compressed
+    own_ref[:, width:] = jnp.where(lane == LANES - 1, squares, jnp.where(lane == LANES - 2, 0.0, rope))
+    send_ref[:, :width] = compressed.astype(BF16)
+    send_ref[:, width:] = jnp.where(
+        lane == LANES - 1, high, jnp.where(lane == LANES - 2, squares - high, rope)
+    ).astype(BF16)
+
+
+def turn(vectors, cosines, sines):
+    half = vectors.shape[1] // 2
+    swapped = jnp.concatenate([vectors[:, half:], vectors[:, :half]], axis=1)
+    return vectors * cosines + swapped * sines
+
+
+def latent_body(own_ref, got_ref, table_ref, gain_ref, block_ref, scale_ref, *, features):
+    rows = own_ref.shape[0]
+    total = own_ref[...] + got_ref[...].astype(F32)
+    width = gain_ref.shape[1]
+    compressed = total[:, :width]
+    rest = total[:, width:]
+    squares = rest[:, LANES - 1 :] + rest[:, LANES - 2 : LANES - 1]
+    row_scale = lax.rsqrt(squares / features + EPSILON)
+    scale_ref[...] = jnp.broadcast_to(row_scale, scale_ref.shape)
+    mean = jnp.mean(compressed * compressed, axis=1, keepdims=True)
+    block_ref[:rows] = (compressed * lax.rsqrt(mean + EPSILON) * gain_ref[...]).astype(BF16)
+    rope = turn(rest[:, :D_ROPE] * row_scale, table_ref[:, :D_ROPE], table_ref[:, D_ROPE:])
+    packed = jnp.concatenate([rope[: rows // 2], rope[rows // 2 :]], axis=1)
+    block_ref[rows:] = packed.astype(BF16)
+
+
+def project_body(
+    part_ref, own_ref, got_ref, scale_ref, table_ref, wq_ref, wk_ref, wv_ref, wl_ref, up_ref,
+    q_ref, kv_ref, qa_ref, qb_ref,
+):
+    rows, half = own_ref.shape
+    part = part_ref[0]
+    mine = pl.multiple_of(part * half, half)
+    theirs = pl.multiple_of((1 - part) * half, half)
+    own = own_ref[...]
+    got = got_ref[...]
+    row_scale = scale_ref[:, :1]
+
+    def project(w_ref):
+        return (
+            dot(own, w_ref[pl.ds(mine, half), :]) + dot(got, w_ref[pl.ds(theirs, half), :])
+        ) * row_scale
+
+    width = wk_ref.shape[1]
+    kv_ref[:, :width] = project(wk_ref).astype(BF16)
+    kv_ref[:, width:] = project(wv_ref).astype(BF16)
+    q_ref[...] = (project(wq_ref) * (DH**-0.5 * LOG2E)).astype(BF16)
+    queries = project(wl_ref)
+    step = UNROTATED_WIDTH + D_ROPE
+    scale = step**-0.5 * LOG2E
+    row = lax.broadcasted_iota(jnp.int32, (LANES, LANES), 0)
+    col = lax.broadcasted_iota(jnp.int32, (LANES, LANES), 1)
+    unit = jnp.where(row == col, 1.0, 0.0).astype(BF16)
+    blank = jnp.zeros((rows, LANES - D_ROPE), F32)
+    chunks = qa_ref.shape[0]
+    span = rows // chunks
+    lat = up_ref.shape[0]
+    for head in range(wl_ref.shape[1] // step):
+        plain = queries[:, head * step : head * step + UNROTATED_WIDTH].astype(BF16)
+        up = up_ref[:, head * UNROTATED_WIDTH : (head + 1) * UNROTATED_WIDTH]
+        low = (dot(up, plain, ((1,), (1,))) * scale).astype(BF16)
+        turned = queries[:, head * step + UNROTATED_WIDTH : (head + 1) * step]
+        turned = turn(turned, table_ref[:, :D_ROPE], table_ref[:, D_ROPE:]) * scale
+        first = jnp.concatenate([turned, blank], axis=1).astype(BF16)
+        second = jnp.concatenate([blank, turned], axis=1).astype(BF16)
+        first = dot(unit, first, ((1,), (1,))).astype(BF16)
+        second = dot(unit, second, ((1,), (1,))).astype(BF16)
+        for c in range(chunks):
+            cols = slice(head * span, (head + 1) * span)
+            rowsl = slice(c * span, (c + 1) * span)
+            qa_ref[c, :lat, cols] = low[:, rowsl]
+            qb_ref[c, :lat, cols] = low[:, rowsl]
+            qa_ref[c, lat:, cols] = first[:, rowsl]
+            qb_ref[c, lat:, cols] = second[:, rowsl]
+
+
+def attend_body(
+    place_ref, sink_ref, *refs, groups, chunk, rows,
+):
+    blocks = refs[:groups]
+    (
+        qa_ref, qb_ref, q_ref, prev_ref, kv_ref, next_ref, up_ref, ow_ref, ol_ref,
+        send_ref, keep_ref, _, cat_ref,
+    ) = refs[groups:]
+    span = q_ref.shape[0] // qa_ref.shape[0]
+    half = rows // 2
+    unit = rows + half
+    columns = qa_ref.shape[2]
+    lat = LANES
+    peak = jnp.full((1, columns), MASKED, F32)
+    total = jnp.zeros((1, columns), F32)
+    weighted = jnp.zeros((lat, columns), F32)
+    for block in blocks:
+        count = block.shape[0] // unit
+        cut = block[...].reshape(count, unit, LANES)
+        rope = cut[:, rows:].reshape(count * half, LANES)
+        first = cut[:, :half].reshape(count * half, LANES)
+        second = cut[:, half:rows].reshape(count * half, LANES)
+        for keys, table in ((first, qa_ref), (second, qb_ref)):
+            score = dot(jnp.concatenate([keys, rope], axis=1), table[chunk])
+            top = jnp.maximum(peak, jnp.max(score, axis=0, keepdims=True))
+            factor = jnp.exp2(peak - top)
+            weight = jnp.exp2(score - top)
+            total = total * factor + jnp.sum(weight, axis=0, keepdims=True)
+            weighted = weighted * factor + dot(keys, weight.astype(BF16), ((0,), (0,)))
+            peak = top
+    mixed = (weighted / total).astype(BF16)
+
+    heads_l = columns // span
+    q = q_ref[chunk * span : (chunk + 1) * span, :]
+    heads = q.shape[1] // DH
+    width = kv_ref.shape[1] // 2
+    key_heads = width // DH
+    group = heads // key_heads
+    padded = jnp.concatenate([prev_ref[...], kv_ref[...], next_ref[...]], axis=0)
+    padded = padded[chunk * span : (chunk + 1) * span + 2 * WINDOW]
+    offset = place_ref[0]
+    key_pos = lax.broadcasted_iota(jnp.int32, (span + 2 * WINDOW, span), 0) - WINDOW
+    query_pos = lax.broadcasted_iota(jnp.int32, (span + 2 * WINDOW, span), 1)
+    distance = jnp.abs(key_pos - query_pos)
+    spot = key_pos + (offset + chunk * span)
+    inside = (distance <= WINDOW) & (spot >= 0) & (spot < place_ref[1])
+    distance = distance.astype(F32)
+    for g in range(key_heads):
+        keys = padded[:, g * DH : (g + 1) * DH]
+        values = padded[:, width + g * DH : width + (g + 1) * DH]
+        for j in range(group):
+            head = g * group + j
+            score = dot(keys, q[:, head * DH : (head + 1) * DH], ((1,), (1,)))
+            score = jnp.where(inside, score - sink_ref[1, head] * distance, MASKED)
+            sink = sink_ref[0, head]
+            top = jnp.maximum(jnp.max(score, axis=0, keepdims=True), sink)
+            weight = jnp.exp2(score - top)
+            total = jnp.sum(weight, axis=0, keepdims=True) + jnp.exp2(sink - top)
+            out = dot(values, weight.astype(BF16), ((0,), (0,))) / total
+            cat_ref[head * DH : (head + 1) * DH, :] = out.astype(BF16)
+    base = heads * DH
+    for head in range(heads_l):
+        up = up_ref[:, head * VALUE_WIDTH : (head + 1) * VALUE_WIDTH]
+        out = dot(up, mixed[:, head * span : (head + 1) * span], ((0,), (0,)))
+        cat_ref[base + head * VALUE_WIDTH : base + (head + 1) * VALUE_WIDTH, :] = out.astype(BF16)
+    keep = keep_ref.shape[1]
+    part = place_ref[2]
+    mine = pl.multiple_of(part * keep, keep)
+    theirs = pl.multiple_of((1 - part) * keep, keep)
+    win = cat_ref[:base, :]
+    low = cat_ref[base:, :]
+
+    def out_of(start):
+        return dot(win, ow_ref[:, pl.ds(start, keep)], ((0,), (0,))) + dot(
+            low, ol_ref[:, pl.ds(start, keep)], ((0,), (0,))
+        )
+
+    send_ref[...] = out_of(theirs).astype(BF16)
+    keep_ref[...] = out_of(mine)
+
+
+def swap(cells, axis, bit):
+    count = lax.axis_size(axis)
+    return lax.ppermute(cells, axis, [(i, i ^ bit) for i in range(count)])
+
+
+def gather(block):
+    count = lax.axis_size("sp")
+    if count % 4 or count > 16 or count & (count - 1):
+        return (lax.all_gather(block, "sp", axis=0, tiled=True),)
+    line = [block] + [swap(block, "sp", 4 * k) for k in reversed(range(1, count // 4))]
+    near = swap(block, "sp", 2)
+    line = jnp.concatenate(line, axis=0)
+    far = swap(line[block.shape[0] :], "sp", 2) if count > 4 else line[:0]
+    mine = jnp.concatenate([line, near, far], axis=0)
+    return (mine, swap(mine, "sp", 1))
+
+
+def per_device(
+    activations,
+    norm_gain,
+    win_query,
+    win_key,
+    win_value,
+    sink_logit,
+    lat_query,
+    key_value_down_weight,
+    rope_key,
+    latent_norm_gain,
+    key_up_weight,
+    value_up_weight,
+    out_win,
+    out_lat,
+):
+    rows, half = activations.shape
+    features = norm_gain.shape[0]
+    part = lax.axis_index("tp").astype(jnp.int32)
+    count = lax.axis_size("sp")
+    offset = lax.axis_index("sp").astype(jnp.int32) * rows
+    shape = jax.ShapeDtypeStruct
+
+    places = (offset + jnp.arange(rows, dtype=jnp.int32)).astype(F32)
+    angles = rotary_angles(places, D_ROPE)
+    cosines, sines = jnp.cos(angles), jnp.sin(angles)
+    table = jnp.concatenate([cosines, cosines, -sines, sines], axis=1)
+
+    lat = key_value_down_weight.shape[1]
+    normalized, own, send = call(
+        compress_body,
+        [shape((rows, half), BF16), shape((rows, lat + LANES), F32), shape((rows, lat + LANES), BF16)],
+        [part[None]],
+        [activations, norm_gain[None], key_value_down_weight, rope_key],
+        2 * rows * half * 192, 8,
+    )
+    got = swap(send, "tp", 1)
+    other = swap(normalized, "tp", 1)
+    block, row_scale = call(
+        partial(latent_body, features=features),
+        [shape((rows + rows // 2, lat), BF16), shape((rows, LANES), F32)],
+        [], [own, got, table, latent_norm_gain[None]],
+        1e6, 4,
+    )
+    blocks = gather(block)
+
+    chunks = rows // WINDOW
+    columns = lat_query.shape[1] // (UNROTATED_WIDTH + D_ROPE) * (rows // chunks)
+    queries, key_value, table_a, table_b = call(
+        project_body,
+        [
+            shape(win_query.shape[1:] and (rows, win_query.shape[1]), BF16),
+            shape((rows, win_key.shape[1] + win_value.shape[1]), BF16),
+            shape((chunks, lat + LANES, columns), BF16),
+            shape((chunks, lat + LANES, columns), BF16),
+        ],
+        [part[None]],
+        [normalized, other, row_scale, table, win_query, win_key, win_value, lat_query, key_up_weight],
+        2 * rows * features * 1792, 20,
+    )
+    after = lax.ppermute(key_value[rows - WINDOW :], "sp", [(i, i + 1) for i in range(count - 1)])
+    before = lax.ppermute(key_value[:WINDOW], "sp", [(i + 1, i) for i in range(count - 1)])
+
+    heads = sink_logit.shape[0]
+    head_ids = lax.axis_index("tp") * heads + jnp.arange(heads, dtype=jnp.int32)
+    slopes = jnp.exp2(-8.0 * (head_ids + 1).astype(F32) / HEADS_A)
+    sinks = jnp.stack([sink_logit, slopes]) * LOG2E
+    place = jnp.stack([offset, jnp.int32(rows * count), part])
+    kept = []
+    for c in range(chunks):
+        span = rows // chunks
+        send, keep = pl.pallas_call(
+            partial(attend_body, groups=len(blocks), chunk=c, rows=rows),
+            out_shape=[shape((span, half), BF16), shape((span, half), F32)],
+            in_specs=scalars(2) + whole(len(blocks) + 9),
+            out_specs=whole(2),
+            scratch_shapes=[
+                pltpu.VMEM((8, LANES), F32),
+                pltpu.VMEM((out_win.shape[0] + out_lat.shape[0], span), BF16),
+            ],
+            cost_estimate=pl.CostEstimate(flops=3 * 10**9, bytes_accessed=8 * 2**20, transcendentals=0),
+            compiler_params=pltpu.CompilerParams(vmem_limit_bytes=32 * 2**20),
+        )(
+            place, sinks, *blocks, table_a, table_b, queries, after, key_value, before,
+            value_up_weight, out_win, out_lat,
+        )
+        kept.append((keep, swap(send, "tp", 1)))
+    return jnp.concatenate([(keep + got.astype(F32)).astype(BF16) for keep, got in kept], axis=0)
+
+
 def solution(mesh):
+    body = per_device if mesh.shape["tp"] == 2 else per_device_wide
     return jax.shard_map(
-        per_device,
+        body,
         mesh=mesh,
         in_specs=(
             P("sp", "tp"),

time: 176 us -> 75.2 us (0.43)
  the two profiles are of different devices: /device:TPU:0 before, /device:TPU:5 now
where the time goes in v1:
time: 75.2 us; the launch traced here: 74.7 us
  waiting for transfers between devices  24.8 us (33%)
  Pallas kernels  20.1 us (27%)
  starting transfers between devices  14.3 us (19%)
  local copies, waits for them, and re-layouts  13.6 us (18%)
  other arithmetic  1.79 us (2%)
    ppermute x10, waiting for transfers between devices, swap(): return lax.ppermute(cells, axis, [(i, i ^ bit) for i in range(count)])  20.4 us
    pallas_call x2, Pallas kernels, per_device(): pl.pallas_call(partial(attend_body, groups=len(blocks), chunk=c, rows=row...  13.5 us
    unnamed x36, local copies, waits for them, and re-layouts  12.8 us
    ppermute x10, starting transfers between devices, swap(): return lax.ppermute(cells, axis, [(i, i ^ bit) for i in range(count)])  9.76 us
    pallas_call x3, Pallas kernels, call(): pl.pallas_call(body, out_shape=outs, in_specs=scalars(len(smem)) + whole(...  6.59 us
    ppermute x1, waiting for transfers between devices, per_device(): lax.ppermute(key_value[:WINDOW], 'sp', [(i + 1, i) for i in range(count -...  4.49 us
    ppermute x1, starting transfers between devices, per_device(): lax.ppermute(key_value[:WINDOW], 'sp', [(i + 1, i) for i in range(count -...  2.59 us
    ppermute x1, starting transfers between devices, per_device(): lax.ppermute(key_value[rows - WINDOW:], 'sp', [(i, i + 1) for i in range(...  1.92 us
  transfers between devices with their start and end apart: 12, of which 6 were waited for; matrix products, arithmetic and copies ran while one was open for 7% of the time, Pallas kernels for 16%

profile of v1, /device:TPU:5, one launch (start us, length us, event | category | flops | bytes accessed | tf_op | source)
XLA Modules:
  0.0 74.7 jit_solution(8029660376836442164)
XLA Ops:
  0.0 0.0 copy-start.10
  0.0 1.2 %copy.16.rope_ref = bf16[2048,64]{1,0:T(8,128)(2,1)S(1)} copy(bf16[2048,64]{0,1:T(8,128)(2,1)} %param.22) | data formatting | bytes 524288 | tf_op args[8]
  1.2 0.0 copy-start.4
  1.3 1.0 %copy-done.4 = bf16[256,1024]{1,0:T(8,128)(2,1)S(1)} copy-done((bf16[256,1024]{1,0:T(8,128)(2,1)S(1)}, bf16[256,1024]{1,0:T(8,128)(2,1)}, u32[]{:S(2)}) %copy-start.4) | copy-done | bytes 524312
  2.3 0.0 copy-start.5
  2.3 1.0 %copy-done.5 = bf16[2048,128]{1,0:T(8,128)(2,1)S(1)} copy-done((bf16[2048,128]{1,0:T(8,128)(2,1)S(1)}, bf16[2048,128]{1,0:T(8,128)(2,1)}, u32[]{:S(2)}) %copy-start.5) | copy-done | bytes 524312
  3.3 0.0 copy-start.9
  3.3 0.7 copy-done.9
  4.0 1.1 %shard_map.136 = (bf16[256,1024]{1,0:T(8,128)(2,1)}, f32[256,256]{1,0:T(8,128)S(1)}, bf16[256,256]{1,0:T(8,128)(2,1)}) custom-call(s32[1]{0:T(128)} %bitcast.1.part_ref, bf16[256,1024]{1,0:T(8,128)(2,1)S(1)} %copy-done.4, f32[1,2048]{1,0:T(1,128)S(1)} %bitcast.5, bf16[2048,128]{1,0:T(8,128)(2,1)S(1)} %copy-done.5, bf16[2048,64]{1,0:T(8,128)(2,1)S(1)} %copy.16.rope_ref), custom_call_target="tpu_custom_call" | custom-call | flops 100663296 | bytes 1318912 | tf_op jit(solution)/shard_map/pallas_call | solution.py:249
  5.1 0.0 copy-start
  5.1 1.2 %collective-permute-start = (bf16[256,256]{1,0:T(8,128)(2,1)}, bf16[256,256]{1,0:T(8,128)(2,1)}, u32[]{:S(2)}, u32[]{:S(2)}) collective-permute-start(bf16[256,256]{1,0:T(8,128)(2,1)} %get-tuple-element.19), channel_id=1, source_target_pairs={{0,1},{1,0},{2,3},{3,2},{4,5},{5,4},{6,7},{7,6},{8,9},{9,8},{10,11... | collective-permute-start | bytes 393224 | tf_op jit(solution)/shard_map/ppermute | solution.py:440
  6.3 0.3 collective-permute-start.7
  6.6 0.5 multiply_cosine_fusion
  7.2 0.2 pad_maximum_fusion.2.table_ref
  7.3 2.5 %collective-permute-done.got_ref = bf16[256,256]{1,0:T(8,128)(2,1)} collective-permute-done((bf16[256,256]{1,0:T(8,128)(2,1)}, bf16[256,256]{1,0:T(8,128)(2,1)}, u32[]{:S(2)}, u32[]{:S(2)}) %collective-permute-start) | collective-permute-done | bytes 131104 | tf_op jit(solution)/shard_map/ppermute | solution.py:440
  9.8 0.0 copy-done.10
  9.8 1.3 %shard_map.137 = (bf16[384,128]{1,0:T(8,128)(2,1)S(1)}, f32[256,128]{1,0:T(8,128)S(1)}) custom-call(f32[256,256]{1,0:T(8,128)S(1)} %get-tuple-element.18.own_ref, bf16[256,256]{1,0:T(8,128)(2,1)} %collective-permute-done.got_ref, f32[256,128]{1,0:T(8,128)S(1)} %pad_maximum_fusion.2.table_ref, f32[1,128]{1,0:T(1,128)S(1)} %bitcast.6), custom_call_target="tpu_custom_call" | custom-call | flops 1000000 | bytes 524800 | tf_op jit(solution)/shard_map/pallas_call | solution.py:249
  11.1 0.0 copy-start.7
  11.1 0.6 copy-done.7
  11.8 3.3 %collective-permute-start.1 = (bf16[384,128]{1,0:T(8,128)(2,1)S(1)}, bf16[384,128]{1,0:T(8,128)(2,1)S(1)}, u32[]{:S(2)}, u32[]{:S(2)}) collective-permute-start(bf16[384,128]{1,0:T(8,128)(2,1)S(1)} %get-tuple-element.20), channel_id=1, source_target_pairs={{0,24},{2,26},{4,28},{6,30},{8,16},{10,18},{12,20},{14,22},{16,8},... | collective-permute-start | bytes 294920 | tf_op jit(solution)/shard_map/ppermute | solution.py:440
  15.1 0.0 collective-permute-start.2
  15.1 0.3 collective-permute-start.3
  15.4 0.2 collective-permute-start.4
  15.6 0.6 constant_dynamic-update-slice_fusion.5
  16.3 0.9 %collective-permute-done.1 = bf16[384,128]{1,0:T(8,128)(2,1)S(1)} collective-permute-done((bf16[384,128]{1,0:T(8,128)(2,1)S(1)}, bf16[384,128]{1,0:T(8,128)(2,1)S(1)}, u32[]{:S(2)}, u32[]{:S(2)}) %collective-permute-start.1) | collective-permute-done | bytes 98336 | tf_op jit(solution)/shard_map/ppermute | solution.py:440
  17.2 5.5 %collective-permute-done.2 = bf16[384,128]{1,0:T(8,128)(2,1)S(1)} collective-permute-done((bf16[384,128]{1,0:T(8,128)(2,1)S(1)}, bf16[384,128]{1,0:T(8,128)(2,1)S(1)}, u32[]{:S(2)}, u32[]{:S(2)}) %collective-permute-start.2) | collective-permute-done | bytes 98336 | tf_op jit(solution)/shard_map/ppermute | solution.py:440
  22.7 0.0 collective-permute-done.3
  22.7 0.3 collective-permute-start.5
  23.0 0.6 constant_dynamic-update-slice_fusion.4
  23.6 0.6 constant_dynamic-update-slice_fusion.3
  24.3 0.6 constant_dynamic-update-slice_fusion.2
  24.9 0.0 collective-permute-done.4
  24.9 0.6 constant_dynamic-update-slice_fusion.1
  25.6 4.0 %collective-permute-done.5 = bf16[1152,128]{1,0:T(8,128)(2,1)S(1)} collective-permute-done((bf16[1152,128]{1,0:T(8,128)(2,1)S(1)}, bf16[1152,128]{1,0:T(8,128)(2,1)S(1)}, u32[]{:S(2)}, u32[]{:S(2)}) %collective-permute-start.5) | collective-permute-done | bytes 294944 | tf_op jit(solution)/shard_map/ppermute | solution.py:440
  29.6 0.7 constant_dynamic-update-slice_fusion.refs_0_
  30.3 2.6 %collective-permute-start.6 = (bf16[3072,128]{1,0:T(8,128)(2,1)}, bf16[3072,128]{1,0:T(8,128)(2,1)}, u32[]{:S(2)}, u32[]{:S(2)}) collective-permute-start(bf16[3072,128]{1,0:T(8,128)(2,1)} %constant_dynamic-update-slice_fusion.refs_0_), channel_id=1, source_target_pairs={{0,2},{2,0},{4,6},{6,4},{8,10},{10,8},{12,14},{14,12},{16,18},{18,... | collective-permute-start | bytes 2359304 | tf_op jit(solution)/shard_map/ppermute | solution.py:440
  32.9 0.0 collective-permute-done.7.got_ref
  32.9 0.0 copy-done
  33.0 0.0 copy-done.8
  33.0 0.0 copy-start.1
  33.0 1.6 %copy-done.1 = bf16[2048,512]{1,0:T(8,128)(2,1)S(1)} copy-done((bf16[2048,512]{1,0:T(8,128)(2,1)S(1)}, bf16[2048,512]{1,0:T(8,128)(2,1)}, u32[]{:S(2)}) %copy-start.1) | copy-done | bytes 2097176
  34.6 1.2 %copy-done.2 = bf16[2048,256]{1,0:T(8,128)(2,1)S(1)} copy-done((bf16[2048,256]{1,0:T(8,128)(2,1)S(1)}, bf16[2048,256]{1,0:T(8,128)(2,1)}, u32[]{:S(2)}) %copy-start.2) | copy-done | bytes 1048600
  35.8 1.2 %copy-done.3 = bf16[2048,256]{1,0:T(8,128)(2,1)S(1)} copy-done((bf16[2048,256]{1,0:T(8,128)(2,1)S(1)}, bf16[2048,256]{1,0:T(8,128)(2,1)}, u32[]{:S(2)}) %copy-start.3) | copy-done | bytes 1048600
  37.0 0.9 %copy-done.6 = bf16[128,512]{1,0:T(8,128)(2,1)S(1)} copy-done((bf16[128,512]{1,0:T(8,128)(2,1)S(1)}, bf16[128,512]{1,0:T(8,128)(2,1)}, u32[]{:S(2)}) %copy-start.6) | copy-done | bytes 131096
  37.9 4.2 %shard_map.138 = (bf16[256,512]{1,0:T(8,128)(2,1)S(1)}, bf16[256,512]{1,0:T(8,128)(2,1)S(1)}, bf16[2,256,512]{2,1,0:T(8,128)(2,1)S(1)}, bf16[2,256,512]{2,1,0:T(8,128)(2,1)S(1)}) custom-call(s32[1]{0:T(128)} %bitcast.1.part_ref, bf16[256,1024]{1,0:T(8,128)(2,1)} %get-tuple-element.21.own_ref, bf16[256,1024]{1,0:T(8,128)(2,1)} %collective-permute-done.7.got_ref, ...), custom_call_target="tpu_custom_call" | custom-call | flops 1879048192 | bytes 8781824 | tf_op jit(solution)/shard_map/pallas_call | solution.py:249
  42.1 1.9 %collective-permute-start.8 = (bf16[128,512]{1,0:T(8,128)(2,1)S(1)}, bf16[128,512]{1,0:T(8,128)(2,1)S(1)}, u32[]{:S(2)}, u32[]{:S(2)}) collective-permute-start(bf16[128,512]{1,0:T(8,128)(2,1)S(1)} %get-tuple-element.32), channel_id=1, source_target_pairs={{0,2},{2,4},{4,6},{6,8},{8,10},{10,12},{12,14},{14,16},{16,18},{18... | collective-permute-start | bytes 393224 | tf_op jit(solution)/shard_map/ppermute | solution.py:515
  44.1 2.6 %collective-permute-start.9 = (bf16[128,512]{1,0:T(8,128)(2,1)S(1)}, bf16[128,512]{1,0:T(8,128)(2,1)S(1)}, u32[]{:S(2)}, u32[]{:S(2)}) collective-permute-start(bf16[128,512]{1,0:T(8,128)(2,1)S(1)} %get-tuple-element.31), channel_id=1, source_target_pairs={{2,0},{4,2},{6,4},{8,6},{10,8},{12,10},{14,12},{16,14},{18,16},{20... | collective-permute-start | bytes 393224 | tf_op jit(solution)/shard_map/ppermute | solution.py:516
  46.7 0.1 pad_add_fusion.place_ref
  46.7 0.0 copy-done.14
  46.8 0.0 collective-permute-done.8.refs_5_
  46.8 4.5 %collective-permute-done.9.refs_7_ = bf16[128,512]{1,0:T(8,128)(2,1)S(1)} collective-permute-done((bf16[128,512]{1,0:T(8,128)(2,1)S(1)}, bf16[128,512]{1,0:T(8,128)(2,1)S(1)}, u32[]{:S(2)}, u32[]{:S(2)}) %collective-permute-start.9) | collective-permute-done | bytes 131104 | tf_op jit(solution)/shard_map/ppermute | solution.py:516
  51.3 0.0 collective-permute-done.6.refs_1_
  51.3 0.0 copy-done.11
  51.3 0.0 copy-done.12
  51.3 0.0 copy-done.13
  51.3 6.7 %shard_map.140 = (bf16[128,1024]{1,0:T(8,128)(2,1)S(1)}, f32[128,1024]{1,0:T(8,128)S(1)}) custom-call(s32[3]{0:T(128)S(1)} %pad_add_fusion.place_ref, f32[2,8]{1,0:T(2,128)S(1)} %maximum_multiply_fusion.sink_ref, bf16[3072,128]{1,0:T(8,128)(2,1)} %constant_dynamic-update-slice_fusion.refs_0_, bf16[3072,128]{1,0:T(8,128)(2,1)} %collective-permute-done.6.refs_1_, ...), custom_call_target="tpu_custom_call" | custom-call | flops 3000000000 | bytes 8388608 | tf_op jit(solution)/shard_map/pallas_call | solution.py:526
  58.0 1.3 %collective-permute-start.11 = (bf16[128,1024]{1,0:T(8,128)(2,1)S(1)}, bf16[128,1024]{1,0:T(8,128)(2,1)S(1)}, u32[]{:S(2)}, u32[]{:S(2)}) collective-permute-start(bf16[128,1024]{1,0:T(8,128)(2,1)S(1)} %get-tuple-element.30), channel_id=1, source_target_pairs={{0,1},{1,0},{2,3},{3,2},{4,5},{5,4},{6,7},{7,6},{8,9},{9,8},{10,11... | collective-permute-start | bytes 786440 | tf_op jit(solution)/shard_map/ppermute | solution.py:440
  59.3 6.7 %shard_map.139 = (bf16[128,1024]{1,0:T(8,128)(2,1)S(1)}, f32[128,1024]{1,0:T(8,128)S(1)}) custom-call(s32[3]{0:T(128)S(1)} %pad_add_fusion.place_ref, f32[2,8]{1,0:T(2,128)S(1)} %maximum_multiply_fusion.sink_ref, bf16[3072,128]{1,0:T(8,128)(2,1)} %constant_dynamic-update-slice_fusion.refs_0_, bf16[3072,128]{1,0:T(8,128)(2,1)} %collective-permute-done.6.refs_1_, ...), custom_call_target="tpu_custom_call" | custom-call | flops 3000000000 | bytes 8388608 | tf_op jit(solution)/shard_map/pallas_call | solution.py:526
  66.0 0.3 collective-permute-start.10
  66.4 0.0 collective-permute-done.11
  66.4 0.1 add_convert_fusion
  66.4 7.4 %collective-permute-done.10 = bf16[128,1024]{1,0:T(8,128)(2,1)S(1)} collective-permute-done((bf16[128,1024]{1,0:T(8,128)(2,1)S(1)}, bf16[128,1024]{1,0:T(8,128)(2,1)S(1)}, u32[]{:S(2)}, u32[]{:S(2)}) %collective-permute-start.10) | collective-permute-done | bytes 262176 | tf_op jit(solution)/shard_map/ppermute | solution.py:440
  73.8 0.1 add_convert_fusion.1
  73.9 0.8 %pad_maximum_fusion = bf16[256,1024]{1,0:T(8,128)(2,1)} fusion(bf16[128,1024]{1,0:T(8,128)(2,1)S(1)} %add_convert_fusion, bf16[128,1024]{1,0:T(8,128)(2,1)S(1)} %add_convert_fusion.1), kind=kLoop, calls=%fused_computation | loop fusion | flops 1048576 | bytes 1048576 | tf_op jit(solution)/shard_map/concatenate | solution.py:542
  (14 shorter events, 0.1 us)
Async XLA Ops:
  0.0 9.8 %copy-start.10 = (f32[128]{0:T(128)S(1)}, f32[128]{0:T(128)}, u32[]{:S(2)}) copy-start(f32[128]{0:T(128)} %param.23) | copy-start | bytes 1540
  1.2 1.0 %copy-start.4 = (bf16[256,1024]{1,0:T(8,128)(2,1)S(1)}, bf16[256,1024]{1,0:T(8,128)(2,1)}, u32[]{:S(2)}) copy-start(bf16[256,1024]{1,0:T(8,128)(2,1)} %x_ref.1) | copy-start | bytes 1572868
  2.3 1.0 %copy-start.5 = (bf16[2048,128]{1,0:T(8,128)(2,1)S(1)}, bf16[2048,128]{1,0:T(8,128)(2,1)}, u32[]{:S(2)}) copy-start(bf16[2048,128]{1,0:T(8,128)(2,1)} %down_ref.1) | copy-start | bytes 1572868
  3.3 0.7 copy-start.9
  5.1 27.8 %copy-start = (bf16[2048,768]{1,0:T(8,128)(2,1)S(1)}, bf16[2048,768]{1,0:T(8,128)(2,1)}, u32[]{:S(2)}) copy-start(bf16[2048,768]{1,0:T(8,128)(2,1)} %wl_ref.1) | copy-start | bytes 9437188
  5.1 4.7 %collective-permute-start = (bf16[256,256]{1,0:T(8,128)(2,1)}, bf16[256,256]{1,0:T(8,128)(2,1)}, u32[]{:S(2)}, u32[]{:S(2)}) collective-permute-start(bf16[256,256]{1,0:T(8,128)(2,1)} %get-tuple-element.19), channel_id=1, source_target_pairs={{0,1},{1,0},{2,3},{3,2},{4,5},{5,4},{6,7},{7,6},{8,9},{9,8},{10,11... | collective-permute-start | bytes 393224 | tf_op jit(solution)/shard_map/ppermute | solution.py:440
  6.3 26.6 %collective-permute-start.7 = (bf16[256,1024]{1,0:T(8,128)(2,1)}, bf16[256,1024]{1,0:T(8,128)(2,1)}, u32[]{:S(2)}, u32[]{:S(2)}) collective-permute-start(bf16[256,1024]{1,0:T(8,128)(2,1)} %get-tuple-element.21.own_ref), channel_id=1, source_target_pairs={{0,1},{1,0},{2,3},{3,2},{4,5},{5,4},{6,7},{7,6},{8,9},{9,8},{10,11... | collective-permute-start | bytes 1572872 | tf_op jit(solution)/shard_map/ppermute | solution.py:440
  11.1 0.6 copy-start.7
  11.8 21.2 %copy-start.8 = (f32[256,128]{1,0:T(8,128)S(1)}, f32[256,128]{1,0:T(8,128)}, u32[]{:S(2)}) copy-start(f32[256,128]{1,0:T(8,128)} %copy-done.7) | copy-start | bytes 393220
  11.8 5.4 %collective-permute-start.1 = (bf16[384,128]{1,0:T(8,128)(2,1)S(1)}, bf16[384,128]{1,0:T(8,128)(2,1)S(1)}, u32[]{:S(2)}, u32[]{:S(2)}) collective-permute-start(bf16[384,128]{1,0:T(8,128)(2,1)S(1)} %get-tuple-element.20), channel_id=1, source_target_pairs={{0,24},{2,26},{4,28},{6,30},{8,16},{10,18},{12,20},{14,22},{16,8},... | collective-permute-start | bytes 294920 | tf_op jit(solution)/shard_map/ppermute | solution.py:440
  15.1 7.6 %collective-permute-start.2 = (bf16[384,128]{1,0:T(8,128)(2,1)S(1)}, bf16[384,128]{1,0:T(8,128)(2,1)S(1)}, u32[]{:S(2)}, u32[]{:S(2)}) collective-permute-start(bf16[384,128]{1,0:T(8,128)(2,1)S(1)} %get-tuple-element.20), channel_id=1, source_target_pairs={{0,16},{2,18},{4,20},{6,22},{8,24},{10,26},{12,28},{14,30},{16,0},... | collective-permute-start | bytes 294920 | tf_op jit(solution)/shard_map/ppermute | solution.py:440
  15.1 7.6 %collective-permute-start.3 = (bf16[384,128]{1,0:T(8,128)(2,1)S(1)}, bf16[384,128]{1,0:T(8,128)(2,1)S(1)}, u32[]{:S(2)}, u32[]{:S(2)}) collective-permute-start(bf16[384,128]{1,0:T(8,128)(2,1)S(1)} %get-tuple-element.20), channel_id=1, source_target_pairs={{0,8},{2,10},{4,12},{6,14},{8,0},{10,2},{12,4},{14,6},{16,24},{18,... | collective-permute-start | bytes 294920 | tf_op jit(solution)/shard_map/ppermute | solution.py:440
  15.4 9.5 %collective-permute-start.4 = (bf16[384,128]{1,0:T(8,128)(2,1)S(1)}, bf16[384,128]{1,0:T(8,128)(2,1)S(1)}, u32[]{:S(2)}, u32[]{:S(2)}) collective-permute-start(bf16[384,128]{1,0:T(8,128)(2,1)S(1)} %get-tuple-element.20), channel_id=1, source_target_pairs={{0,4},{2,6},{4,0},{6,2},{8,12},{10,14},{12,8},{14,10},{16,20},{18,... | collective-permute-start | bytes 294920 | tf_op jit(solution)/shard_map/ppermute | solution.py:440
  22.7 6.9 %collective-permute-start.5 = (bf16[1152,128]{1,0:T(8,128)(2,1)S(1)}, bf16[1152,128]{1,0:T(8,128)(2,1)S(1)}, u32[]{:S(2)}, u32[]{:S(2)}) collective-permute-start(bf16[1152,128]{1,0:T(8,128)(2,1)S(1)} %pad_maximum_fusion.1), channel_id=1, source_target_pairs={{0,4},{2,6},{4,0},{6,2},{8,12},{10,14},{12,8},{14,10},{16,20},{18,... | collective-permute-start | bytes 884744 | tf_op jit(solution)/shard_map/ppermute | solution.py:440
  30.3 20.9 %collective-permute-start.6 = (bf16[3072,128]{1,0:T(8,128)(2,1)}, bf16[3072,128]{1,0:T(8,128)(2,1)}, u32[]{:S(2)}, u32[]{:S(2)}) collective-permute-start(bf16[3072,128]{1,0:T(8,128)(2,1)} %constant_dynamic-update-slice_fusion.refs_0_), channel_id=1, source_target_pairs={{0,2},{2,0},{4,6},{6,4},{8,10},{10,8},{12,14},{14,12},{16,18},{18,... | collective-permute-start | bytes 2359304 | tf_op jit(solution)/shard_map/ppermute | solution.py:440
  33.0 1.6 %copy-start.1 = (bf16[2048,512]{1,0:T(8,128)(2,1)S(1)}, bf16[2048,512]{1,0:T(8,128)(2,1)}, u32[]{:S(2)}) copy-start(bf16[2048,512]{1,0:T(8,128)(2,1)} %wq_ref.1) | copy-start | bytes 6291460
  34.6 1.2 %copy-start.2 = (bf16[2048,256]{1,0:T(8,128)(2,1)S(1)}, bf16[2048,256]{1,0:T(8,128)(2,1)}, u32[]{:S(2)}) copy-start(bf16[2048,256]{1,0:T(8,128)(2,1)} %wk_ref.1) | copy-start | bytes 3145732
  35.8 1.2 %copy-start.3 = (bf16[2048,256]{1,0:T(8,128)(2,1)S(1)}, bf16[2048,256]{1,0:T(8,128)(2,1)}, u32[]{:S(2)}) copy-start(bf16[2048,256]{1,0:T(8,128)(2,1)} %wv_ref.1) | copy-start | bytes 3145732
  37.0 0.9 %copy-start.6 = (bf16[128,512]{1,0:T(8,128)(2,1)S(1)}, bf16[128,512]{1,0:T(8,128)(2,1)}, u32[]{:S(2)}) copy-start(bf16[128,512]{1,0:T(8,128)(2,1)} %up_ref.1) | copy-start | bytes 393220
  37.9 8.8 %copy-start.14 = (f32[8]{0:T(128)S(1)}, f32[8]{0:T(128)}, u32[]{:S(2)}) copy-start(f32[8]{0:T(128)} %param.19) | copy-start | bytes 100
  37.9 13.3 %copy-start.11 = (bf16[512,2048]{1,0:T(8,128)(2,1)S(1)}, bf16[512,2048]{1,0:T(8,128)(2,1)}, u32[]{:S(2)}) copy-start(bf16[512,2048]{1,0:T(8,128)(2,1)} %refs_9_.3) | copy-start | bytes 6291460
  37.9 13.3 %copy-start.12 = (bf16[512,2048]{1,0:T(8,128)(2,1)S(1)}, bf16[512,2048]{1,0:T(8,128)(2,1)}, u32[]{:S(2)}) copy-start(bf16[512,2048]{1,0:T(8,128)(2,1)} %refs_10_.3) | copy-start | bytes 6291460
  37.9 13.4 %copy-start.13 = (bf16[128,512]{1,0:T(8,128)(2,1)S(1)}, bf16[128,512]{1,0:T(8,128)(2,1)}, u32[]{:S(2)}) copy-start(bf16[128,512]{1,0:T(8,128)(2,1)} %refs_8_.3) | copy-start | bytes 393220
  42.1 4.6 %collective-permute-start.8 = (bf16[128,512]{1,0:T(8,128)(2,1)S(1)}, bf16[128,512]{1,0:T(8,128)(2,1)S(1)}, u32[]{:S(2)}, u32[]{:S(2)}) collective-permute-start(bf16[128,512]{1,0:T(8,128)(2,1)S(1)} %get-tuple-element.32), channel_id=1, source_target_pairs={{0,2},{2,4},{4,6},{6,8},{8,10},{10,12},{12,14},{14,16},{16,18},{18... | collective-permute-start | bytes 393224 | tf_op jit(solution)/shard_map/ppermute | solution.py:515
  44.1 7.2 %collective-permute-start.9 = (bf16[128,512]{1,0:T(8,128)(2,1)S(1)}, bf16[128,512]{1,0:T(8,128)(2,1)S(1)}, u32[]{:S(2)}, u32[]{:S(2)}) collective-permute-start(bf16[128,512]{1,0:T(8,128)(2,1)S(1)} %get-tuple-element.31), channel_id=1, source_target_pairs={{2,0},{4,2},{6,4},{8,6},{10,8},{12,10},{14,12},{16,14},{18,16},{20... | collective-permute-start | bytes 393224 | tf_op jit(solution)/shard_map/ppermute | solution.py:516
  58.0 8.3 %collective-permute-start.11 = (bf16[128,1024]{1,0:T(8,128)(2,1)S(1)}, bf16[128,1024]{1,0:T(8,128)(2,1)S(1)}, u32[]{:S(2)}, u32[]{:S(2)}) collective-permute-start(bf16[128,1024]{1,0:T(8,128)(2,1)S(1)} %get-tuple-element.30), channel_id=1, source_target_pairs={{0,1},{1,0},{2,3},{3,2},{4,5},{5,4},{6,7},{7,6},{8,9},{9,8},{10,11... | collective-permute-start | bytes 786440 | tf_op jit(solution)/shard_map/ppermute | solution.py:440
  66.0 7.8 %collective-permute-start.10 = (bf16[128,1024]{1,0:T(8,128)(2,1)S(1)}, bf16[128,1024]{1,0:T(8,128)(2,1)S(1)}, u32[]{:S(2)}, u32[]{:S(2)}) collective-permute-start(bf16[128,1024]{1,0:T(8,128)(2,1)S(1)} %get-tuple-element.28), channel_id=1, source_target_pairs={{0,1},{1,0},{2,3},{3,2},{4,5},{5,4},{6,7},{7,6},{8,9},{9,8},{10,11... | collective-permute-start | bytes 786440 | tf_op jit(solution)/shard_map/ppermute | solution.py:440

commit v2 on v1

--- a/solution.py
+++ b/solution.py
@@ -6,6 +6,7 @@
 from jax.experimental import pallas as pl
 from jax.experimental.pallas import tpu as pltpu
 from jax.sharding import PartitionSpec as P
+
 
 HEADS_A = 16
 DH = 64
@@ -243,33 +244,51 @@
     return [pl.BlockSpec(memory_space=pltpu.SMEM)] * count
 
 
-def call(body, shapes, smem, operands, flops, mib):
+def call(body, shapes, smem, hbm, operands, flops, mib, scratch=()):
     single = not isinstance(shapes, (list, tuple))
     outs = [shapes] if single else list(shapes)
     result = pl.pallas_call(
         body,
         out_shape=outs,
-        in_specs=scalars(len(smem)) + whole(len(operands)),
+        in_specs=scalars(len(smem))
+        + [pl.BlockSpec(memory_space=pltpu.HBM)] * len(hbm)
+        + whole(len(operands)),
         out_specs=whole(len(outs)),
+        scratch_shapes=list(scratch),
         cost_estimate=pl.CostEstimate(
             flops=int(flops),
-            bytes_accessed=sum(x.size * x.dtype.itemsize for x in operands),
+            bytes_accessed=sum(x.size * x.dtype.itemsize for x in [*hbm, *operands]),
             transcendentals=0,
         ),
         compiler_params=pltpu.CompilerParams(vmem_limit_bytes=mib * 2**20),
-    )(*smem, *operands)
+    )(*smem, *[pltpu.with_memory_space_constraint(x, pltpu.HBM) for x in hbm], *operands)
     return result[0] if single else result
 
 
-def compress_body(part_ref, x_ref, gain_ref, down_ref, rope_ref, norm_ref, own_ref, send_ref):
-    rows, half = x_ref.shape
+def compress_body(
+    part_ref, x_hbm, gain_hbm, down_hbm, rope_hbm, norm_ref, own_ref, send_ref,
+    x_ref, gain_ref, down_ref, rope_ref, sems,
+):
+    rows, half = x_hbm.shape
     start = pl.multiple_of(part_ref[0] * half, half)
+    copies = [
+        pltpu.make_async_copy(x_hbm, x_ref, sems.at[0]),
+        pltpu.make_async_copy(gain_hbm.at[:, pl.ds(start, half)], gain_ref, sems.at[3]),
+        pltpu.make_async_copy(down_hbm.at[pl.ds(start, half), :], down_ref, sems.at[1]),
+        pltpu.make_async_copy(rope_hbm.at[:, pl.ds(start, half)], rope_ref, sems.at[2]),
+    ]
+    for copy in copies:
+        copy.start()
+    copies[0].wait()
+    copies[1].wait()
     wide = x_ref[...].astype(F32)
-    normalized = (wide * gain_ref[:, pl.ds(start, half)]).astype(BF16)
+    normalized = (wide * gain_ref[...]).astype(BF16)
     norm_ref[...] = normalized
-    compressed = dot(normalized, down_ref[pl.ds(start, half), :])
-    rope = dot(normalized, rope_ref[pl.ds(start, half), :])
     squares = jnp.sum(wide * wide, axis=1, keepdims=True)
+    copies[2].wait()
+    compressed = dot(normalized, down_ref[...])
+    copies[3].wait()
+    rope = dot(normalized, rope_ref[...], ((1,), (1,)))
     high = squares.astype(BF16).astype(F32)
     lane = lax.broadcasted_iota(jnp.int32, (rows, LANES), 1)
     rope = jnp.concatenate([rope, jnp.zeros((rows, LANES - rope.shape[1]), F32)], axis=1)
@@ -304,28 +323,51 @@
     block_ref[rows:] = packed.astype(BF16)
 
 
-def project_body(
-    part_ref, own_ref, got_ref, scale_ref, table_ref, wq_ref, wk_ref, wv_ref, wl_ref, up_ref,
-    q_ref, kv_ref, qa_ref, qb_ref,
-):
-    rows, half = own_ref.shape
+def own_body(part_ref, *refs, count):
+    weights = refs[:count]
+    own_ref = refs[count]
+    sums = refs[count + 1 : 2 * count + 1]
+    rests = refs[2 * count + 1 : 3 * count + 1]
+    mines = refs[3 * count + 1 : 4 * count + 1]
+    sems = refs[-1]
+    half = own_ref.shape[1]
     part = part_ref[0]
     mine = pl.multiple_of(part * half, half)
     theirs = pl.multiple_of((1 - part) * half, half)
+    first = [
+        pltpu.make_async_copy(w.at[pl.ds(mine, half), :], m, sems.at[0, i])
+        for i, (w, m) in enumerate(zip(weights, mines))
+    ]
+    second = [
+        pltpu.make_async_copy(w.at[pl.ds(theirs, half), :], r, sems.at[1, i])
+        for i, (w, r) in enumerate(zip(weights, rests))
+    ]
+    for copy in first + second:
+        copy.start()
     own = own_ref[...]
+    for copy, mine_ref, sum_ref in zip(first, mines, sums):
+        copy.wait()
+        sum_ref[...] = dot(own, mine_ref[...])
+    for copy in second:
+        copy.wait()
+
+
+def project_body(
+    got_ref, scale_ref, table_ref, sk_ref, sv_ref, sq_ref, sl_ref, wk_ref, wv_ref, wq_ref, wl_ref,
+    up_ref, q_ref, kv_ref, qa_ref, qb_ref,
+):
     got = got_ref[...]
+    rows = got.shape[0]
     row_scale = scale_ref[:, :1]
 
-    def project(w_ref):
-        return (
-            dot(own, w_ref[pl.ds(mine, half), :]) + dot(got, w_ref[pl.ds(theirs, half), :])
-        ) * row_scale
+    def project(sum_ref, w_ref):
+        return (sum_ref[...] + dot(got, w_ref[...])) * row_scale
 
     width = wk_ref.shape[1]
-    kv_ref[:, :width] = project(wk_ref).astype(BF16)
-    kv_ref[:, width:] = project(wv_ref).astype(BF16)
-    q_ref[...] = (project(wq_ref) * (DH**-0.5 * LOG2E)).astype(BF16)
-    queries = project(wl_ref)
+    kv_ref[:, :width] = project(sk_ref, wk_ref).astype(BF16)
+    kv_ref[:, width:] = project(sv_ref, wv_ref).astype(BF16)
+    win = (project(sq_ref, wq_ref) * (DH**-0.5 * LOG2E)).astype(BF16)
+    queries = project(sl_ref, wl_ref)
     step = UNROTATED_WIDTH + D_ROPE
     scale = step**-0.5 * LOG2E
     row = lax.broadcasted_iota(jnp.int32, (LANES, LANES), 0)
@@ -334,6 +376,17 @@
     blank = jnp.zeros((rows, LANES - D_ROPE), F32)
     chunks = qa_ref.shape[0]
     span = rows // chunks
+    shared = LANES // DH
+    group = win.shape[1] // width
+    for g in range(width // DH):
+        pair = dot(unit, win[:, g * group * DH : (g + 1) * group * DH], ((1,), (1,))).astype(BF16)
+        spot = g % shared * DH
+        for c in range(chunks):
+            q_ref[c, g] = jnp.zeros(q_ref.shape[2:], BF16)
+            for j in range(group):
+                q_ref[c, g, spot : spot + DH, j * span : (j + 1) * span] = pair[
+                    j * DH : (j + 1) * DH, c * span : (c + 1) * span
+                ]
     lat = up_ref.shape[0]
     for head in range(wl_ref.shape[1] // step):
         plain = queries[:, head * step : head * step + UNROTATED_WIDTH].astype(BF16)
@@ -354,85 +407,116 @@
             qb_ref[c, lat:, cols] = second[:, rowsl]
 
 
-def attend_body(
-    place_ref, sink_ref, *refs, groups, chunk, rows,
+def attend_body(*refs, groups, chunk, rows):
+    qa_ref, qb_ref, mixed_ref = refs[-3:]
+    half = rows // 2
+    columns = qa_ref.shape[2]
+    steps = []
+    start = 0
+    for size in groups:
+        steps += [(refs[start : start + size], 0, qa_ref), (refs[start : start + size], 1, qb_ref)]
+        start += size
+
+    def keys_of(step):
+        blocks, part, _ = step
+        return jnp.concatenate([b[part * half : (part + 1) * half] for b in blocks], axis=0)
+
+    def score_of(step):
+        rope = jnp.concatenate([b[rows : rows + half] for b in step[0]], axis=0)
+        return dot(jnp.concatenate([keys_of(step), rope], axis=1), step[2][chunk])
+
+    peak = jnp.full((1, columns), MASKED, F32)
+    total = jnp.zeros((8, columns), F32)
+    weighted = jnp.zeros((LANES, columns), F32)
+    coming = score_of(steps[0])
+    for i, step in enumerate(steps):
+        score = coming
+        if i + 1 < len(steps):
+            coming = score_of(steps[i + 1])
+        top = jnp.maximum(peak, jnp.max(score, axis=0, keepdims=True))
+        factor = jnp.exp2(peak - top)
+        weight = jnp.exp2(score - top)
+        total = total * factor + jnp.sum(weight.reshape(-1, 8, columns), axis=0)
+        weighted = weighted * factor + dot(keys_of(step), weight.astype(BF16), ((0,), (0,)))
+        peak = top
+    mixed_ref[...] = (weighted / jnp.sum(total, axis=0, keepdims=True)).astype(BF16)
+
+
+def finish_body(
+    place_ref, sink_ref, mixed_ref, q_ref, prev_ref, kv_ref, next_ref, up_ref, ow_ref, ol_ref,
+    send_ref, keep_ref, cat_ref, *, chunk,
 ):
-    blocks = refs[:groups]
-    (
-        qa_ref, qb_ref, q_ref, prev_ref, kv_ref, next_ref, up_ref, ow_ref, ol_ref,
-        send_ref, keep_ref, _, cat_ref,
-    ) = refs[groups:]
-    span = q_ref.shape[0] // qa_ref.shape[0]
-    half = rows // 2
-    unit = rows + half
-    columns = qa_ref.shape[2]
-    lat = LANES
-    peak = jnp.full((1, columns), MASKED, F32)
-    total = jnp.zeros((1, columns), F32)
-    weighted = jnp.zeros((lat, columns), F32)
-    for block in blocks:
-        count = block.shape[0] // unit
-        cut = block[...].reshape(count, unit, LANES)
-        rope = cut[:, rows:].reshape(count * half, LANES)
-        first = cut[:, :half].reshape(count * half, LANES)
-        second = cut[:, half:rows].reshape(count * half, LANES)
-        for keys, table in ((first, qa_ref), (second, qb_ref)):
-            score = dot(jnp.concatenate([keys, rope], axis=1), table[chunk])
-            top = jnp.maximum(peak, jnp.max(score, axis=0, keepdims=True))
-            factor = jnp.exp2(peak - top)
-            weight = jnp.exp2(score - top)
-            total = total * factor + jnp.sum(weight, axis=0, keepdims=True)
-            weighted = weighted * factor + dot(keys, weight.astype(BF16), ((0,), (0,)))
-            peak = top
-    mixed = (weighted / total).astype(BF16)
-
+    span, columns = send_ref.shape[0], mixed_ref.shape[1]
+    mixed = mixed_ref[...]
     heads_l = columns // span
-    q = q_ref[chunk * span : (chunk + 1) * span, :]
-    heads = q.shape[1] // DH
-    width = kv_ref.shape[1] // 2
-    key_heads = width // DH
-    group = heads // key_heads
-    padded = jnp.concatenate([prev_ref[...], kv_ref[...], next_ref[...]], axis=0)
-    padded = padded[chunk * span : (chunk + 1) * span + 2 * WINDOW]
+    _, key_heads, lanes, width = q_ref.shape
+    group = width // span
+    shared = lanes // DH
+    own_rows = kv_ref.shape[0]
+    pieces = []
+    if chunk == 0:
+        pieces = [prev_ref[...]]
+    low_row = max(chunk * span - WINDOW, 0)
+    high_row = min((chunk + 1) * span + WINDOW, own_rows)
+    pieces.append(kv_ref[low_row:high_row])
+    if (chunk + 1) * span == own_rows:
+        pieces.append(next_ref[...])
+    padded = jnp.concatenate(pieces, axis=0)
     offset = place_ref[0]
     key_pos = lax.broadcasted_iota(jnp.int32, (span + 2 * WINDOW, span), 0) - WINDOW
     query_pos = lax.broadcasted_iota(jnp.int32, (span + 2 * WINDOW, span), 1)
     distance = jnp.abs(key_pos - query_pos)
     spot = key_pos + (offset + chunk * span)
     inside = (distance <= WINDOW) & (spot >= 0) & (spot < place_ref[1])
-    distance = distance.astype(F32)
+    distance = jnp.where(inside, distance.astype(F32), -MASKED)
+    distance = jnp.concatenate([distance] * group, axis=1)
+    values_at = kv_ref.shape[1] // 2
+
+    def spread(row, g):
+        return jnp.concatenate(
+            [jnp.full((1, span), sink_ref[row, g * group + j], F32) for j in range(group)], axis=1
+        )
+
+    def score_of(g):
+        at = g // shared * lanes
+        return dot(padded[:, at : at + lanes], q_ref[chunk, g])
+
+    coming = score_of(0)
     for g in range(key_heads):
-        keys = padded[:, g * DH : (g + 1) * DH]
-        values = padded[:, width + g * DH : width + (g + 1) * DH]
+        score = coming
+        if g + 1 < key_heads:
+            coming = score_of(g + 1)
+        at = values_at + g // shared * lanes
+        score = score - spread(1, g) * distance
+        sink = spread(0, g)
+        top = jnp.maximum(jnp.max(score, axis=0, keepdims=True), sink)
+        weight = jnp.exp2(score - top)
+        total = jnp.sum(weight, axis=0, keepdims=True) + jnp.exp2(sink - top)
+        out = dot(padded[:, at : at + lanes], weight.astype(BF16), ((0,), (0,)))
+        row = g % shared * DH
+        out = (out[row : row + DH] / total).astype(BF16)
         for j in range(group):
             head = g * group + j
-            score = dot(keys, q[:, head * DH : (head + 1) * DH], ((1,), (1,)))
-            score = jnp.where(inside, score - sink_ref[1, head] * distance, MASKED)
-            sink = sink_ref[0, head]
-            top = jnp.maximum(jnp.max(score, axis=0, keepdims=True), sink)
-            weight = jnp.exp2(score - top)
-            total = jnp.sum(weight, axis=0, keepdims=True) + jnp.exp2(sink - top)
-            out = dot(values, weight.astype(BF16), ((0,), (0,))) / total
-            cat_ref[head * DH : (head + 1) * DH, :] = out.astype(BF16)
-    base = heads * DH
+            cat_ref[head * DH : (head + 1) * DH, :] = out[:, j * span : (j + 1) * span]
+    base = key_heads * group * DH
     for head in range(heads_l):
         up = up_ref[:, head * VALUE_WIDTH : (head + 1) * VALUE_WIDTH]
         out = dot(up, mixed[:, head * span : (head + 1) * span], ((0,), (0,)))
         cat_ref[base + head * VALUE_WIDTH : base + (head + 1) * VALUE_WIDTH, :] = out.astype(BF16)
     keep = keep_ref.shape[1]
-    part = place_ref[2]
-    mine = pl.multiple_of(part * keep, keep)
-    theirs = pl.multiple_of((1 - part) * keep, keep)
     win = cat_ref[:base, :]
     low = cat_ref[base:, :]
 
     def out_of(start):
-        return dot(win, ow_ref[:, pl.ds(start, keep)], ((0,), (0,))) + dot(
-            low, ol_ref[:, pl.ds(start, keep)], ((0,), (0,))
+        return dot(win, ow_ref[:, start : start + keep], ((0,), (0,))) + dot(
+            low, ol_ref[:, start : start + keep], ((0,), (0,))
         )
 
-    send_ref[...] = out_of(theirs).astype(BF16)
-    keep_ref[...] = out_of(mine)
+    first = out_of(0)
+    second = out_of(keep)
+    lower = place_ref[2] == 0
+    send_ref[...] = jnp.where(lower, second, first).astype(BF16)
+    keep_ref[...] = jnp.where(lower, first, second)
 
 
 def swap(cells, axis, bit):
@@ -443,13 +527,10 @@
 def gather(block):
     count = lax.axis_size("sp")
     if count % 4 or count > 16 or count & (count - 1):
-        return (lax.all_gather(block, "sp", axis=0, tiled=True),)
-    line = [block] + [swap(block, "sp", 4 * k) for k in reversed(range(1, count // 4))]
-    near = swap(block, "sp", 2)
-    line = jnp.concatenate(line, axis=0)
-    far = swap(line[block.shape[0] :], "sp", 2) if count > 4 else line[:0]
-    mine = jnp.concatenate([line, near, far], axis=0)
-    return (mine, swap(mine, "sp", 1))
+        return [[block_of] for block_of in jnp.split(lax.all_gather(block, "sp", axis=0, tiled=True), count)]
+    line = [block] + [swap(block, "sp", 4 * k) for k in range(1, count // 4)]
+    mine = line + [swap(b, "sp", 2) for b in line]
+    return [mine, [swap(b, "sp", 1) for b in mine]]
 
 
 def per_device(
@@ -484,33 +565,51 @@
     normalized, own, send = call(
         compress_body,
         [shape((rows, half), BF16), shape((rows, lat + LANES), F32), shape((rows, lat + LANES), BF16)],
-        [part[None]],
-        [activations, norm_gain[None], key_value_down_weight, rope_key],
+        [part[None]], [activations, norm_gain[None], key_value_down_weight, rope_key.T], [],
         2 * rows * half * 192, 8,
+        [
+            pltpu.VMEM((rows, half), BF16),
+            pltpu.VMEM((1, half), F32),
+            pltpu.VMEM((half, lat), BF16),
+            pltpu.VMEM((rope_key.shape[1], half), BF16),
+            pltpu.SemaphoreType.DMA((4,)),
+        ],
     )
     got = swap(send, "tp", 1)
     other = swap(normalized, "tp", 1)
+    weights = [win_key, win_value, win_query, lat_query]
+    partial_sums = call(
+        partial(own_body, count=len(weights)),
+        [shape((rows, w.shape[1]), F32) for w in weights]
+        + [shape((half, w.shape[1]), BF16) for w in weights],
+        [part[None]], weights, [normalized],
+        2 * rows * half * 1792, 16,
+        [pltpu.VMEM((half, w.shape[1]), BF16) for w in weights]
+        + [pltpu.SemaphoreType.DMA((2, len(weights)))],
+    )
     block, row_scale = call(
         partial(latent_body, features=features),
         [shape((rows + rows // 2, lat), BF16), shape((rows, LANES), F32)],
-        [], [own, got, table, latent_norm_gain[None]],
+        [], [], [own, got, table, latent_norm_gain[None]],
         1e6, 4,
     )
-    blocks = gather(block)
+    groups = gather(block)
 
     chunks = rows // WINDOW
+    span = rows // chunks
+    group = win_query.shape[1] // win_key.shape[1]
     columns = lat_query.shape[1] // (UNROTATED_WIDTH + D_ROPE) * (rows // chunks)
     queries, key_value, table_a, table_b = call(
         project_body,
         [
-            shape(win_query.shape[1:] and (rows, win_query.shape[1]), BF16),
+            shape((chunks, win_key.shape[1] // DH, LANES, group * span), BF16),
             shape((rows, win_key.shape[1] + win_value.shape[1]), BF16),
             shape((chunks, lat + LANES, columns), BF16),
             shape((chunks, lat + LANES, columns), BF16),
         ],
-        [part[None]],
-        [normalized, other, row_scale, table, win_query, win_key, win_value, lat_query, key_up_weight],
-        2 * rows * features * 1792, 20,
+        [], [],
+        [other, row_scale, table, *partial_sums, key_up_weight],
+        2 * rows * half * 1792, 16,
     )
     after = lax.ppermute(key_value[rows - WINDOW :], "sp", [(i, i + 1) for i in range(count - 1)])
     before = lax.ppermute(key_value[:WINDOW], "sp", [(i + 1, i) for i in range(count - 1)])
@@ -521,29 +620,27 @@
     sinks = jnp.stack([sink_logit, slopes]) * LOG2E
     place = jnp.stack([offset, jnp.int32(rows * count), part])
     kept = []
+    flat = [b for group in groups for b in group]
     for c in range(chunks):
-        span = rows // chunks
-        send, keep = pl.pallas_call(
-            partial(attend_body, groups=len(blocks), chunk=c, rows=rows),
-            out_shape=[shape((span, half), BF16), shape((span, half), F32)],
-            in_specs=scalars(2) + whole(len(blocks) + 9),
-            out_specs=whole(2),
-            scratch_shapes=[
-                pltpu.VMEM((8, LANES), F32),
-                pltpu.VMEM((out_win.shape[0] + out_lat.shape[0], span), BF16),
-            ],
-            cost_estimate=pl.CostEstimate(flops=3 * 10**9, bytes_accessed=8 * 2**20, transcendentals=0),
-            compiler_params=pltpu.CompilerParams(vmem_limit_bytes=32 * 2**20),
-        )(
-            place, sinks, *blocks, table_a, table_b, queries, after, key_value, before,
-            value_up_weight, out_win, out_lat,
+        mixed = call(
+            partial(attend_body, groups=[len(g) for g in groups], chunk=c, rows=rows),
+            shape((lat, columns), BF16), [], [], [*flat, table_a, table_b], 3e9, 32,
+        )
+        send, keep = call(
+            partial(finish_body, chunk=c),
+            [shape((span, half), BF16), shape((span, half), F32)],
+            [place, sinks], [],
+            [mixed, queries, after, key_value, before, value_up_weight, out_win, out_lat],
+            1e9, 16,
+            [pltpu.VMEM((out_win.shape[0] + out_lat.shape[0], span), BF16)],
         )
         kept.append((keep, swap(send, "tp", 1)))
     return jnp.concatenate([(keep + got.astype(F32)).astype(BF16) for keep, got in kept], axis=0)
 
 
 def solution(mesh):
-    body = per_device if mesh.shape["tp"] == 2 else per_device_wide
+    narrow = mesh.shape["tp"] == 2
+    body = per_device if narrow else per_device_wide
     return jax.shard_map(
         body,
         mesh=mesh,

time: 75.2 us -> 55.3 us (0.74)
  local copies, waits for them, and re-layouts: 13.6 us -> 0.05 us
  waiting for transfers between devices: 24.8 us -> 12.8 us
  starting transfers between devices: 14.3 us -> 23.6 us
  Pallas kernels: 20.1 us -> 16.6 us
    unnamed x36 -> x12, local copies, waits for them, and re-layouts: 12.8 us -> 0.03 us
    ppermute x10 -> x19, waiting for transfers between devices: 20.4 us -> 10.4 us  [swap(): return lax.ppermute(cells, axis, [(i, i ^ bit) for i in range(count)])]
    ppermute x10 -> x19, starting transfers between devices: 9.76 us -> 18.8 us  [swap(): return lax.ppermute(cells, axis, [(i, i ^ bit) for i in range(count)])]
    pallas_call x5 -> x8, Pallas kernels: 20.1 us -> 16.6 us  [call(): pl.pallas_call(body, out_shape=outs, in_specs=scalars(len(smem)) + [pl.Bl...]
    ppermute x1, waiting for transfers between devices: 4.49 us -> 2.48 us  [per_device(): lax.ppermute(key_value[:WINDOW], 'sp', [(i + 1, i) for i in range(count -...]
    ppermute x1, starting transfers between devices: 1.92 us -> 2.77 us  [per_device(): lax.ppermute(key_value[rows - WINDOW:], 'sp', [(i, i + 1) for i in range(...]
  transfers between devices with their start and end apart: 12 -> 21, of which waited for: 6 -> 5; matrix products, arithmetic and copies ran while one was open for 7% -> 2% of each run, Pallas kernels for 16% -> 23%
where the time goes in v2:
time: 55.3 us; the launch traced here: 55.1 us
  starting transfers between devices  23.6 us (43%)
  Pallas kernels  16.6 us (30%)
  waiting for transfers between devices  12.8 us (23%)
  other arithmetic  1.77 us (3%)
    ppermute x19, starting transfers between devices, swap(): return lax.ppermute(cells, axis, [(i, i ^ bit) for i in range(count)])  18.8 us
    pallas_call x8, Pallas kernels, call(): pl.pallas_call(body, out_shape=outs, in_specs=scalars(len(smem)) + [pl.Bl...  16.6 us
    ppermute x19, waiting for transfers between devices, swap(): return lax.ppermute(cells, axis, [(i, i ^ bit) for i in range(count)])  10.4 us
    ppermute x1, starting transfers between devices, per_device(): lax.ppermute(key_value[rows - WINDOW:], 'sp', [(i, i + 1) for i in range(...  2.77 us
    ppermute x1, waiting for transfers between devices, per_device(): lax.ppermute(key_value[:WINDOW], 'sp', [(i + 1, i) for i in range(count -...  2.48 us
    ppermute x1, starting transfers between devices, per_device(): lax.ppermute(key_value[:WINDOW], 'sp', [(i + 1, i) for i in range(count -...  2.1 us
  transfers between devices with their start and end apart: 21, of which 5 were waited for; matrix products, arithmetic and copies ran while one was open for 2% of the time, Pallas kernels for 23%

profile of v2, /device:TPU:5, one launch (start us, length us, event | category | flops | bytes accessed | tf_op | source)
XLA Modules:
  0.0 55.1 jit_solution(8442599261722684143)
XLA Ops:
  0.0 2.2 %shard_map.136 = (bf16[256,1024]{1,0:T(8,128)(2,1)S(1)}, f32[256,256]{1,0:T(8,128)S(1)}, bf16[256,256]{1,0:T(8,128)(2,1)S(1)}) custom-call(s32[1]{0:T(128)} %bitcast.1.part_ref, bf16[256,1024]{1,0:T(8,128)(2,1)} %x_hbm.1, f32[1,2048]{1,0:T(1,128)} %bitcast.8, bf16[2048,128]{1,0:T(8,128)(2,1)} %down_hbm.1, bf16[64,2048]{1,0:T(8,128)(2,1)} %bitcast.7), custom_call_target="tpu_custom_call" | custom-call | flops 100663296 | bytes 1318912 | tf_op jit(solution)/shard_map/pallas_call | solution.py:250
  2.2 1.3 %collective-permute-start = (bf16[256,256]{1,0:T(8,128)(2,1)S(1)}, bf16[256,256]{1,0:T(8,128)(2,1)S(1)}, u32[]{:S(2)}, u32[]{:S(2)}) collective-permute-start(bf16[256,256]{1,0:T(8,128)(2,1)S(1)} %get-tuple-element.27), channel_id=1, source_target_pairs={{0,1},{1,0},{2,3},{3,2},{4,5},{5,4},{6,7},{7,6},{8,9},{9,8},{10,11... | collective-permute-start | bytes 393224 | tf_op jit(solution)/shard_map/ppermute | solution.py:524
  3.5 0.3 collective-permute-start.16
  3.7 0.5 multiply_cosine_fusion
  4.3 0.2 pad_maximum_fusion.1.table_ref
  4.5 2.2 %collective-permute-done.got_ref = bf16[256,256]{1,0:T(8,128)(2,1)S(1)} collective-permute-done((bf16[256,256]{1,0:T(8,128)(2,1)S(1)}, bf16[256,256]{1,0:T(8,128)(2,1)S(1)}, u32[]{:S(2)}, u32[]{:S(2)}) %collective-permute-start) | collective-permute-done | bytes 131104 | tf_op jit(solution)/shard_map/ppermute | solution.py:524
  6.6 0.0 copy-done.4
  6.6 0.4 shard_map.137
  7.0 1.4 %collective-permute-start.1 = (bf16[384,128]{1,0:T(8,128)(2,1)S(1)}, bf16[384,128]{1,0:T(8,128)(2,1)S(1)}, u32[]{:S(2)}, u32[]{:S(2)}) collective-permute-start(bf16[384,128]{1,0:T(8,128)(2,1)S(1)} %get-tuple-element.28.refs_0_), channel_id=1, source_target_pairs={{0,8},{2,10},{4,12},{6,14},{8,0},{10,2},{12,4},{14,6},{16,24},{18,... | collective-permute-start | bytes 294920 | tf_op jit(solution)/shard_map/ppermute | solution.py:524
  8.4 0.0 copy-done.5
  8.4 2.4 %collective-permute-start.2 = (bf16[384,128]{1,0:T(8,128)(2,1)S(1)}, bf16[384,128]{1,0:T(8,128)(2,1)S(1)}, u32[]{:S(2)}, u32[]{:S(2)}) collective-permute-start(bf16[384,128]{1,0:T(8,128)(2,1)S(1)} %get-tuple-element.28.refs_0_), channel_id=1, source_target_pairs={{0,16},{2,18},{4,20},{6,22},{8,24},{10,26},{12,28},{14,30},{16,0},... | collective-permute-start | bytes 294920 | tf_op jit(solution)/shard_map/ppermute | solution.py:524
  10.8 0.0 collective-permute-start.3
  10.8 0.2 collective-permute-start.4
  11.0 0.0 collective-permute-done.1.refs_1_
  11.0 3.5 %collective-permute-start.8 = (bf16[384,128]{1,0:T(8,128)(2,1)S(1)}, bf16[384,128]{1,0:T(8,128)(2,1)S(1)}, u32[]{:S(2)}, u32[]{:S(2)}) collective-permute-start(bf16[384,128]{1,0:T(8,128)(2,1)S(1)} %get-tuple-element.28.refs_0_), channel_id=1, source_target_pairs={{0,2},{2,0},{4,6},{6,4},{8,10},{10,8},{12,14},{14,12},{16,18},{18,... | collective-permute-start | bytes 294920 | tf_op jit(solution)/shard_map/ppermute | solution.py:524
  14.5 0.1 pad_add_fusion.place_ref
  14.6 0.0 collective-permute-done.2.refs_2_
  14.6 1.5 %collective-permute-start.6 = (bf16[384,128]{1,0:T(8,128)(2,1)S(1)}, bf16[384,128]{1,0:T(8,128)(2,1)S(1)}, u32[]{:S(2)}, u32[]{:S(2)}) collective-permute-start(bf16[384,128]{1,0:T(8,128)(2,1)S(1)} %collective-permute-done.2.refs_2_), channel_id=1, source_target_pairs={{0,4},{2,6},{4,0},{6,2},{8,12},{10,14},{12,8},{14,10},{16,20},{18,... | collective-permute-start | bytes 294920 | tf_op jit(solution)/shard_map/ppermute | solution.py:524
  16.1 1.1 %collective-permute-done.3.refs_3_ = bf16[384,128]{1,0:T(8,128)(2,1)S(1)} collective-permute-done((bf16[384,128]{1,0:T(8,128)(2,1)S(1)}, bf16[384,128]{1,0:T(8,128)(2,1)S(1)}, u32[]{:S(2)}, u32[]{:S(2)}) %collective-permute-start.3) | collective-permute-done | bytes 98336 | tf_op jit(solution)/shard_map/ppermute | solution.py:524
  17.2 3.3 %collective-permute-start.10 = (bf16[384,128]{1,0:T(8,128)(2,1)S(1)}, bf16[384,128]{1,0:T(8,128)(2,1)S(1)}, u32[]{:S(2)}, u32[]{:S(2)}) collective-permute-start(bf16[384,128]{1,0:T(8,128)(2,1)S(1)} %collective-permute-done.2.refs_2_), channel_id=1, source_target_pairs={{0,2},{2,0},{4,6},{6,4},{8,10},{10,8},{12,14},{14,12},{16,18},{18,... | collective-permute-start | bytes 294920 | tf_op jit(solution)/shard_map/ppermute | solution.py:524
  20.5 0.0 collective-permute-done.4.refs_4_
  20.5 0.2 collective-permute-start.7
  20.8 0.0 collective-permute-done.8.refs_8_
  20.8 0.3 collective-permute-start.11
  21.1 0.0 collective-permute-done.16.got_ref
  21.1 1.2 %collective-permute-start.5 = (bf16[384,128]{1,0:T(8,128)(2,1)S(1)}, bf16[384,128]{1,0:T(8,128)(2,1)S(1)}, u32[]{:S(2)}, u32[]{:S(2)}) collective-permute-start(bf16[384,128]{1,0:T(8,128)(2,1)S(1)} %collective-permute-done.1.refs_1_), channel_id=1, source_target_pairs={{0,4},{2,6},{4,0},{6,2},{8,12},{10,14},{12,8},{14,10},{16,20},{18,... | collective-permute-start | bytes 294920 | tf_op jit(solution)/shard_map/ppermute | solution.py:524
  22.3 3.2 %shard_map.138 = (f32[256,256]{1,0:T(8,128)S(1)}, f32[256,256]{1,0:T(8,128)S(1)}, f32[256,512]{1,0:T(8,128)S(1)}, f32[256,768]{1,0:T(8,128)S(1)}, bf16[1024,256]...) custom-call(s32[1]{0:T(128)} %bitcast.1.part_ref, ...), custom_call_target="tpu_custom_call" | custom-call | flops 939524096 | bytes 7864320 | tf_op jit(solution)/shard_map/pallas_call | solution.py:250
  25.5 0.0 copy-done.3
  25.5 1.9 %shard_map.139 = (bf16[2,4,128,256]{3,2,1,0:T(8,128)(2,1)S(1)}, bf16[256,512]{1,0:T(8,128)(2,1)S(1)}, bf16[2,256,512]{2,1,0:T(8,128)(2,1)S(1)}, bf16[2,256,512]{2,1,0:T(8,128)(2,1)S(1)}) custom-call(bf16[256,1024]{1,0:T(8,128)(2,1)S(1)} %collective-permute-done.16.got_ref, f32[256,128]{1,0:T(8,128)S(1)} %get-tuple-element.30.scale_ref, ...), custom_call_target="tpu_custom_call" | custom-call | flops 939524096 | bytes 6422528 | tf_op jit(solution)/shard_map/pallas_call | solution.py:250
  27.4 0.0 collective-permute-done.5.refs_5_
  27.4 0.6 %collective-permute-start.9 = (bf16[384,128]{1,0:T(8,128)(2,1)S(1)}, bf16[384,128]{1,0:T(8,128)(2,1)S(1)}, u32[]{:S(2)}, u32[]{:S(2)}) collective-permute-start(bf16[384,128]{1,0:T(8,128)(2,1)S(1)} %collective-permute-done.1.refs_1_), channel_id=1, source_target_pairs={{0,2},{2,0},{4,6},{6,4},{8,10},{10,8},{12,14},{14,12},{16,18},{18,... | collective-permute-start | bytes 294920 | tf_op jit(solution)/shard_map/ppermute | solution.py:524
  28.0 0.0 collective-permute-done.6.refs_6_
  28.0 0.1 collective-permute-start.12
  28.1 0.0 collective-permute-done.7.refs_7_
  28.1 0.4 collective-permute-start.13
  28.5 0.0 collective-permute-done.10.refs_10_
  28.5 0.1 collective-permute-start.14
  28.6 0.0 collective-permute-done.11.refs_11_
  28.6 0.4 collective-permute-start.15
  29.0 0.0 collective-permute-done.9.refs_9_
  29.0 2.8 %collective-permute-start.17 = (bf16[128,512]{1,0:T(8,128)(2,1)S(1)}, bf16[128,512]{1,0:T(8,128)(2,1)S(1)}, u32[]{:S(2)}, u32[]{:S(2)}) collective-permute-start(bf16[128,512]{1,0:T(8,128)(2,1)S(1)} %get-tuple-element.48), channel_id=1, source_target_pairs={{0,2},{2,4},{4,6},{6,8},{8,10},{10,12},{12,14},{14,16},{16,18},{18... | collective-permute-start | bytes 393224 | tf_op jit(solution)/shard_map/ppermute | solution.py:614
  31.8 0.0 collective-permute-done.12.refs_12_
  31.8 2.1 %collective-permute-start.18 = (bf16[128,512]{1,0:T(8,128)(2,1)S(1)}, bf16[128,512]{1,0:T(8,128)(2,1)S(1)}, u32[]{:S(2)}, u32[]{:S(2)}) collective-permute-start(bf16[128,512]{1,0:T(8,128)(2,1)S(1)} %get-tuple-element.47), channel_id=1, source_target_pairs={{2,0},{4,2},{6,4},{8,6},{10,8},{12,10},{14,12},{16,14},{18,16},{20... | collective-permute-start | bytes 393224 | tf_op jit(solution)/shard_map/ppermute | solution.py:615
  33.9 0.0 collective-permute-done.13.refs_13_
  34.0 0.0 collective-permute-done.14.refs_14_
  34.0 0.0 collective-permute-done.15.refs_15_
  34.0 0.0 copy-start
  34.0 0.0 copy-start.1
  34.0 0.0 copy-start.2
  34.0 2.5 %shard_map.140.mixed_ref = bf16[128,512]{1,0:T(8,128)(2,1)S(1)} custom-call(bf16[384,128]{1,0:T(8,128)(2,1)S(1)} %get-tuple-element.28.refs_0_, bf16[384,128]{1,0:T(8,128)(2,1)S(1)} %collective-permute-done.1.refs_1_, bf16[384,128]{1,0:T(8,128)(2,1)S(1)} %collective-permute-done.2.refs_2_, bf16[384,128]{1,0:T(8,128)(2,1)S(1)} %collective-permute-done.3.refs_3_, ...), custom_call_target="tpu_custom_call" | custom-call | flops 3000000000 | bytes 2621440 | tf_op jit(solution)/shard_map/pallas_call | solution.py:250
  36.5 0.0 collective-permute-done.17.prev_ref
  36.5 2.5 %collective-permute-done.18.next_ref = bf16[128,512]{1,0:T(8,128)(2,1)S(1)} collective-permute-done((bf16[128,512]{1,0:T(8,128)(2,1)S(1)}, bf16[128,512]{1,0:T(8,128)(2,1)S(1)}, u32[]{:S(2)}, u32[]{:S(2)}) %collective-permute-start.18) | collective-permute-done | bytes 131104 | tf_op jit(solution)/shard_map/ppermute | solution.py:615
  39.0 0.0 copy-done
  39.0 0.0 copy-done.1
  39.0 2.0 %shard_map.141 = (bf16[128,1024]{1,0:T(8,128)(2,1)S(1)}, f32[128,1024]{1,0:T(8,128)S(1)}) custom-call(s32[3]{0:T(128)S(1)} %pad_add_fusion.place_ref, f32[2,8]{1,0:T(2,128)S(1)} %maximum_multiply_fusion.sink_ref, bf16[128,512]{1,0:T(8,128)(2,1)S(1)} %shard_map.140.mixed_ref, bf16[2,4,128,256]{3,2,1,0:T(8,128)(2,1)S(1)} %get-tuple-element.41.q_ref, ...), custom_call_target="tpu_custom_call" | custom-call | flops 1000000000 | bytes 5505024 | tf_op jit(solution)/shard_map/pallas_call | solution.py:250
  41.0 1.3 %collective-permute-start.19 = (bf16[128,1024]{1,0:T(8,128)(2,1)S(1)}, bf16[128,1024]{1,0:T(8,128)(2,1)S(1)}, u32[]{:S(2)}, u32[]{:S(2)}) collective-permute-start(bf16[128,1024]{1,0:T(8,128)(2,1)S(1)} %get-tuple-element.44), channel_id=1, source_target_pairs={{0,1},{1,0},{2,3},{3,2},{4,5},{5,4},{6,7},{7,6},{8,9},{9,8},{10,11... | collective-permute-start | bytes 786440 | tf_op jit(solution)/shard_map/ppermute | solution.py:524
  42.3 2.5 %shard_map.142.mixed_ref = bf16[128,512]{1,0:T(8,128)(2,1)S(1)} custom-call(bf16[384,128]{1,0:T(8,128)(2,1)S(1)} %get-tuple-element.28.refs_0_, bf16[384,128]{1,0:T(8,128)(2,1)S(1)} %collective-permute-done.1.refs_1_, bf16[384,128]{1,0:T(8,128)(2,1)S(1)} %collective-permute-done.2.refs_2_, bf16[384,128]{1,0:T(8,128)(2,1)S(1)} %collective-permute-done.3.refs_3_, ...), custom_call_target="tpu_custom_call" | custom-call | flops 3000000000 | bytes 2621440 | tf_op jit(solution)/shard_map/pallas_call | solution.py:250
  44.8 2.0 %shard_map.143 = (bf16[128,1024]{1,0:T(8,128)(2,1)S(1)}, f32[128,1024]{1,0:T(8,128)S(1)}) custom-call(s32[3]{0:T(128)S(1)} %pad_add_fusion.place_ref, f32[2,8]{1,0:T(2,128)S(1)} %maximum_multiply_fusion.sink_ref, bf16[128,512]{1,0:T(8,128)(2,1)S(1)} %shard_map.142.mixed_ref, bf16[2,4,128,256]{3,2,1,0:T(8,128)(2,1)S(1)} %get-tuple-element.41.q_ref, ...), custom_call_target="tpu_custom_call" | custom-call | flops 1000000000 | bytes 5505024 | tf_op jit(solution)/shard_map/pallas_call | solution.py:250
  46.7 0.3 collective-permute-start.20
  47.1 1.1 %collective-permute-done.19 = bf16[128,1024]{1,0:T(8,128)(2,1)S(1)} collective-permute-done((bf16[128,1024]{1,0:T(8,128)(2,1)S(1)}, bf16[128,1024]{1,0:T(8,128)(2,1)S(1)}, u32[]{:S(2)}, u32[]{:S(2)}) %collective-permute-start.19) | collective-permute-done | bytes 262176 | tf_op jit(solution)/shard_map/ppermute | solution.py:524
  48.2 0.1 add_convert_fusion.1
  48.3 5.9 %collective-permute-done.20 = bf16[128,1024]{1,0:T(8,128)(2,1)S(1)} collective-permute-done((bf16[128,1024]{1,0:T(8,128)(2,1)S(1)}, bf16[128,1024]{1,0:T(8,128)(2,1)S(1)}, u32[]{:S(2)}, u32[]{:S(2)}) %collective-permute-start.20) | collective-permute-done | bytes 262176 | tf_op jit(solution)/shard_map/ppermute | solution.py:524
  54.2 0.1 add_convert_fusion
  54.3 0.8 %pad_maximum_fusion = bf16[256,1024]{1,0:T(8,128)(2,1)} fusion(bf16[128,1024]{1,0:T(8,128)(2,1)S(1)} %add_convert_fusion, bf16[128,1024]{1,0:T(8,128)(2,1)S(1)} %add_convert_fusion.1), kind=kLoop, calls=%fused_computation | loop fusion | flops 1048576 | bytes 1048576 | tf_op jit(solution)/shard_map/concatenate | solution.py:638
  (9 shorter events, 0.1 us)
Async XLA Ops:
  0.0 6.6 %copy-start.4 = (f32[128]{0:T(128)S(1)}, f32[128]{0:T(128)}, u32[]{:S(2)}) copy-start(f32[128]{0:T(128)} %param.23) | copy-start | bytes 1540
  0.0 8.4 %copy-start.5 = (f32[8]{0:T(128)S(1)}, f32[8]{0:T(128)}, u32[]{:S(2)}) copy-start(f32[8]{0:T(128)} %param.19) | copy-start | bytes 100
  2.2 4.4 %collective-permute-start = (bf16[256,256]{1,0:T(8,128)(2,1)S(1)}, bf16[256,256]{1,0:T(8,128)(2,1)S(1)}, u32[]{:S(2)}, u32[]{:S(2)}) collective-permute-start(bf16[256,256]{1,0:T(8,128)(2,1)S(1)} %get-tuple-element.27), channel_id=1, source_target_pairs={{0,1},{1,0},{2,3},{3,2},{4,5},{5,4},{6,7},{7,6},{8,9},{9,8},{10,11... | collective-permute-start | bytes 393224 | tf_op jit(solution)/shard_map/ppermute | solution.py:524
  3.5 17.6 %collective-permute-start.16 = (bf16[256,1024]{1,0:T(8,128)(2,1)S(1)}, bf16[256,1024]{1,0:T(8,128)(2,1)S(1)}, u32[]{:S(2)}, u32[]{:S(2)}) collective-permute-start(bf16[256,1024]{1,0:T(8,128)(2,1)S(1)} %get-tuple-element.29.refs_4_), channel_id=1, source_target_pairs={{0,1},{1,0},{2,3},{3,2},{4,5},{5,4},{6,7},{7,6},{8,9},{9,8},{10,11... | collective-permute-start | bytes 1572872 | tf_op jit(solution)/shard_map/ppermute | solution.py:524
  7.0 4.0 %collective-permute-start.1 = (bf16[384,128]{1,0:T(8,128)(2,1)S(1)}, bf16[384,128]{1,0:T(8,128)(2,1)S(1)}, u32[]{:S(2)}, u32[]{:S(2)}) collective-permute-start(bf16[384,128]{1,0:T(8,128)(2,1)S(1)} %get-tuple-element.28.refs_0_), channel_id=1, source_target_pairs={{0,8},{2,10},{4,12},{6,14},{8,0},{10,2},{12,4},{14,6},{16,24},{18,... | collective-permute-start | bytes 294920 | tf_op jit(solution)/shard_map/ppermute | solution.py:524
  8.4 6.2 %collective-permute-start.2 = (bf16[384,128]{1,0:T(8,128)(2,1)S(1)}, bf16[384,128]{1,0:T(8,128)(2,1)S(1)}, u32[]{:S(2)}, u32[]{:S(2)}) collective-permute-start(bf16[384,128]{1,0:T(8,128)(2,1)S(1)} %get-tuple-element.28.refs_0_), channel_id=1, source_target_pairs={{0,16},{2,18},{4,20},{6,22},{8,24},{10,26},{12,28},{14,30},{16,0},... | collective-permute-start | bytes 294920 | tf_op jit(solution)/shard_map/ppermute | solution.py:524
  10.8 6.4 %collective-permute-start.3 = (bf16[384,128]{1,0:T(8,128)(2,1)S(1)}, bf16[384,128]{1,0:T(8,128)(2,1)S(1)}, u32[]{:S(2)}, u32[]{:S(2)}) collective-permute-start(bf16[384,128]{1,0:T(8,128)(2,1)S(1)} %get-tuple-element.28.refs_0_), channel_id=1, source_target_pairs={{0,24},{2,26},{4,28},{6,30},{8,16},{10,18},{12,20},{14,22},{16,8},... | collective-permute-start | bytes 294920 | tf_op jit(solution)/shard_map/ppermute | solution.py:524
  10.8 9.7 %collective-permute-start.4 = (bf16[384,128]{1,0:T(8,128)(2,1)S(1)}, bf16[384,128]{1,0:T(8,128)(2,1)S(1)}, u32[]{:S(2)}, u32[]{:S(2)}) collective-permute-start(bf16[384,128]{1,0:T(8,128)(2,1)S(1)} %get-tuple-element.28.refs_0_), channel_id=1, source_target_pairs={{0,4},{2,6},{4,0},{6,2},{8,12},{10,14},{12,8},{14,10},{16,20},{18,... | collective-permute-start | bytes 294920 | tf_op jit(solution)/shard_map/ppermute | solution.py:524
  11.0 9.7 %collective-permute-start.8 = (bf16[384,128]{1,0:T(8,128)(2,1)S(1)}, bf16[384,128]{1,0:T(8,128)(2,1)S(1)}, u32[]{:S(2)}, u32[]{:S(2)}) collective-permute-start(bf16[384,128]{1,0:T(8,128)(2,1)S(1)} %get-tuple-element.28.refs_0_), channel_id=1, source_target_pairs={{0,2},{2,0},{4,6},{6,4},{8,10},{10,8},{12,14},{14,12},{16,18},{18,... | collective-permute-start | bytes 294920 | tf_op jit(solution)/shard_map/ppermute | solution.py:524
  14.6 10.9 %copy-start.3 = (bf16[128,512]{1,0:T(8,128)(2,1)S(1)}, bf16[128,512]{1,0:T(8,128)(2,1)}, u32[]{:S(2)}) copy-start(bf16[128,512]{1,0:T(8,128)(2,1)} %up_ref.3) | copy-start | bytes 393220
  14.6 13.4 %collective-permute-start.6 = (bf16[384,128]{1,0:T(8,128)(2,1)S(1)}, bf16[384,128]{1,0:T(8,128)(2,1)S(1)}, u32[]{:S(2)}, u32[]{:S(2)}) collective-permute-start(bf16[384,128]{1,0:T(8,128)(2,1)S(1)} %collective-permute-done.2.refs_2_), channel_id=1, source_target_pairs={{0,4},{2,6},{4,0},{6,2},{8,12},{10,14},{12,8},{14,10},{16,20},{18,... | collective-permute-start | bytes 294920 | tf_op jit(solution)/shard_map/ppermute | solution.py:524
  17.2 11.3 %collective-permute-start.10 = (bf16[384,128]{1,0:T(8,128)(2,1)S(1)}, bf16[384,128]{1,0:T(8,128)(2,1)S(1)}, u32[]{:S(2)}, u32[]{:S(2)}) collective-permute-start(bf16[384,128]{1,0:T(8,128)(2,1)S(1)} %collective-permute-done.2.refs_2_), channel_id=1, source_target_pairs={{0,2},{2,0},{4,6},{6,4},{8,10},{10,8},{12,14},{14,12},{16,18},{18,... | collective-permute-start | bytes 294920 | tf_op jit(solution)/shard_map/ppermute | solution.py:524
  20.5 7.5 %collective-permute-start.7 = (bf16[384,128]{1,0:T(8,128)(2,1)S(1)}, bf16[384,128]{1,0:T(8,128)(2,1)S(1)}, u32[]{:S(2)}, u32[]{:S(2)}) collective-permute-start(bf16[384,128]{1,0:T(8,128)(2,1)S(1)} %collective-permute-done.3.refs_3_), channel_id=1, source_target_pairs={{0,4},{2,6},{4,0},{6,2},{8,12},{10,14},{12,8},{14,10},{16,20},{18,... | collective-permute-start | bytes 294920 | tf_op jit(solution)/shard_map/ppermute | solution.py:524
  20.8 7.8 %collective-permute-start.11 = (bf16[384,128]{1,0:T(8,128)(2,1)S(1)}, bf16[384,128]{1,0:T(8,128)(2,1)S(1)}, u32[]{:S(2)}, u32[]{:S(2)}) collective-permute-start(bf16[384,128]{1,0:T(8,128)(2,1)S(1)} %collective-permute-done.3.refs_3_), channel_id=1, source_target_pairs={{0,2},{2,0},{4,6},{6,4},{8,10},{10,8},{12,14},{14,12},{16,18},{18,... | collective-permute-start | bytes 294920 | tf_op jit(solution)/shard_map/ppermute | solution.py:524
  21.1 6.3 %collective-permute-start.5 = (bf16[384,128]{1,0:T(8,128)(2,1)S(1)}, bf16[384,128]{1,0:T(8,128)(2,1)S(1)}, u32[]{:S(2)}, u32[]{:S(2)}) collective-permute-start(bf16[384,128]{1,0:T(8,128)(2,1)S(1)} %collective-permute-done.1.refs_1_), channel_id=1, source_target_pairs={{0,4},{2,6},{4,0},{6,2},{8,12},{10,14},{12,8},{14,10},{16,20},{18,... | collective-permute-start | bytes 294920 | tf_op jit(solution)/shard_map/ppermute | solution.py:524
  27.4 1.6 %collective-permute-start.9 = (bf16[384,128]{1,0:T(8,128)(2,1)S(1)}, bf16[384,128]{1,0:T(8,128)(2,1)S(1)}, u32[]{:S(2)}, u32[]{:S(2)}) collective-permute-start(bf16[384,128]{1,0:T(8,128)(2,1)S(1)} %collective-permute-done.1.refs_1_), channel_id=1, source_target_pairs={{0,2},{2,0},{4,6},{6,4},{8,10},{10,8},{12,14},{14,12},{16,18},{18,... | collective-permute-start | bytes 294920 | tf_op jit(solution)/shard_map/ppermute | solution.py:524
  28.0 3.9 %collective-permute-start.12 = (bf16[384,128]{1,0:T(8,128)(2,1)S(1)}, bf16[384,128]{1,0:T(8,128)(2,1)S(1)}, u32[]{:S(2)}, u32[]{:S(2)}) collective-permute-start(bf16[384,128]{1,0:T(8,128)(2,1)S(1)} %collective-permute-done.4.refs_4_), channel_id=1, source_target_pairs={{0,2},{2,0},{4,6},{6,4},{8,10},{10,8},{12,14},{14,12},{16,18},{18,... | collective-permute-start | bytes 294920 | tf_op jit(solution)/shard_map/ppermute | solution.py:524
  28.1 5.9 %collective-permute-start.13 = (bf16[384,128]{1,0:T(8,128)(2,1)S(1)}, bf16[384,128]{1,0:T(8,128)(2,1)S(1)}, u32[]{:S(2)}, u32[]{:S(2)}) collective-permute-start(bf16[384,128]{1,0:T(8,128)(2,1)S(1)} %collective-permute-done.5.refs_5_), channel_id=1, source_target_pairs={{0,2},{2,0},{4,6},{6,4},{8,10},{10,8},{12,14},{14,12},{16,18},{18,... | collective-permute-start | bytes 294920 | tf_op jit(solution)/shard_map/ppermute | solution.py:524
  28.5 5.5 %collective-permute-start.14 = (bf16[384,128]{1,0:T(8,128)(2,1)S(1)}, bf16[384,128]{1,0:T(8,128)(2,1)S(1)}, u32[]{:S(2)}, u32[]{:S(2)}) collective-permute-start(bf16[384,128]{1,0:T(8,128)(2,1)S(1)} %collective-permute-done.6.refs_6_), channel_id=1, source_target_pairs={{0,2},{2,0},{4,6},{6,4},{8,10},{10,8},{12,14},{14,12},{16,18},{18,... | collective-permute-start | bytes 294920 | tf_op jit(solution)/shard_map/ppermute | solution.py:524
  28.6 5.4 %collective-permute-start.15 = (bf16[384,128]{1,0:T(8,128)(2,1)S(1)}, bf16[384,128]{1,0:T(8,128)(2,1)S(1)}, u32[]{:S(2)}, u32[]{:S(2)}) collective-permute-start(bf16[384,128]{1,0:T(8,128)(2,1)S(1)} %collective-permute-done.7.refs_7_), channel_id=1, source_target_pairs={{0,2},{2,0},{4,6},{6,4},{8,10},{10,8},{12,14},{14,12},{16,18},{18,... | collective-permute-start | bytes 294920 | tf_op jit(solution)/shard_map/ppermute | solution.py:524
  29.0 7.5 %collective-permute-start.17 = (bf16[128,512]{1,0:T(8,128)(2,1)S(1)}, bf16[128,512]{1,0:T(8,128)(2,1)S(1)}, u32[]{:S(2)}, u32[]{:S(2)}) collective-permute-start(bf16[128,512]{1,0:T(8,128)(2,1)S(1)} %get-tuple-element.48), channel_id=1, source_target_pairs={{0,2},{2,4},{4,6},{6,8},{8,10},{10,12},{12,14},{14,16},{16,18},{18... | collective-permute-start | bytes 393224 | tf_op jit(solution)/shard_map/ppermute | solution.py:614
  31.8 7.2 %collective-permute-start.18 = (bf16[128,512]{1,0:T(8,128)(2,1)S(1)}, bf16[128,512]{1,0:T(8,128)(2,1)S(1)}, u32[]{:S(2)}, u32[]{:S(2)}) collective-permute-start(bf16[128,512]{1,0:T(8,128)(2,1)S(1)} %get-tuple-element.47), channel_id=1, source_target_pairs={{2,0},{4,2},{6,4},{8,6},{10,8},{12,10},{14,12},{16,14},{18,16},{20... | collective-permute-start | bytes 393224 | tf_op jit(solution)/shard_map/ppermute | solution.py:615
  34.0 5.0 %copy-start = (bf16[512,2048]{1,0:T(8,128)(2,1)S(1)}, bf16[512,2048]{1,0:T(8,128)(2,1)}, u32[]{:S(2)}) copy-start(bf16[512,2048]{1,0:T(8,128)(2,1)} %ow_ref.3) | copy-start | bytes 6291460
  34.0 5.0 %copy-start.1 = (bf16[512,2048]{1,0:T(8,128)(2,1)S(1)}, bf16[512,2048]{1,0:T(8,128)(2,1)}, u32[]{:S(2)}) copy-start(bf16[512,2048]{1,0:T(8,128)(2,1)} %ol_ref.3) | copy-start | bytes 6291460
  34.0 5.0 %copy-start.2 = (bf16[128,512]{1,0:T(8,128)(2,1)S(1)}, bf16[128,512]{1,0:T(8,128)(2,1)}, u32[]{:S(2)}) copy-start(bf16[128,512]{1,0:T(8,128)(2,1)} %up_ref.5) | copy-start | bytes 393220
  41.0 7.2 %collective-permute-start.19 = (bf16[128,1024]{1,0:T(8,128)(2,1)S(1)}, bf16[128,1024]{1,0:T(8,128)(2,1)S(1)}, u32[]{:S(2)}, u32[]{:S(2)}) collective-permute-start(bf16[128,1024]{1,0:T(8,128)(2,1)S(1)} %get-tuple-element.44), channel_id=1, source_target_pairs={{0,1},{1,0},{2,3},{3,2},{4,5},{5,4},{6,7},{7,6},{8,9},{9,8},{10,11... | collective-permute-start | bytes 786440 | tf_op jit(solution)/shard_map/ppermute | solution.py:524
  46.7 7.5 %collective-permute-start.20 = (bf16[128,1024]{1,0:T(8,128)(2,1)S(1)}, bf16[128,1024]{1,0:T(8,128)(2,1)S(1)}, u32[]{:S(2)}, u32[]{:S(2)}) collective-permute-start(bf16[128,1024]{1,0:T(8,128)(2,1)S(1)} %get-tuple-element.46), channel_id=1, source_target_pairs={{0,1},{1,0},{2,3},{3,2},{4,5},{5,4},{6,7},{7,6},{8,9},{9,8},{10,11... | collective-permute-start | bytes 786440 | tf_op jit(solution)/shard_map/ppermute | solution.py:524

commit v3 on v2

--- a/solution.py
+++ b/solution.py
@@ -266,10 +266,11 @@
 
 
 def compress_body(
-    part_ref, x_hbm, gain_hbm, down_hbm, rope_hbm, norm_ref, own_ref, send_ref,
+    offset_ref, part_ref, parity_ref, x_hbm, gain_hbm, down_hbm, rope_hbm, norm_ref, own_ref, send_ref,
     x_ref, gain_ref, down_ref, rope_ref, sems,
 ):
     rows, half = x_hbm.shape
+    del offset_ref, parity_ref
     start = pl.multiple_of(part_ref[0] * half, half)
     copies = [
         pltpu.make_async_copy(x_hbm, x_ref, sems.at[0]),
@@ -353,8 +354,8 @@
 
 
 def project_body(
-    got_ref, scale_ref, table_ref, sk_ref, sv_ref, sq_ref, sl_ref, wk_ref, wv_ref, wq_ref, wl_ref,
-    up_ref, q_ref, kv_ref, qa_ref, qb_ref,
+    parity_ref, got_ref, scale_ref, table_ref, sk_ref, sv_ref, sq_ref, sl_ref, wk_ref, wv_ref, wq_ref, wl_ref,
+    up_ref, q_ref, kv_ref, in_ref, out_ref, qa_ref, qb_ref,
 ):
     got = got_ref[...]
     rows = got.shape[0]
@@ -366,6 +367,11 @@
     width = wk_ref.shape[1]
     kv_ref[:, :width] = project(sk_ref, wk_ref).astype(BF16)
     kv_ref[:, width:] = project(sv_ref, wv_ref).astype(BF16)
+    even = parity_ref[0] == 0
+    head = kv_ref[:WINDOW]
+    tail = kv_ref[rows - WINDOW :]
+    in_ref[...] = jnp.where(even, tail, head)
+    out_ref[...] = jnp.where(even, head, tail)
     win = (project(sq_ref, wq_ref) * (DH**-0.5 * LOG2E)).astype(BF16)
     queries = project(sl_ref, wl_ref)
     step = UNROTATED_WIDTH + D_ROPE
@@ -443,8 +449,8 @@
 
 
 def finish_body(
-    place_ref, sink_ref, mixed_ref, q_ref, prev_ref, kv_ref, next_ref, up_ref, ow_ref, ol_ref,
-    send_ref, keep_ref, cat_ref, *, chunk,
+    offset_ref, part_ref, parity_ref, sink_ref, mixed_ref, q_ref, inner_ref, kv_ref, outer_ref, up_ref, ow_ref, ol_ref,
+    send_ref, keep_ref, cat_ref, *, chunk, seq_total,
 ):
     span, columns = send_ref.shape[0], mixed_ref.shape[1]
     mixed = mixed_ref[...]
@@ -453,29 +459,35 @@
     group = width // span
     shared = lanes // DH
     own_rows = kv_ref.shape[0]
+    even = parity_ref[0] == 0
     pieces = []
     if chunk == 0:
-        pieces = [prev_ref[...]]
+        pieces = [jnp.where(even, outer_ref[...], inner_ref[...])]
     low_row = max(chunk * span - WINDOW, 0)
     high_row = min((chunk + 1) * span + WINDOW, own_rows)
     pieces.append(kv_ref[low_row:high_row])
     if (chunk + 1) * span == own_rows:
-        pieces.append(next_ref[...])
+        pieces.append(jnp.where(even, inner_ref[...], outer_ref[...]))
     padded = jnp.concatenate(pieces, axis=0)
-    offset = place_ref[0]
+    offset = offset_ref[0]
     key_pos = lax.broadcasted_iota(jnp.int32, (span + 2 * WINDOW, span), 0) - WINDOW
     query_pos = lax.broadcasted_iota(jnp.int32, (span + 2 * WINDOW, span), 1)
     distance = jnp.abs(key_pos - query_pos)
     spot = key_pos + (offset + chunk * span)
-    inside = (distance <= WINDOW) & (spot >= 0) & (spot < place_ref[1])
+    inside = (distance <= WINDOW) & (spot >= 0) & (spot < seq_total)
     distance = jnp.where(inside, distance.astype(F32), -MASKED)
     distance = jnp.concatenate([distance] * group, axis=1)
     values_at = kv_ref.shape[1] // 2
 
-    def spread(row, g):
+    def sinks_of(g):
         return jnp.concatenate(
-            [jnp.full((1, span), sink_ref[row, g * group + j], F32) for j in range(group)], axis=1
+            [sink_ref[g * group + j : g * group + j + 1] for j in range(group)], axis=1
         )
+
+    def slopes_of(g):
+        first = part_ref[0] * (key_heads * group) + g * group + 1
+        heads = first + lax.broadcasted_iota(jnp.int32, (1, group * span), 1) // span
+        return jnp.exp2(heads.astype(F32) * (-8.0 / HEADS_A)) * LOG2E
 
     def score_of(g):
         at = g // shared * lanes
@@ -487,8 +499,8 @@
         if g + 1 < key_heads:
             coming = score_of(g + 1)
         at = values_at + g // shared * lanes
-        score = score - spread(1, g) * distance
-        sink = spread(0, g)
+        score = score - slopes_of(g) * distance
+        sink = sinks_of(g)
         top = jnp.maximum(jnp.max(score, axis=0, keepdims=True), sink)
         weight = jnp.exp2(score - top)
         total = jnp.sum(weight, axis=0, keepdims=True) + jnp.exp2(sink - top)
@@ -514,7 +526,7 @@
 
     first = out_of(0)
     second = out_of(keep)
-    lower = place_ref[2] == 0
+    lower = part_ref[0] == 0
     send_ref[...] = jnp.where(lower, second, first).astype(BF16)
     keep_ref[...] = jnp.where(lower, first, second)
 
@@ -556,6 +568,9 @@
     offset = lax.axis_index("sp").astype(jnp.int32) * rows
     shape = jax.ShapeDtypeStruct
 
+    heads = sink_logit.shape[0]
+    parity = lax.axis_index("sp").astype(jnp.int32) % 2
+
     places = (offset + jnp.arange(rows, dtype=jnp.int32)).astype(F32)
     angles = rotary_angles(places, D_ROPE)
     cosines, sines = jnp.cos(angles), jnp.sin(angles)
@@ -565,7 +580,7 @@
     normalized, own, send = call(
         compress_body,
         [shape((rows, half), BF16), shape((rows, lat + LANES), F32), shape((rows, lat + LANES), BF16)],
-        [part[None]], [activations, norm_gain[None], key_value_down_weight, rope_key.T], [],
+        [offset[None], part[None], parity[None]], [activations, norm_gain[None], key_value_down_weight, rope_key.T], [],
         2 * rows * half * 192, 8,
         [
             pltpu.VMEM((rows, half), BF16),
@@ -599,26 +614,26 @@
     span = rows // chunks
     group = win_query.shape[1] // win_key.shape[1]
     columns = lat_query.shape[1] // (UNROTATED_WIDTH + D_ROPE) * (rows // chunks)
-    queries, key_value, table_a, table_b = call(
+    queries, key_value, inward, outward, table_a, table_b = call(
         project_body,
         [
             shape((chunks, win_key.shape[1] // DH, LANES, group * span), BF16),
             shape((rows, win_key.shape[1] + win_value.shape[1]), BF16),
+            shape((WINDOW, win_key.shape[1] + win_value.shape[1]), BF16),
+            shape((WINDOW, win_key.shape[1] + win_value.shape[1]), BF16),
             shape((chunks, lat + LANES, columns), BF16),
             shape((chunks, lat + LANES, columns), BF16),
         ],
-        [], [],
+        [parity[None]], [],
         [other, row_scale, table, *partial_sums, key_up_weight],
         2 * rows * half * 1792, 16,
     )
-    after = lax.ppermute(key_value[rows - WINDOW :], "sp", [(i, i + 1) for i in range(count - 1)])
-    before = lax.ppermute(key_value[:WINDOW], "sp", [(i + 1, i) for i in range(count - 1)])
-
-    heads = sink_logit.shape[0]
-    head_ids = lax.axis_index("tp") * heads + jnp.arange(heads, dtype=jnp.int32)
-    slopes = jnp.exp2(-8.0 * (head_ids + 1).astype(F32) / HEADS_A)
-    sinks = jnp.stack([sink_logit, slopes]) * LOG2E
-    place = jnp.stack([offset, jnp.int32(rows * count), part])
+    inner = lax.ppermute(inward, "sp", [(i, i ^ 1) for i in range(count) if i ^ 1 < count])
+    outer = lax.ppermute(
+        outward, "sp", [(i, (i - 1 ^ 1) + 1) for i in range(1, count) if (i - 1 ^ 1) + 1 < count]
+    )
+
+    sinks = jnp.broadcast_to(sink_logit[:, None] * LOG2E, (heads, LANES))
     kept = []
     flat = [b for group in groups for b in group]
     for c in range(chunks):
@@ -627,10 +642,10 @@
             shape((lat, columns), BF16), [], [], [*flat, table_a, table_b], 3e9, 32,
         )
         send, keep = call(
-            partial(finish_body, chunk=c),
+            partial(finish_body, chunk=c, seq_total=rows * count),
             [shape((span, half), BF16), shape((span, half), F32)],
-            [place, sinks], [],
-            [mixed, queries, after, key_value, before, value_up_weight, out_win, out_lat],
+            [offset[None], part[None], parity[None]], [],
+            [sinks, mixed, queries, inner, key_value, outer, value_up_weight, out_win, out_lat],
             1e9, 16,
             [pltpu.VMEM((out_win.shape[0] + out_lat.shape[0], span), BF16)],
         )

time: 55.3 us -> 57.3 us (1.036)
  the two profiles are of different devices: /device:TPU:5 before, /device:TPU:25 now
where the time goes in v3:
time: 57.3 us; the launch traced here: 57.1 us
  starting transfers between devices  26.8 us (47%)
  Pallas kernels  15.6 us (27%)
  waiting for transfers between devices  12.7 us (22%)
  other arithmetic  1.68 us (3%)
    ppermute x19, starting transfers between devices, swap(): return lax.ppermute(cells, axis, [(i, i ^ bit) for i in range(count)])  23.5 us
    pallas_call x8, Pallas kernels, call(): pl.pallas_call(body, out_shape=outs, in_specs=scalars(len(smem)) + [pl.Bl...  15.6 us
    ppermute x19, waiting for transfers between devices, swap(): return lax.ppermute(cells, axis, [(i, i ^ bit) for i in range(count)])  10.5 us
    ppermute x1, starting transfers between devices, per_device(): lax.ppermute(outward, 'sp', [(i, (i - 1 ^ 1) + 1) for i in range(1, count...  2.8 us
    ppermute x1, waiting for transfers between devices, per_device(): lax.ppermute(outward, 'sp', [(i, (i - 1 ^ 1) + 1) for i in range(1, count...  2.26 us
  transfers between devices with their start and end apart: 21, of which 4 were waited for; matrix products, arithmetic and copies ran while one was open for 1% of the time, Pallas kernels for 21%

profile of v3, /device:TPU:25, one launch (start us, length us, event | category | flops | bytes accessed | tf_op | source)
XLA Modules:
  0.0 57.1 jit_solution(3742583813550463980)
XLA Ops:
  0.0 2.2 %shard_map.136 = (bf16[256,1024]{1,0:T(8,128)(2,1)S(1)}, f32[256,256]{1,0:T(8,128)S(1)}, bf16[256,256]{1,0:T(8,128)(2,1)S(1)}) custom-call(s32[1]{0:T(128)} %bitcast.offset_ref, s32[1]{0:T(128)} %bitcast.1.part_ref, s32[1]{0:T(128)} %bitcast.2.parity_ref, bf16[256,1024]{1,0:T(8,128)(2,1)} %x_hbm.1, f32[1,2048]{1,0:T(1,128)} %bitcast.8, ...), custom_call_target="tpu_custom_call" | custom-call | flops 100663296 | bytes 1318912 | tf_op jit(solution)/shard_map/pallas_call | solution.py:250
  2.2 1.3 %collective-permute-start = (bf16[256,256]{1,0:T(8,128)(2,1)S(1)}, bf16[256,256]{1,0:T(8,128)(2,1)S(1)}, u32[]{:S(2)}, u32[]{:S(2)}) collective-permute-start(bf16[256,256]{1,0:T(8,128)(2,1)S(1)} %get-tuple-element.29), channel_id=1, source_target_pairs={{0,1},{1,0},{2,3},{3,2},{4,5},{5,4},{6,7},{7,6},{8,9},{9,8},{10,11... | collective-permute-start | bytes 393224 | tf_op jit(solution)/shard_map/ppermute | solution.py:536
  3.5 0.3 collective-permute-start.16
  3.7 0.5 multiply_cosine_fusion
  4.3 0.2 pad_maximum_fusion.1.table_ref
  4.5 2.2 %collective-permute-done.got_ref = bf16[256,256]{1,0:T(8,128)(2,1)S(1)} collective-permute-done((bf16[256,256]{1,0:T(8,128)(2,1)S(1)}, bf16[256,256]{1,0:T(8,128)(2,1)S(1)}, u32[]{:S(2)}, u32[]{:S(2)}) %collective-permute-start) | collective-permute-done | bytes 131104 | tf_op jit(solution)/shard_map/ppermute | solution.py:536
  6.6 0.0 copy-done.4
  6.6 0.4 shard_map.137
  7.0 0.2 collective-permute-start.1
  7.3 0.1 collective-permute-start.2
  7.4 3.3 %collective-permute-start.3 = (bf16[384,128]{1,0:T(8,128)(2,1)S(1)}, bf16[384,128]{1,0:T(8,128)(2,1)S(1)}, u32[]{:S(2)}, u32[]{:S(2)}) collective-permute-start(bf16[384,128]{1,0:T(8,128)(2,1)S(1)} %get-tuple-element.30.refs_0_), channel_id=1, source_target_pairs={{0,24},{2,26},{4,28},{6,30},{8,16},{10,18},{12,20},{14,22},{16,8},... | collective-permute-start | bytes 294920 | tf_op jit(solution)/shard_map/ppermute | solution.py:536
  10.6 1.2 %collective-permute-start.4 = (bf16[384,128]{1,0:T(8,128)(2,1)S(1)}, bf16[384,128]{1,0:T(8,128)(2,1)S(1)}, u32[]{:S(2)}, u32[]{:S(2)}) collective-permute-start(bf16[384,128]{1,0:T(8,128)(2,1)S(1)} %get-tuple-element.30.refs_0_), channel_id=1, source_target_pairs={{0,4},{2,6},{4,0},{6,2},{8,12},{10,14},{12,8},{14,10},{16,20},{18,... | collective-permute-start | bytes 294920 | tf_op jit(solution)/shard_map/ppermute | solution.py:536
  11.9 0.0 collective-permute-done.1.refs_1_
  11.9 3.8 %collective-permute-start.8 = (bf16[384,128]{1,0:T(8,128)(2,1)S(1)}, bf16[384,128]{1,0:T(8,128)(2,1)S(1)}, u32[]{:S(2)}, u32[]{:S(2)}) collective-permute-start(bf16[384,128]{1,0:T(8,128)(2,1)S(1)} %get-tuple-element.30.refs_0_), channel_id=1, source_target_pairs={{0,2},{2,0},{4,6},{6,4},{8,10},{10,8},{12,14},{14,12},{16,18},{18,... | collective-permute-start | bytes 294920 | tf_op jit(solution)/shard_map/ppermute | solution.py:536
  15.7 0.0 collective-permute-done.2.refs_2_
  15.7 1.3 %collective-permute-start.5 = (bf16[384,128]{1,0:T(8,128)(2,1)S(1)}, bf16[384,128]{1,0:T(8,128)(2,1)S(1)}, u32[]{:S(2)}, u32[]{:S(2)}) collective-permute-start(bf16[384,128]{1,0:T(8,128)(2,1)S(1)} %collective-permute-done.1.refs_1_), channel_id=1, source_target_pairs={{0,4},{2,6},{4,0},{6,2},{8,12},{10,14},{12,8},{14,10},{16,20},{18,... | collective-permute-start | bytes 294920 | tf_op jit(solution)/shard_map/ppermute | solution.py:536
  16.9 0.0 collective-permute-done.3.refs_3_
  16.9 0.2 collective-permute-start.6
  17.2 0.0 collective-permute-done.4.refs_4_
  17.2 3.5 %collective-permute-start.10 = (bf16[384,128]{1,0:T(8,128)(2,1)S(1)}, bf16[384,128]{1,0:T(8,128)(2,1)S(1)}, u32[]{:S(2)}, u32[]{:S(2)}) collective-permute-start(bf16[384,128]{1,0:T(8,128)(2,1)S(1)} %collective-permute-done.2.refs_2_), channel_id=1, source_target_pairs={{0,2},{2,0},{4,6},{6,4},{8,10},{10,8},{12,14},{14,12},{16,18},{18,... | collective-permute-start | bytes 294920 | tf_op jit(solution)/shard_map/ppermute | solution.py:536
  20.7 0.0 collective-permute-done.8.refs_8_
  20.7 1.2 %collective-permute-start.7 = (bf16[384,128]{1,0:T(8,128)(2,1)S(1)}, bf16[384,128]{1,0:T(8,128)(2,1)S(1)}, u32[]{:S(2)}, u32[]{:S(2)}) collective-permute-start(bf16[384,128]{1,0:T(8,128)(2,1)S(1)} %collective-permute-done.3.refs_3_), channel_id=1, source_target_pairs={{0,4},{2,6},{4,0},{6,2},{8,12},{10,14},{12,8},{14,10},{16,20},{18,... | collective-permute-start | bytes 294920 | tf_op jit(solution)/shard_map/ppermute | solution.py:536
  21.9 0.0 collective-permute-done.5.refs_5_
  21.9 1.3 %collective-permute-start.11 = (bf16[384,128]{1,0:T(8,128)(2,1)S(1)}, bf16[384,128]{1,0:T(8,128)(2,1)S(1)}, u32[]{:S(2)}, u32[]{:S(2)}) collective-permute-start(bf16[384,128]{1,0:T(8,128)(2,1)S(1)} %collective-permute-done.3.refs_3_), channel_id=1, source_target_pairs={{0,2},{2,0},{4,6},{6,4},{8,10},{10,8},{12,14},{14,12},{16,18},{18,... | collective-permute-start | bytes 294920 | tf_op jit(solution)/shard_map/ppermute | solution.py:536
  23.3 0.0 copy-done.5
  23.3 0.0 collective-permute-done.6.refs_6_
  23.3 2.5 %collective-permute-start.9 = (bf16[384,128]{1,0:T(8,128)(2,1)S(1)}, bf16[384,128]{1,0:T(8,128)(2,1)S(1)}, u32[]{:S(2)}, u32[]{:S(2)}) collective-permute-start(bf16[384,128]{1,0:T(8,128)(2,1)S(1)} %collective-permute-done.1.refs_1_), channel_id=1, source_target_pairs={{0,2},{2,0},{4,6},{6,4},{8,10},{10,8},{12,14},{14,12},{16,18},{18,... | collective-permute-start | bytes 294920 | tf_op jit(solution)/shard_map/ppermute | solution.py:536
  25.8 0.0 collective-permute-done.7.refs_7_
  25.8 1.1 %collective-permute-start.12 = (bf16[384,128]{1,0:T(8,128)(2,1)S(1)}, bf16[384,128]{1,0:T(8,128)(2,1)S(1)}, u32[]{:S(2)}, u32[]{:S(2)}) collective-permute-start(bf16[384,128]{1,0:T(8,128)(2,1)S(1)} %collective-permute-done.4.refs_4_), channel_id=1, source_target_pairs={{0,2},{2,0},{4,6},{6,4},{8,10},{10,8},{12,14},{14,12},{16,18},{18,... | collective-permute-start | bytes 294920 | tf_op jit(solution)/shard_map/ppermute | solution.py:536
  26.9 0.0 collective-permute-done.10.refs_10_
  26.9 0.0 collective-permute-start.13
  26.9 0.0 collective-permute-done.11.refs_11_
  26.9 0.5 collective-permute-start.14
  27.4 0.0 collective-permute-done.16.got_ref
  27.4 0.1 collective-permute-start.15
  27.5 3.2 %shard_map.138 = (f32[256,256]{1,0:T(8,128)S(1)}, f32[256,256]{1,0:T(8,128)S(1)}, f32[256,512]{1,0:T(8,128)S(1)}, f32[256,768]{1,0:T(8,128)S(1)}, bf16[1024,256]...) custom-call(s32[1]{0:T(128)} %bitcast.1.part_ref, ...), custom_call_target="tpu_custom_call" | custom-call | flops 939524096 | bytes 7864320 | tf_op jit(solution)/shard_map/pallas_call | solution.py:250
  30.7 0.0 copy-done.3
  30.7 1.9 %shard_map.139 = (bf16[2,4,128,256]{3,2,1,0:T(8,128)(2,1)S(1)}, bf16[256,512]{1,0:T(8,128)(2,1)S(1)}, bf16[128,512]{1,0:T(8,128)(2,1)S(1)}, bf16[128,512]{1,0:T(...) custom-call(s32[1]{0:T(128)} %bitcast.2.parity_ref, ...), custom_call_target="tpu_custom_call" | custom-call | flops 939524096 | bytes 6422528 | tf_op jit(solution)/shard_map/pallas_call | solution.py:250
  32.6 0.0 collective-permute-done.12.refs_12_
  32.6 0.5 collective-permute-start.17
  33.1 0.0 collective-permute-done.9.refs_9_
  33.1 2.8 %collective-permute-start.18 = (bf16[128,512]{1,0:T(8,128)(2,1)S(1)}, bf16[128,512]{1,0:T(8,128)(2,1)S(1)}, u32[]{:S(2)}, u32[]{:S(2)}) collective-permute-start(bf16[128,512]{1,0:T(8,128)(2,1)S(1)} %get-tuple-element.46), channel_id=1, source_target_pairs={{2,4},{4,2},{6,8},{8,6},{10,12},{12,10},{14,16},{16,14},{18,20},{2... | collective-permute-start | bytes 393224 | tf_op jit(solution)/shard_map/ppermute | solution.py:632
  35.9 0.0 collective-permute-done.13.refs_13_
  36.0 0.0 collective-permute-done.14.refs_14_
  36.0 0.0 collective-permute-done.15.refs_15_
  36.0 0.0 copy-start
  36.0 0.0 copy-start.1
  36.0 0.0 copy-start.2
  36.0 2.5 %shard_map.140.mixed_ref = bf16[128,512]{1,0:T(8,128)(2,1)S(1)} custom-call(bf16[384,128]{1,0:T(8,128)(2,1)S(1)} %get-tuple-element.30.refs_0_, bf16[384,128]{1,0:T(8,128)(2,1)S(1)} %collective-permute-done.1.refs_1_, bf16[384,128]{1,0:T(8,128)(2,1)S(1)} %collective-permute-done.2.refs_2_, bf16[384,128]{1,0:T(8,128)(2,1)S(1)} %collective-permute-done.3.refs_3_, ...), custom_call_target="tpu_custom_call" | custom-call | flops 3000000000 | bytes 2621440 | tf_op jit(solution)/shard_map/pallas_call | solution.py:250
  38.5 0.0 collective-permute-done.17.inner_ref
  38.5 2.3 %collective-permute-done.18.outer_ref = bf16[128,512]{1,0:T(8,128)(2,1)S(1)} collective-permute-done((bf16[128,512]{1,0:T(8,128)(2,1)S(1)}, bf16[128,512]{1,0:T(8,128)(2,1)S(1)}, u32[]{:S(2)}, u32[]{:S(2)}) %collective-permute-start.18) | collective-permute-done | bytes 131104 | tf_op jit(solution)/shard_map/ppermute | solution.py:632
  40.8 0.1 broadcast_in_dim.15.sink_ref
  40.9 0.0 copy-done
  40.9 0.0 copy-done.1
  40.9 1.4 %shard_map.141 = (bf16[128,1024]{1,0:T(8,128)(2,1)S(1)}, f32[128,1024]{1,0:T(8,128)S(1)}) custom-call(s32[1]{0:T(128)} %bitcast.offset_ref, s32[1]{0:T(128)} %bitcast.1.part_ref, s32[1]{0:T(128)} %bitcast.2.parity_ref, f32[8,128]{1,0:T(8,128)S(1)} %broadcast_in_dim.15.sink_ref, bf16[128,512]{1,0:T(8,128)(2,1)S(1)} %shard_map.140.mixed_ref, ...), custom_call_target="tpu_custom_call" | custom-call | flops 1000000000 | bytes 5509120 | tf_op jit(solution)/shard_map/pallas_call | solution.py:250
  42.3 1.3 %collective-permute-start.19 = (bf16[128,1024]{1,0:T(8,128)(2,1)S(1)}, bf16[128,1024]{1,0:T(8,128)(2,1)S(1)}, u32[]{:S(2)}, u32[]{:S(2)}) collective-permute-start(bf16[128,1024]{1,0:T(8,128)(2,1)S(1)} %get-tuple-element.48), channel_id=1, source_target_pairs={{0,1},{1,0},{2,3},{3,2},{4,5},{5,4},{6,7},{7,6},{8,9},{9,8},{10,11... | collective-permute-start | bytes 786440 | tf_op jit(solution)/shard_map/ppermute | solution.py:536
  43.6 2.5 %shard_map.142.mixed_ref = bf16[128,512]{1,0:T(8,128)(2,1)S(1)} custom-call(bf16[384,128]{1,0:T(8,128)(2,1)S(1)} %get-tuple-element.30.refs_0_, bf16[384,128]{1,0:T(8,128)(2,1)S(1)} %collective-permute-done.1.refs_1_, bf16[384,128]{1,0:T(8,128)(2,1)S(1)} %collective-permute-done.2.refs_2_, bf16[384,128]{1,0:T(8,128)(2,1)S(1)} %collective-permute-done.3.refs_3_, ...), custom_call_target="tpu_custom_call" | custom-call | flops 3000000000 | bytes 2621440 | tf_op jit(solution)/shard_map/pallas_call | solution.py:250
  46.1 1.4 %shard_map.143 = (bf16[128,1024]{1,0:T(8,128)(2,1)S(1)}, f32[128,1024]{1,0:T(8,128)S(1)}) custom-call(s32[1]{0:T(128)} %bitcast.offset_ref, s32[1]{0:T(128)} %bitcast.1.part_ref, s32[1]{0:T(128)} %bitcast.2.parity_ref, f32[8,128]{1,0:T(8,128)S(1)} %broadcast_in_dim.15.sink_ref, bf16[128,512]{1,0:T(8,128)(2,1)S(1)} %shard_map.142.mixed_ref, ...), custom_call_target="tpu_custom_call" | custom-call | flops 1000000000 | bytes 5509120 | tf_op jit(solution)/shard_map/pallas_call | solution.py:250
  47.6 0.3 collective-permute-start.20
  47.9 2.7 %collective-permute-done.19 = bf16[128,1024]{1,0:T(8,128)(2,1)S(1)} collective-permute-done((bf16[128,1024]{1,0:T(8,128)(2,1)S(1)}, bf16[128,1024]{1,0:T(8,128)(2,1)S(1)}, u32[]{:S(2)}, u32[]{:S(2)}) %collective-permute-start.19) | collective-permute-done | bytes 262176 | tf_op jit(solution)/shard_map/ppermute | solution.py:536
  50.6 0.1 add_convert_fusion.1
  50.7 5.5 %collective-permute-done.20 = bf16[128,1024]{1,0:T(8,128)(2,1)S(1)} collective-permute-done((bf16[128,1024]{1,0:T(8,128)(2,1)S(1)}, bf16[128,1024]{1,0:T(8,128)(2,1)S(1)}, u32[]{:S(2)}, u32[]{:S(2)}) %collective-permute-start.20) | collective-permute-done | bytes 262176 | tf_op jit(solution)/shard_map/ppermute | solution.py:536
  56.2 0.1 add_convert_fusion
  56.3 0.8 %pad_maximum_fusion = bf16[256,1024]{1,0:T(8,128)(2,1)} fusion(bf16[128,1024]{1,0:T(8,128)(2,1)S(1)} %add_convert_fusion, bf16[128,1024]{1,0:T(8,128)(2,1)S(1)} %add_convert_fusion.1), kind=kLoop, calls=%fused_computation | loop fusion | flops 1048576 | bytes 1048576 | tf_op jit(solution)/shard_map/concatenate | solution.py:653
  (7 shorter events, 0.0 us)
Async XLA Ops:
  0.0 6.6 %copy-start.4 = (f32[128]{0:T(128)S(1)}, f32[128]{0:T(128)}, u32[]{:S(2)}) copy-start(f32[128]{0:T(128)} %param.23) | copy-start | bytes 1540
  0.0 23.3 %copy-start.5 = (f32[8]{0:T(128)S(1)}, f32[8]{0:T(128)}, u32[]{:S(2)}) copy-start(f32[8]{0:T(128)} %param.19) | copy-start | bytes 100
  2.2 4.4 %collective-permute-start = (bf16[256,256]{1,0:T(8,128)(2,1)S(1)}, bf16[256,256]{1,0:T(8,128)(2,1)S(1)}, u32[]{:S(2)}, u32[]{:S(2)}) collective-permute-start(bf16[256,256]{1,0:T(8,128)(2,1)S(1)} %get-tuple-element.29), channel_id=1, source_target_pairs={{0,1},{1,0},{2,3},{3,2},{4,5},{5,4},{6,7},{7,6},{8,9},{9,8},{10,11... | collective-permute-start | bytes 393224 | tf_op jit(solution)/shard_map/ppermute | solution.py:536
  3.5 24.0 %collective-permute-start.16 = (bf16[256,1024]{1,0:T(8,128)(2,1)S(1)}, bf16[256,1024]{1,0:T(8,128)(2,1)S(1)}, u32[]{:S(2)}, u32[]{:S(2)}) collective-permute-start(bf16[256,1024]{1,0:T(8,128)(2,1)S(1)} %get-tuple-element.31.refs_4_), channel_id=1, source_target_pairs={{0,1},{1,0},{2,3},{3,2},{4,5},{5,4},{6,7},{7,6},{8,9},{9,8},{10,11... | collective-permute-start | bytes 1572872 | tf_op jit(solution)/shard_map/ppermute | solution.py:536
  7.0 4.8 %collective-permute-start.1 = (bf16[384,128]{1,0:T(8,128)(2,1)S(1)}, bf16[384,128]{1,0:T(8,128)(2,1)S(1)}, u32[]{:S(2)}, u32[]{:S(2)}) collective-permute-start(bf16[384,128]{1,0:T(8,128)(2,1)S(1)} %get-tuple-element.30.refs_0_), channel_id=1, source_target_pairs={{0,8},{2,10},{4,12},{6,14},{8,0},{10,2},{12,4},{14,6},{16,24},{18,... | collective-permute-start | bytes 294920 | tf_op jit(solution)/shard_map/ppermute | solution.py:536
  7.3 8.4 %collective-permute-start.2 = (bf16[384,128]{1,0:T(8,128)(2,1)S(1)}, bf16[384,128]{1,0:T(8,128)(2,1)S(1)}, u32[]{:S(2)}, u32[]{:S(2)}) collective-permute-start(bf16[384,128]{1,0:T(8,128)(2,1)S(1)} %get-tuple-element.30.refs_0_), channel_id=1, source_target_pairs={{0,16},{2,18},{4,20},{6,22},{8,24},{10,26},{12,28},{14,30},{16,0},... | collective-permute-start | bytes 294920 | tf_op jit(solution)/shard_map/ppermute | solution.py:536
  7.4 9.6 %collective-permute-start.3 = (bf16[384,128]{1,0:T(8,128)(2,1)S(1)}, bf16[384,128]{1,0:T(8,128)(2,1)S(1)}, u32[]{:S(2)}, u32[]{:S(2)}) collective-permute-start(bf16[384,128]{1,0:T(8,128)(2,1)S(1)} %get-tuple-element.30.refs_0_), channel_id=1, source_target_pairs={{0,24},{2,26},{4,28},{6,30},{8,16},{10,18},{12,20},{14,22},{16,8},... | collective-permute-start | bytes 294920 | tf_op jit(solution)/shard_map/ppermute | solution.py:536
  10.6 6.5 %collective-permute-start.4 = (bf16[384,128]{1,0:T(8,128)(2,1)S(1)}, bf16[384,128]{1,0:T(8,128)(2,1)S(1)}, u32[]{:S(2)}, u32[]{:S(2)}) collective-permute-start(bf16[384,128]{1,0:T(8,128)(2,1)S(1)} %get-tuple-element.30.refs_0_), channel_id=1, source_target_pairs={{0,4},{2,6},{4,0},{6,2},{8,12},{10,14},{12,8},{14,10},{16,20},{18,... | collective-permute-start | bytes 294920 | tf_op jit(solution)/shard_map/ppermute | solution.py:536
  11.9 8.8 %collective-permute-start.8 = (bf16[384,128]{1,0:T(8,128)(2,1)S(1)}, bf16[384,128]{1,0:T(8,128)(2,1)S(1)}, u32[]{:S(2)}, u32[]{:S(2)}) collective-permute-start(bf16[384,128]{1,0:T(8,128)(2,1)S(1)} %get-tuple-element.30.refs_0_), channel_id=1, source_target_pairs={{0,2},{2,0},{4,6},{6,4},{8,10},{10,8},{12,14},{14,12},{16,18},{18,... | collective-permute-start | bytes 294920 | tf_op jit(solution)/shard_map/ppermute | solution.py:536
  15.7 6.2 %collective-permute-start.5 = (bf16[384,128]{1,0:T(8,128)(2,1)S(1)}, bf16[384,128]{1,0:T(8,128)(2,1)S(1)}, u32[]{:S(2)}, u32[]{:S(2)}) collective-permute-start(bf16[384,128]{1,0:T(8,128)(2,1)S(1)} %collective-permute-done.1.refs_1_), channel_id=1, source_target_pairs={{0,4},{2,6},{4,0},{6,2},{8,12},{10,14},{12,8},{14,10},{16,20},{18,... | collective-permute-start | bytes 294920 | tf_op jit(solution)/shard_map/ppermute | solution.py:536
  16.9 6.3 %collective-permute-start.6 = (bf16[384,128]{1,0:T(8,128)(2,1)S(1)}, bf16[384,128]{1,0:T(8,128)(2,1)S(1)}, u32[]{:S(2)}, u32[]{:S(2)}) collective-permute-start(bf16[384,128]{1,0:T(8,128)(2,1)S(1)} %collective-permute-done.2.refs_2_), channel_id=1, source_target_pairs={{0,4},{2,6},{4,0},{6,2},{8,12},{10,14},{12,8},{14,10},{16,20},{18,... | collective-permute-start | bytes 294920 | tf_op jit(solution)/shard_map/ppermute | solution.py:536
  17.2 9.7 %collective-permute-start.10 = (bf16[384,128]{1,0:T(8,128)(2,1)S(1)}, bf16[384,128]{1,0:T(8,128)(2,1)S(1)}, u32[]{:S(2)}, u32[]{:S(2)}) collective-permute-start(bf16[384,128]{1,0:T(8,128)(2,1)S(1)} %collective-permute-done.2.refs_2_), channel_id=1, source_target_pairs={{0,2},{2,0},{4,6},{6,4},{8,10},{10,8},{12,14},{14,12},{16,18},{18,... | collective-permute-start | bytes 294920 | tf_op jit(solution)/shard_map/ppermute | solution.py:536
  20.7 5.1 %collective-permute-start.7 = (bf16[384,128]{1,0:T(8,128)(2,1)S(1)}, bf16[384,128]{1,0:T(8,128)(2,1)S(1)}, u32[]{:S(2)}, u32[]{:S(2)}) collective-permute-start(bf16[384,128]{1,0:T(8,128)(2,1)S(1)} %collective-permute-done.3.refs_3_), channel_id=1, source_target_pairs={{0,4},{2,6},{4,0},{6,2},{8,12},{10,14},{12,8},{14,10},{16,20},{18,... | collective-permute-start | bytes 294920 | tf_op jit(solution)/shard_map/ppermute | solution.py:536
  21.9 5.0 %collective-permute-start.11 = (bf16[384,128]{1,0:T(8,128)(2,1)S(1)}, bf16[384,128]{1,0:T(8,128)(2,1)S(1)}, u32[]{:S(2)}, u32[]{:S(2)}) collective-permute-start(bf16[384,128]{1,0:T(8,128)(2,1)S(1)} %collective-permute-done.3.refs_3_), channel_id=1, source_target_pairs={{0,2},{2,0},{4,6},{6,4},{8,10},{10,8},{12,14},{14,12},{16,18},{18,... | collective-permute-start | bytes 294920 | tf_op jit(solution)/shard_map/ppermute | solution.py:536
  23.3 7.5 %copy-start.3 = (bf16[128,512]{1,0:T(8,128)(2,1)S(1)}, bf16[128,512]{1,0:T(8,128)(2,1)}, u32[]{:S(2)}) copy-start(bf16[128,512]{1,0:T(8,128)(2,1)} %up_ref.3) | copy-start | bytes 393220
  23.3 9.9 %collective-permute-start.9 = (bf16[384,128]{1,0:T(8,128)(2,1)S(1)}, bf16[384,128]{1,0:T(8,128)(2,1)S(1)}, u32[]{:S(2)}, u32[]{:S(2)}) collective-permute-start(bf16[384,128]{1,0:T(8,128)(2,1)S(1)} %collective-permute-done.1.refs_1_), channel_id=1, source_target_pairs={{0,2},{2,0},{4,6},{6,4},{8,10},{10,8},{12,14},{14,12},{16,18},{18,... | collective-permute-start | bytes 294920 | tf_op jit(solution)/shard_map/ppermute | solution.py:536
  25.8 6.8 %collective-permute-start.12 = (bf16[384,128]{1,0:T(8,128)(2,1)S(1)}, bf16[384,128]{1,0:T(8,128)(2,1)S(1)}, u32[]{:S(2)}, u32[]{:S(2)}) collective-permute-start(bf16[384,128]{1,0:T(8,128)(2,1)S(1)} %collective-permute-done.4.refs_4_), channel_id=1, source_target_pairs={{0,2},{2,0},{4,6},{6,4},{8,10},{10,8},{12,14},{14,12},{16,18},{18,... | collective-permute-start | bytes 294920 | tf_op jit(solution)/shard_map/ppermute | solution.py:536
  26.9 9.0 %collective-permute-start.13 = (bf16[384,128]{1,0:T(8,128)(2,1)S(1)}, bf16[384,128]{1,0:T(8,128)(2,1)S(1)}, u32[]{:S(2)}, u32[]{:S(2)}) collective-permute-start(bf16[384,128]{1,0:T(8,128)(2,1)S(1)} %collective-permute-done.5.refs_5_), channel_id=1, source_target_pairs={{0,2},{2,0},{4,6},{6,4},{8,10},{10,8},{12,14},{14,12},{16,18},{18,... | collective-permute-start | bytes 294920 | tf_op jit(solution)/shard_map/ppermute | solution.py:536
  26.9 9.0 %collective-permute-start.14 = (bf16[384,128]{1,0:T(8,128)(2,1)S(1)}, bf16[384,128]{1,0:T(8,128)(2,1)S(1)}, u32[]{:S(2)}, u32[]{:S(2)}) collective-permute-start(bf16[384,128]{1,0:T(8,128)(2,1)S(1)} %collective-permute-done.6.refs_6_), channel_id=1, source_target_pairs={{0,2},{2,0},{4,6},{6,4},{8,10},{10,8},{12,14},{14,12},{16,18},{18,... | collective-permute-start | bytes 294920 | tf_op jit(solution)/shard_map/ppermute | solution.py:536
  27.4 8.5 %collective-permute-start.15 = (bf16[384,128]{1,0:T(8,128)(2,1)S(1)}, bf16[384,128]{1,0:T(8,128)(2,1)S(1)}, u32[]{:S(2)}, u32[]{:S(2)}) collective-permute-start(bf16[384,128]{1,0:T(8,128)(2,1)S(1)} %collective-permute-done.7.refs_7_), channel_id=1, source_target_pairs={{0,2},{2,0},{4,6},{6,4},{8,10},{10,8},{12,14},{14,12},{16,18},{18,... | collective-permute-start | bytes 294920 | tf_op jit(solution)/shard_map/ppermute | solution.py:536
  32.6 5.9 %collective-permute-start.17 = (bf16[128,512]{1,0:T(8,128)(2,1)S(1)}, bf16[128,512]{1,0:T(8,128)(2,1)S(1)}, u32[]{:S(2)}, u32[]{:S(2)}) collective-permute-start(bf16[128,512]{1,0:T(8,128)(2,1)S(1)} %get-tuple-element.44), channel_id=1, source_target_pairs={{0,2},{2,0},{4,6},{6,4},{8,10},{10,8},{12,14},{14,12},{16,18},{18,... | collective-permute-start | bytes 393224 | tf_op jit(solution)/shard_map/ppermute | solution.py:631
  33.1 7.7 %collective-permute-start.18 = (bf16[128,512]{1,0:T(8,128)(2,1)S(1)}, bf16[128,512]{1,0:T(8,128)(2,1)S(1)}, u32[]{:S(2)}, u32[]{:S(2)}) collective-permute-start(bf16[128,512]{1,0:T(8,128)(2,1)S(1)} %get-tuple-element.46), channel_id=1, source_target_pairs={{2,4},{4,2},{6,8},{8,6},{10,12},{12,10},{14,16},{16,14},{18,20},{2... | collective-permute-start | bytes 393224 | tf_op jit(solution)/shard_map/ppermute | solution.py:632
  36.0 4.9 %copy-start = (bf16[512,2048]{1,0:T(8,128)(2,1)S(1)}, bf16[512,2048]{1,0:T(8,128)(2,1)}, u32[]{:S(2)}) copy-start(bf16[512,2048]{1,0:T(8,128)(2,1)} %ow_ref.3) | copy-start | bytes 6291460
  36.0 4.9 %copy-start.1 = (bf16[512,2048]{1,0:T(8,128)(2,1)S(1)}, bf16[512,2048]{1,0:T(8,128)(2,1)}, u32[]{:S(2)}) copy-start(bf16[512,2048]{1,0:T(8,128)(2,1)} %ol_ref.3) | copy-start | bytes 6291460
  36.0 4.9 %copy-start.2 = (bf16[128,512]{1,0:T(8,128)(2,1)S(1)}, bf16[128,512]{1,0:T(8,128)(2,1)}, u32[]{:S(2)}) copy-start(bf16[128,512]{1,0:T(8,128)(2,1)} %up_ref.5) | copy-start | bytes 393220
  42.3 8.3 %collective-permute-start.19 = (bf16[128,1024]{1,0:T(8,128)(2,1)S(1)}, bf16[128,1024]{1,0:T(8,128)(2,1)S(1)}, u32[]{:S(2)}, u32[]{:S(2)}) collective-permute-start(bf16[128,1024]{1,0:T(8,128)(2,1)S(1)} %get-tuple-element.48), channel_id=1, source_target_pairs={{0,1},{1,0},{2,3},{3,2},{4,5},{5,4},{6,7},{7,6},{8,9},{9,8},{10,11... | collective-permute-start | bytes 786440 | tf_op jit(solution)/shard_map/ppermute | solution.py:536
  47.6 8.6 %collective-permute-start.20 = (bf16[128,1024]{1,0:T(8,128)(2,1)S(1)}, bf16[128,1024]{1,0:T(8,128)(2,1)S(1)}, u32[]{:S(2)}, u32[]{:S(2)}) collective-permute-start(bf16[128,1024]{1,0:T(8,128)(2,1)S(1)} %get-tuple-element.50), channel_id=1, source_target_pairs={{0,1},{1,0},{2,3},{3,2},{4,5},{5,4},{6,7},{7,6},{8,9},{9,8},{10,11... | collective-permute-start | bytes 786440 | tf_op jit(solution)/shard_map/ppermute | solution.py:536

commit v4 on v3

--- a/solution.py
+++ b/solution.py
@@ -266,11 +266,11 @@
 
 
 def compress_body(
-    offset_ref, part_ref, parity_ref, x_hbm, gain_hbm, down_hbm, rope_hbm, norm_ref, own_ref, send_ref,
+    offset_ref, part_ref, parity_ref, other_ref, x_hbm, gain_hbm, down_hbm, rope_hbm, norm_ref, own_ref, send_ref,
     x_ref, gain_ref, down_ref, rope_ref, sems,
 ):
     rows, half = x_hbm.shape
-    del offset_ref, parity_ref
+    del offset_ref, parity_ref, other_ref
     start = pl.multiple_of(part_ref[0] * half, half)
     copies = [
         pltpu.make_async_copy(x_hbm, x_ref, sems.at[0]),
@@ -413,15 +413,11 @@
             qb_ref[c, lat:, cols] = second[:, rowsl]
 
 
-def attend_body(*refs, groups, chunk, rows):
-    qa_ref, qb_ref, mixed_ref = refs[-3:]
+def attend(groups, qa, qb, state):
+    rows = groups[0][0].shape[0] * 2 // 3
     half = rows // 2
-    columns = qa_ref.shape[2]
-    steps = []
-    start = 0
-    for size in groups:
-        steps += [(refs[start : start + size], 0, qa_ref), (refs[start : start + size], 1, qb_ref)]
-        start += size
+    columns = qa.shape[1]
+    steps = [(blocks, part, table) for blocks in groups for part, table in ((0, qa), (1, qb))]
 
     def keys_of(step):
         blocks, part, _ = step
@@ -429,46 +425,64 @@
 
     def score_of(step):
         rope = jnp.concatenate([b[rows : rows + half] for b in step[0]], axis=0)
-        return dot(jnp.concatenate([keys_of(step), rope], axis=1), step[2][chunk])
-
-    peak = jnp.full((1, columns), MASKED, F32)
-    total = jnp.zeros((8, columns), F32)
-    weighted = jnp.zeros((LANES, columns), F32)
+        return dot(jnp.concatenate([keys_of(step), rope], axis=1), step[2])
+
+    peak, total, weighted = state
     coming = score_of(steps[0])
     for i, step in enumerate(steps):
         score = coming
         if i + 1 < len(steps):
             coming = score_of(steps[i + 1])
-        top = jnp.maximum(peak, jnp.max(score, axis=0, keepdims=True))
-        factor = jnp.exp2(peak - top)
+        top = jnp.max(score, axis=0, keepdims=True)
+        if peak is not None:
+            top = jnp.maximum(peak, top)
         weight = jnp.exp2(score - top)
-        total = total * factor + jnp.sum(weight.reshape(-1, 8, columns), axis=0)
-        weighted = weighted * factor + dot(keys_of(step), weight.astype(BF16), ((0,), (0,)))
-        peak = top
-    mixed_ref[...] = (weighted / jnp.sum(total, axis=0, keepdims=True)).astype(BF16)
+        new_total = jnp.sum(weight.reshape(-1, 8, columns), axis=0)
+        new_weighted = dot(keys_of(step), weight.astype(BF16), ((0,), (0,)))
+        if peak is not None:
+            factor = jnp.exp2(peak - top)
+            new_total = total * factor + new_total
+            new_weighted = weighted * factor + new_weighted
+        peak, total, weighted = top, new_total, new_weighted
+    return peak, total, weighted
+
+
+def begin_body(chunk_ref, *refs, groups):
+    chunk = chunk_ref[0]
+    qa_ref, qb_ref, stat_ref, sum_ref = refs[sum(groups) :]
+    blocks = list(refs[: sum(groups)])
+    parts = [[blocks.pop(0) for _ in range(size)] for size in groups]
+    peak, total, weighted = attend(parts, qa_ref[chunk], qb_ref[chunk], (None, None, None))
+    stat_ref[:8] = jnp.broadcast_to(peak, total.shape)
+    stat_ref[8:] = total
+    sum_ref[...] = weighted
 
 
 def finish_body(
-    offset_ref, part_ref, parity_ref, sink_ref, mixed_ref, q_ref, inner_ref, kv_ref, outer_ref, up_ref, ow_ref, ol_ref,
-    send_ref, keep_ref, cat_ref, *, chunk, seq_total,
+    offset_ref, part_ref, chunk_ref, *refs, groups, seq_total,
 ):
-    span, columns = send_ref.shape[0], mixed_ref.shape[1]
-    mixed = mixed_ref[...]
+    count = sum(groups)
+    (
+        qa_ref, qb_ref, stat_ref, sum_ref, sink_ref, q_ref, halo_ref, kv_ref, up_ref,
+        ow_ref, ol_ref, send_ref, keep_ref, cat_ref, pad_ref,
+    ) = refs[count:]
+    chunk = chunk_ref[0]
+    total, weighted = stat_ref[8:], sum_ref[...]
+    if count:
+        blocks = list(refs[:count])
+        parts = [[blocks.pop(0) for _ in range(size)] for size in groups]
+        state = (stat_ref[:1], total, weighted)
+        _, total, weighted = attend(parts, qa_ref[chunk], qb_ref[chunk], state)
+    mixed = (weighted / jnp.sum(total, axis=0, keepdims=True)).astype(BF16)
+    span, columns = send_ref.shape[0], mixed.shape[1]
     heads_l = columns // span
     _, key_heads, lanes, width = q_ref.shape
     group = width // span
     shared = lanes // DH
     own_rows = kv_ref.shape[0]
-    even = parity_ref[0] == 0
-    pieces = []
-    if chunk == 0:
-        pieces = [jnp.where(even, outer_ref[...], inner_ref[...])]
-    low_row = max(chunk * span - WINDOW, 0)
-    high_row = min((chunk + 1) * span + WINDOW, own_rows)
-    pieces.append(kv_ref[low_row:high_row])
-    if (chunk + 1) * span == own_rows:
-        pieces.append(jnp.where(even, inner_ref[...], outer_ref[...]))
-    padded = jnp.concatenate(pieces, axis=0)
+    pad_ref[pl.ds(pl.multiple_of((1 - chunk) * WINDOW, WINDOW), own_rows), :] = kv_ref[...]
+    pad_ref[pl.ds(pl.multiple_of(chunk * own_rows, WINDOW), WINDOW), :] = halo_ref[...]
+    padded = pad_ref[...]
     offset = offset_ref[0]
     key_pos = lax.broadcasted_iota(jnp.int32, (span + 2 * WINDOW, span), 0) - WINDOW
     query_pos = lax.broadcasted_iota(jnp.int32, (span + 2 * WINDOW, span), 1)
@@ -531,6 +545,31 @@
     keep_ref[...] = jnp.where(lower, first, second)
 
 
+def store_body(chunk_ref, *refs, fresh):
+    keep_ref, got_ref, out_ref, row_ref, sem = refs if fresh else refs[1:]
+    span = keep_ref.shape[0]
+    row_ref[...] = (keep_ref[...] + got_ref[...].astype(F32)).astype(BF16)
+    place = pl.multiple_of(chunk_ref[0] * span, span)
+    copy = pltpu.make_async_copy(row_ref, out_ref.at[pl.ds(place, span), :], sem)
+    copy.start()
+    copy.wait()
+
+
+def store(chunk, keep, got, rows, whole_out=None):
+    fresh = whole_out is None
+    hbm = pl.BlockSpec(memory_space=pltpu.HBM)
+    return pl.pallas_call(
+        partial(store_body, fresh=fresh),
+        out_shape=jax.ShapeDtypeStruct((rows, keep.shape[1]), BF16),
+        in_specs=scalars(1) + ([] if fresh else [hbm]) + whole(2),
+        out_specs=hbm,
+        scratch_shapes=[pltpu.VMEM(keep.shape, BF16), pltpu.SemaphoreType.DMA],
+        input_output_aliases={} if fresh else {1: 0},
+        name="store" if fresh else "store_rest",
+        compiler_params=pltpu.CompilerParams(vmem_limit_bytes=4 * 2**20),
+    )(chunk[None], *([] if fresh else [whole_out]), keep, got)
+
+
 def swap(cells, axis, bit):
     count = lax.axis_size(axis)
     return lax.ppermute(cells, axis, [(i, i ^ bit) for i in range(count)])
@@ -539,10 +578,17 @@
 def gather(block):
     count = lax.axis_size("sp")
     if count % 4 or count > 16 or count & (count - 1):
-        return [[block_of] for block_of in jnp.split(lax.all_gather(block, "sp", axis=0, tiled=True), count)]
+        pieces = jnp.split(lax.all_gather(block, "sp", axis=0, tiled=True), count)
+        return [pieces[: count // 2], pieces[count // 2 :]]
     line = [block] + [swap(block, "sp", 4 * k) for k in range(1, count // 4)]
     mine = line + [swap(b, "sp", 2) for b in line]
-    return [mine, [swap(b, "sp", 1) for b in mine]]
+    across = [swap(b, "sp", 1) for b in mine]
+    late = len(line) // 2
+    early = len(mine) - late
+    return [
+        [*mine[:late], *across[:late], *mine[late:early], *across[late:early]],
+        [*mine[early:], *across[early:]],
+    ]
 
 
 def per_device(
@@ -570,6 +616,7 @@
 
     heads = sink_logit.shape[0]
     parity = lax.axis_index("sp").astype(jnp.int32) % 2
+    flip = 1 - parity
 
     places = (offset + jnp.arange(rows, dtype=jnp.int32)).astype(F32)
     angles = rotary_angles(places, D_ROPE)
@@ -580,7 +627,7 @@
     normalized, own, send = call(
         compress_body,
         [shape((rows, half), BF16), shape((rows, lat + LANES), F32), shape((rows, lat + LANES), BF16)],
-        [offset[None], part[None], parity[None]], [activations, norm_gain[None], key_value_down_weight, rope_key.T], [],
+        [offset[None], part[None], parity[None], flip[None]], [activations, norm_gain[None], key_value_down_weight, rope_key.T], [],
         2 * rows * half * 192, 8,
         [
             pltpu.VMEM((rows, half), BF16),
@@ -629,28 +676,49 @@
         2 * rows * half * 1792, 16,
     )
     inner = lax.ppermute(inward, "sp", [(i, i ^ 1) for i in range(count) if i ^ 1 < count])
+
+    def partner(i):
+        other = i + 1 if i % 2 else i - 1
+        return other if 0 <= other < count else i
+
     outer = lax.ppermute(
-        outward, "sp", [(i, (i - 1 ^ 1) + 1) for i in range(1, count) if (i - 1 ^ 1) + 1 < count]
+        outward, "sp", [(i, partner(i)) for i in range(count)]
     )
 
     sinks = jnp.broadcast_to(sink_logit[:, None] * LOG2E, (heads, LANES))
     kept = []
-    flat = [b for group in groups for b in group]
-    for c in range(chunks):
-        mixed = call(
-            partial(attend_body, groups=[len(g) for g in groups], chunk=c, rows=rows),
-            shape((lat, columns), BF16), [], [], [*flat, table_a, table_b], 3e9, 32,
+    assert chunks == 2
+    result = None
+    order = (flip, parity)
+    for c, (chunk, halo) in enumerate(zip(order, (inner, outer))):
+        first = groups[:1] if c == 0 else groups
+        last = groups[1:] if c == 0 else []
+        sizes = []
+        for g in first:
+            sizes += [len(g) // 2, len(g) - len(g) // 2] if len(g) > 8 else [len(g)]
+        state = call(
+            partial(begin_body, groups=sizes),
+            [shape((16, columns), F32), shape((lat, columns), F32)],
+            [chunk[None]], [], [*(b for g in first for b in g), table_a, table_b], 3e9, 32,
         )
         send, keep = call(
-            partial(finish_body, chunk=c, seq_total=rows * count),
+            partial(finish_body, groups=[len(g) for g in last], seq_total=rows * count),
             [shape((span, half), BF16), shape((span, half), F32)],
-            [offset[None], part[None], parity[None]], [],
-            [sinks, mixed, queries, inner, key_value, outer, value_up_weight, out_win, out_lat],
+            [offset[None], part[None], chunk[None]], [],
+            [
+                *(b for g in last for b in g), table_a, table_b, *state, sinks, queries, halo,
+                key_value, value_up_weight, out_win, out_lat,
+            ],
             1e9, 16,
-            [pltpu.VMEM((out_win.shape[0] + out_lat.shape[0], span), BF16)],
+            [
+                pltpu.VMEM((out_win.shape[0] + out_lat.shape[0], span), BF16),
+                pltpu.VMEM((rows + WINDOW, key_value.shape[1]), BF16),
+            ],
         )
-        kept.append((keep, swap(send, "tp", 1)))
-    return jnp.concatenate([(keep + got.astype(F32)).astype(BF16) for keep, got in kept], axis=0)
+        kept.append((chunk, keep, swap(send, "tp", 1)))
+    for chunk, keep, got in kept:
+        result = store(chunk, keep, got, rows, result)
+    return result
 
 
 def solution(mesh):

time: 57.3 us -> 59.4 us (1.037)
  the two profiles are of different devices: /device:TPU:25 before, /device:TPU:0 now
where the time goes in v4:
time: 59.4 us; the launch traced here: 59.3 us
  waiting for transfers between devices  20.3 us (34%)
  starting transfers between devices  19.8 us (33%)
  Pallas kernels  18 us (30%)
  other arithmetic  0.73 us (1%)
    ppermute x19, waiting for transfers between devices, swap(): return lax.ppermute(cells, axis, [(i, i ^ bit) for i in range(count)])  20.3 us
    ppermute x19, starting transfers between devices, swap(): return lax.ppermute(cells, axis, [(i, i ^ bit) for i in range(count)])  16.5 us
    pallas_call x8, Pallas kernels, call(): pl.pallas_call(body, out_shape=outs, in_specs=scalars(len(smem)) + [pl.Bl...  16.4 us
    ppermute x1, starting transfers between devices, per_device(): lax.ppermute(inward, 'sp', [(i, i ^ 1) for i in range(count) if i ^ 1 < c...  2.47 us
    pallas_call x2, Pallas kernels, store(): pl.pallas_call(partial(store_body, fresh=fresh), out_shape=jax.ShapeDtype...  1.55 us
  transfers between devices with their start and end apart: 21, of which 8 were waited for; matrix products, arithmetic and copies ran while one was open for 1% of the time, Pallas kernels for 25%

profile of v4, /device:TPU:0, one launch (start us, length us, event | category | flops | bytes accessed | tf_op | source)
XLA Modules:
  0.0 59.3 jit_solution(6790811667754889136)
XLA Ops:
  0.0 2.2 %shard_map.136 = (bf16[256,1024]{1,0:T(8,128)(2,1)S(1)}, f32[256,256]{1,0:T(8,128)S(1)}, bf16[256,256]{1,0:T(8,128)(2,1)S(1)}) custom-call(s32[1]{0:T(128)} %bitcast.2.offset_ref, s32[1]{0:T(128)} %bitcast.3.part_ref, s32[1]{0:T(128)} %bitcast.parity_ref.chunk_ref, s32[1]{0:T(128)} %bitcast.1.other_ref.chunk_ref, bf16[256,1024]{1,0:T(8,128)(2,1)} %x_hbm.1, ...), custom_call_target="tpu_custom_call" | custom-call | flops 100663296 | bytes 1318912 | tf_op jit(solution)/shard_map/pallas_call | solution.py:250
  2.2 3.0 %collective-permute-start = (bf16[256,256]{1,0:T(8,128)(2,1)S(1)}, bf16[256,256]{1,0:T(8,128)(2,1)S(1)}, u32[]{:S(2)}, u32[]{:S(2)}) collective-permute-start(bf16[256,256]{1,0:T(8,128)(2,1)S(1)} %get-tuple-element.33), channel_id=1, source_target_pairs={{0,1},{1,0},{2,3},{3,2},{4,5},{5,4},{6,7},{7,6},{8,9},{9,8},{10,11... | collective-permute-start | bytes 393224 | tf_op jit(solution)/shard_map/ppermute | solution.py:575
  5.2 0.1 collective-permute-start.7
  5.3 0.5 multiply_cosine_fusion
  5.9 0.2 pad_maximum_fusion.table_ref
  6.0 3.5 %collective-permute-done.got_ref = bf16[256,256]{1,0:T(8,128)(2,1)S(1)} collective-permute-done((bf16[256,256]{1,0:T(8,128)(2,1)S(1)}, bf16[256,256]{1,0:T(8,128)(2,1)S(1)}, u32[]{:S(2)}, u32[]{:S(2)}) %collective-permute-start) | collective-permute-done | bytes 131104 | tf_op jit(solution)/shard_map/ppermute | solution.py:575
  9.6 0.0 copy-done.4
  9.6 0.4 shard_map.137
  10.0 2.2 %collective-permute-start.8 = (bf16[384,128]{1,0:T(8,128)(2,1)S(1)}, bf16[384,128]{1,0:T(8,128)(2,1)S(1)}, u32[]{:S(2)}, u32[]{:S(2)}) collective-permute-start(bf16[384,128]{1,0:T(8,128)(2,1)S(1)} %get-tuple-element.34.refs_0_), channel_id=1, source_target_pairs={{0,8},{2,10},{4,12},{6,14},{8,0},{10,2},{12,4},{14,6},{16,24},{18,... | collective-permute-start | bytes 294920 | tf_op jit(solution)/shard_map/ppermute | solution.py:575
  12.1 2.6 %collective-permute-start.1 = (bf16[384,128]{1,0:T(8,128)(2,1)S(1)}, bf16[384,128]{1,0:T(8,128)(2,1)S(1)}, u32[]{:S(2)}, u32[]{:S(2)}) collective-permute-start(bf16[384,128]{1,0:T(8,128)(2,1)S(1)} %get-tuple-element.34.refs_0_), channel_id=1, source_target_pairs={{0,16},{2,18},{4,20},{6,22},{8,24},{10,26},{12,28},{14,30},{16,0},... | collective-permute-start | bytes 294920 | tf_op jit(solution)/shard_map/ppermute | solution.py:575
  14.7 0.0 collective-permute-start.3
  14.7 1.7 %collective-permute-start.11 = (bf16[384,128]{1,0:T(8,128)(2,1)S(1)}, bf16[384,128]{1,0:T(8,128)(2,1)S(1)}, u32[]{:S(2)}, u32[]{:S(2)}) collective-permute-start(bf16[384,128]{1,0:T(8,128)(2,1)S(1)} %get-tuple-element.34.refs_0_), channel_id=1, source_target_pairs={{0,4},{2,6},{4,0},{6,2},{8,12},{10,14},{12,8},{14,10},{16,20},{18,... | collective-permute-start | bytes 294920 | tf_op jit(solution)/shard_map/ppermute | solution.py:575
  16.5 0.0 collective-permute-done.8.refs_1_
  16.5 0.0 collective-permute-start.9
  16.5 3.2 %collective-permute-done.1.refs_4_ = bf16[384,128]{1,0:T(8,128)(2,1)S(1)} collective-permute-done((bf16[384,128]{1,0:T(8,128)(2,1)S(1)}, bf16[384,128]{1,0:T(8,128)(2,1)S(1)}, u32[]{:S(2)}, u32[]{:S(2)}) %collective-permute-start.1) | collective-permute-done | bytes 98336 | tf_op jit(solution)/shard_map/ppermute | solution.py:575
  19.7 1.5 %collective-permute-start.12 = (bf16[384,128]{1,0:T(8,128)(2,1)S(1)}, bf16[384,128]{1,0:T(8,128)(2,1)S(1)}, u32[]{:S(2)}, u32[]{:S(2)}) collective-permute-start(bf16[384,128]{1,0:T(8,128)(2,1)S(1)} %collective-permute-done.8.refs_1_), channel_id=1, source_target_pairs={{0,4},{2,6},{4,0},{6,2},{8,12},{10,14},{12,8},{14,10},{16,20},{18,... | collective-permute-start | bytes 294920 | tf_op jit(solution)/shard_map/ppermute | solution.py:575
  21.2 0.1 collective-permute-done.3.refs_5_
  21.2 1.5 %collective-permute-start.2 = (bf16[384,128]{1,0:T(8,128)(2,1)S(1)}, bf16[384,128]{1,0:T(8,128)(2,1)S(1)}, u32[]{:S(2)}, u32[]{:S(2)}) collective-permute-start(bf16[384,128]{1,0:T(8,128)(2,1)S(1)} %collective-permute-done.1.refs_4_), channel_id=1, source_target_pairs={{0,4},{2,6},{4,0},{6,2},{8,12},{10,14},{12,8},{14,10},{16,20},{18,... | collective-permute-start | bytes 294920 | tf_op jit(solution)/shard_map/ppermute | solution.py:575
  22.8 0.0 collective-permute-done.11.refs_6_
  22.8 0.5 collective-permute-start.4
  23.3 0.0 copy-done.5
  23.3 0.0 collective-permute-done.9.refs_2_
  23.3 0.1 collective-permute-start.10
  23.4 1.0 %collective-permute-done.12.refs_7_ = bf16[384,128]{1,0:T(8,128)(2,1)S(1)} collective-permute-done((bf16[384,128]{1,0:T(8,128)(2,1)S(1)}, bf16[384,128]{1,0:T(8,128)(2,1)S(1)}, u32[]{:S(2)}, u32[]{:S(2)}) %collective-permute-start.12) | collective-permute-done | bytes 98336 | tf_op jit(solution)/shard_map/ppermute | solution.py:575
  24.4 0.0 collective-permute-start.13
  24.4 1.5 %collective-permute-done.2.refs_0_.refs_12_ = bf16[384,128]{1,0:T(8,128)(2,1)S(1)} collective-permute-done((bf16[384,128]{1,0:T(8,128)(2,1)S(1)}, bf16[384,128]{1,0:T(8,128)(2,1)S(1)}, u32[]{:S(2)}, u32[]{:S(2)}) %collective-permute-start.2) | collective-permute-done | bytes 98336 | tf_op jit(solution)/shard_map/ppermute | solution.py:575
  25.9 0.0 collective-permute-start.14
  25.9 1.5 %collective-permute-done.4.refs_1_.refs_13_ = bf16[384,128]{1,0:T(8,128)(2,1)S(1)} collective-permute-done((bf16[384,128]{1,0:T(8,128)(2,1)S(1)}, bf16[384,128]{1,0:T(8,128)(2,1)S(1)}, u32[]{:S(2)}, u32[]{:S(2)}) %collective-permute-start.4) | collective-permute-done | bytes 98336 | tf_op jit(solution)/shard_map/ppermute | solution.py:575
  27.4 0.0 collective-permute-start.15
  27.4 0.0 collective-permute-done.7.got_ref
  27.4 0.5 collective-permute-start.16
  27.9 3.2 %shard_map.138 = (f32[256,256]{1,0:T(8,128)S(1)}, f32[256,256]{1,0:T(8,128)S(1)}, f32[256,512]{1,0:T(8,128)S(1)}, f32[256,768]{1,0:T(8,128)S(1)}, bf16[1024,256]...) custom-call(s32[1]{0:T(128)} %bitcast.3.part_ref, ...), custom_call_target="tpu_custom_call" | custom-call | flops 939524096 | bytes 7864320 | tf_op jit(solution)/shard_map/pallas_call | solution.py:250
  31.1 0.0 copy-done.3
  31.1 1.9 %shard_map.139 = (bf16[2,4,128,256]{3,2,1,0:T(8,128)(2,1)S(1)}, bf16[256,512]{1,0:T(8,128)(2,1)S(1)}, bf16[128,512]{1,0:T(8,128)(2,1)S(1)}, bf16[128,512]{1,0:T(...) custom-call(s32[1]{0:T(128)} %bitcast.parity_ref.chunk_ref, ...), custom_call_target="tpu_custom_call" | custom-call | flops 939524096 | bytes 6422528 | tf_op jit(solution)/shard_map/pallas_call | solution.py:250
  33.0 0.0 collective-permute-done.10.refs_3_
  33.0 0.1 collective-permute-start.5
  33.1 0.0 collective-permute-done.13.refs_8_
  33.1 0.5 collective-permute-start.6
  33.6 0.0 collective-permute-done.14.refs_9_
  33.6 0.8 %collective-permute-start.19 = (bf16[128,512]{1,0:T(8,128)(2,1)S(1)}, bf16[128,512]{1,0:T(8,128)(2,1)S(1)}, u32[]{:S(2)}, u32[]{:S(2)}) collective-permute-start(bf16[128,512]{1,0:T(8,128)(2,1)S(1)} %get-tuple-element.56), channel_id=1, source_target_pairs={{0,0},{2,4},{4,2},{6,8},{8,6},{10,12},{12,10},{14,16},{16,14},{18,... | collective-permute-start | bytes 393224 | tf_op jit(solution)/shard_map/ppermute | solution.py:684
  34.5 0.0 collective-permute-done.15.refs_10_
  34.5 2.5 %collective-permute-start.17 = (bf16[128,512]{1,0:T(8,128)(2,1)S(1)}, bf16[128,512]{1,0:T(8,128)(2,1)S(1)}, u32[]{:S(2)}, u32[]{:S(2)}) collective-permute-start(bf16[128,512]{1,0:T(8,128)(2,1)S(1)} %get-tuple-element.50), channel_id=1, source_target_pairs={{0,2},{2,0},{4,6},{6,4},{8,10},{10,8},{12,14},{14,12},{16,18},{18,... | collective-permute-start | bytes 393224 | tf_op jit(solution)/shard_map/ppermute | solution.py:678
  36.9 0.0 collective-permute-done.16.refs_11_
  36.9 2.2 %shard_map.140 = (f32[16,512]{1,0:T(8,128)S(1)}, f32[128,512]{1,0:T(8,128)S(1)}) custom-call(s32[1]{0:T(128)} %bitcast.1.other_ref.chunk_ref, bf16[384,128]{1,0:T(8,128)(2,1)S(1)} %get-tuple-element.34.refs_0_, bf16[384,128]{1,0:T(8,128)(2,1)S(1)} %collective-permute-done.8.refs_1_, bf16[384,128]{1,0:T(8,128)(2,1)S(1)} %collective-permute-done.9.refs_2_, ...), custom_call_target="tpu_custom_call" | custom-call | flops 3000000000 | bytes 2228224 | tf_op jit(solution)/shard_map/pallas_call | solution.py:250
  39.2 0.0 copy-start
  39.2 0.0 copy-start.1
  39.2 0.0 copy-start.2
  39.2 0.0 collective-permute-done.5.refs_2_.refs_14_
  39.2 0.0 collective-permute-done.6.refs_3_.refs_15_
  39.2 2.8 %shard_map.142 = (f32[16,512]{1,0:T(8,128)S(1)}, f32[128,512]{1,0:T(8,128)S(1)}) custom-call(s32[1]{0:T(128)} %bitcast.parity_ref.chunk_ref, bf16[384,128]{1,0:T(8,128)(2,1)S(1)} %get-tuple-element.34.refs_0_, bf16[384,128]{1,0:T(8,128)(2,1)S(1)} %collective-permute-done.8.refs_1_, bf16[384,128]{1,0:T(8,128)(2,1)S(1)} %collective-permute-done.9.refs_2_, ...), custom_call_target="tpu_custom_call" | custom-call | flops 3000000000 | bytes 2621440 | tf_op jit(solution)/shard_map/pallas_call | solution.py:250
  42.0 0.0 collective-permute-done.17.refs_10_
  42.0 0.1 broadcast_in_dim.20.refs_8_.refs_4_
  42.1 0.0 copy-done
  42.1 0.0 copy-done.1
  42.1 0.0 copy-done.2
  42.1 2.3 %shard_map.141 = (bf16[128,1024]{1,0:T(8,128)(2,1)S(1)}, f32[128,1024]{1,0:T(8,128)S(1)}) custom-call(s32[1]{0:T(128)} %bitcast.2.offset_ref, s32[1]{0:T(128)} %bitcast.3.part_ref, s32[1]{0:T(128)} %bitcast.1.other_ref.chunk_ref, bf16[384,128]{1,0:T(8,128)(2,1)S(1)} %collective-permute-done.2.refs_0_.refs_12_, ...), custom_call_target="tpu_custom_call" | custom-call | flops 1000000000 | bytes 6983680 | tf_op jit(solution)/shard_map/pallas_call | solution.py:250
  44.4 1.6 %collective-permute-start.18 = (bf16[128,1024]{1,0:T(8,128)(2,1)S(1)}, bf16[128,1024]{1,0:T(8,128)(2,1)S(1)}, u32[]{:S(2)}, u32[]{:S(2)}) collective-permute-start(bf16[128,1024]{1,0:T(8,128)(2,1)S(1)} %get-tuple-element.53), channel_id=1, source_target_pairs={{0,1},{1,0},{2,3},{3,2},{4,5},{5,4},{6,7},{7,6},{8,9},{9,8},{10,11... | collective-permute-start | bytes 786440 | tf_op jit(solution)/shard_map/ppermute | solution.py:575
  45.9 0.0 collective-permute-done.19.refs_6_
  45.9 1.5 %shard_map.143 = (bf16[128,1024]{1,0:T(8,128)(2,1)S(1)}, f32[128,1024]{1,0:T(8,128)S(1)}) custom-call(s32[1]{0:T(128)} %bitcast.2.offset_ref, s32[1]{0:T(128)} %bitcast.3.part_ref, s32[1]{0:T(128)} %bitcast.parity_ref.chunk_ref, bf16[2,256,512]{2,1,0:T(8,128)(2,1)S(1)} %get-tuple-element.45.refs_12_.refs_4_.refs_16_.refs_0_, ...), custom_call_target="tpu_custom_call" | custom-call | flops 1000000000 | bytes 6590464 | tf_op jit(solution)/shard_map/pallas_call | solution.py:250
  47.4 0.6 %collective-permute-start.20 = (bf16[128,1024]{1,0:T(8,128)(2,1)S(1)}, bf16[128,1024]{1,0:T(8,128)(2,1)S(1)}, u32[]{:S(2)}, u32[]{:S(2)}) collective-permute-start(bf16[128,1024]{1,0:T(8,128)(2,1)S(1)} %get-tuple-element.58), channel_id=1, source_target_pairs={{0,1},{1,0},{2,3},{3,2},{4,5},{5,4},{6,7},{7,6},{8,9},{9,8},{10,11... | collective-permute-start | bytes 786440 | tf_op jit(solution)/shard_map/ppermute | solution.py:575
  48.1 5.6 %collective-permute-done.18.refs_1_ = bf16[128,1024]{1,0:T(8,128)(2,1)S(1)} collective-permute-done((bf16[128,1024]{1,0:T(8,128)(2,1)S(1)}, bf16[128,1024]{1,0:T(8,128)(2,1)S(1)}, u32[]{:S(2)}, u32[]{:S(2)}) %collective-permute-start.18) | collective-permute-done | bytes 262176 | tf_op jit(solution)/shard_map/ppermute | solution.py:575
  53.6 0.8 %store.1.refs_0_ = bf16[256,1024]{1,0:T(8,128)(2,1)} custom-call(s32[1]{0:T(128)} %bitcast.1.other_ref.chunk_ref, f32[128,1024]{1,0:T(8,128)S(1)} %get-tuple-element.52.refs_0_, bf16[128,1024]{1,0:T(8,128)(2,1)S(1)} %collective-permute-done.18.refs_1_), custom_call_target="tpu_custom_call" | custom-call | tf_op jit(solution)/shard_map/store/pallas_call | solution.py:561
  54.4 3.9 %collective-permute-done.20.refs_2_ = bf16[128,1024]{1,0:T(8,128)(2,1)S(1)} collective-permute-done((bf16[128,1024]{1,0:T(8,128)(2,1)S(1)}, bf16[128,1024]{1,0:T(8,128)(2,1)S(1)}, u32[]{:S(2)}, u32[]{:S(2)}) %collective-permute-start.20) | collective-permute-done | bytes 262176 | tf_op jit(solution)/shard_map/ppermute | solution.py:575
  58.3 0.8 %store_rest.1 = bf16[256,1024]{1,0:T(8,128)(2,1)} custom-call(s32[1]{0:T(128)} %bitcast.parity_ref.chunk_ref, bf16[256,1024]{1,0:T(8,128)(2,1)} %store.1.refs_0_, f32[128,1024]{1,0:T(8,128)S(1)} %get-tuple-element.57.refs_1_, bf16[128,1024]{1,0:T(8,128)(2,1)S(1)} %collective-permute-done.20.refs_2_), custom_call_target="tpu_custom_call", output_to_operand_aliasing={{}: (1, {})} | custom-call | tf_op jit(solution)/shard_map/store_rest/pallas_call | solution.py:561
  (6 shorter events, 0.0 us)
Async XLA Ops:
  0.0 9.6 %copy-start.4 = (f32[128]{0:T(128)S(1)}, f32[128]{0:T(128)}, u32[]{:S(2)}) copy-start(f32[128]{0:T(128)} %param.23) | copy-start | bytes 1540
  0.0 23.3 %copy-start.5 = (f32[8]{0:T(128)S(1)}, f32[8]{0:T(128)}, u32[]{:S(2)}) copy-start(f32[8]{0:T(128)} %param.19) | copy-start | bytes 100
  2.2 7.4 %collective-permute-start = (bf16[256,256]{1,0:T(8,128)(2,1)S(1)}, bf16[256,256]{1,0:T(8,128)(2,1)S(1)}, u32[]{:S(2)}, u32[]{:S(2)}) collective-permute-start(bf16[256,256]{1,0:T(8,128)(2,1)S(1)} %get-tuple-element.33), channel_id=1, source_target_pairs={{0,1},{1,0},{2,3},{3,2},{4,5},{5,4},{6,7},{7,6},{8,9},{9,8},{10,11... | collective-permute-start | bytes 393224 | tf_op jit(solution)/shard_map/ppermute | solution.py:575
  5.2 22.2 %collective-permute-start.7 = (bf16[256,1024]{1,0:T(8,128)(2,1)S(1)}, bf16[256,1024]{1,0:T(8,128)(2,1)S(1)}, u32[]{:S(2)}, u32[]{:S(2)}) collective-permute-start(bf16[256,1024]{1,0:T(8,128)(2,1)S(1)} %get-tuple-element.35.refs_4_), channel_id=1, source_target_pairs={{0,1},{1,0},{2,3},{3,2},{4,5},{5,4},{6,7},{7,6},{8,9},{9,8},{10,11... | collective-permute-start | bytes 1572872 | tf_op jit(solution)/shard_map/ppermute | solution.py:575
  10.0 6.5 %collective-permute-start.8 = (bf16[384,128]{1,0:T(8,128)(2,1)S(1)}, bf16[384,128]{1,0:T(8,128)(2,1)S(1)}, u32[]{:S(2)}, u32[]{:S(2)}) collective-permute-start(bf16[384,128]{1,0:T(8,128)(2,1)S(1)} %get-tuple-element.34.refs_0_), channel_id=1, source_target_pairs={{0,8},{2,10},{4,12},{6,14},{8,0},{10,2},{12,4},{14,6},{16,24},{18,... | collective-permute-start | bytes 294920 | tf_op jit(solution)/shard_map/ppermute | solution.py:575
  12.1 7.5 %collective-permute-start.1 = (bf16[384,128]{1,0:T(8,128)(2,1)S(1)}, bf16[384,128]{1,0:T(8,128)(2,1)S(1)}, u32[]{:S(2)}, u32[]{:S(2)}) collective-permute-start(bf16[384,128]{1,0:T(8,128)(2,1)S(1)} %get-tuple-element.34.refs_0_), channel_id=1, source_target_pairs={{0,16},{2,18},{4,20},{6,22},{8,24},{10,26},{12,28},{14,30},{16,0},... | collective-permute-start | bytes 294920 | tf_op jit(solution)/shard_map/ppermute | solution.py:575
  14.7 6.5 %collective-permute-start.3 = (bf16[384,128]{1,0:T(8,128)(2,1)S(1)}, bf16[384,128]{1,0:T(8,128)(2,1)S(1)}, u32[]{:S(2)}, u32[]{:S(2)}) collective-permute-start(bf16[384,128]{1,0:T(8,128)(2,1)S(1)} %get-tuple-element.34.refs_0_), channel_id=1, source_target_pairs={{0,24},{2,26},{4,28},{6,30},{8,16},{10,18},{12,20},{14,22},{16,8},... | collective-permute-start | bytes 294920 | tf_op jit(solution)/shard_map/ppermute | solution.py:575
  14.7 8.0 %collective-permute-start.11 = (bf16[384,128]{1,0:T(8,128)(2,1)S(1)}, bf16[384,128]{1,0:T(8,128)(2,1)S(1)}, u32[]{:S(2)}, u32[]{:S(2)}) collective-permute-start(bf16[384,128]{1,0:T(8,128)(2,1)S(1)} %get-tuple-element.34.refs_0_), channel_id=1, source_target_pairs={{0,4},{2,6},{4,0},{6,2},{8,12},{10,14},{12,8},{14,10},{16,20},{18,... | collective-permute-start | bytes 294920 | tf_op jit(solution)/shard_map/ppermute | solution.py:575
  16.5 6.8 %collective-permute-start.9 = (bf16[384,128]{1,0:T(8,128)(2,1)S(1)}, bf16[384,128]{1,0:T(8,128)(2,1)S(1)}, u32[]{:S(2)}, u32[]{:S(2)}) collective-permute-start(bf16[384,128]{1,0:T(8,128)(2,1)S(1)} %get-tuple-element.34.refs_0_), channel_id=1, source_target_pairs={{0,2},{2,0},{4,6},{6,4},{8,10},{10,8},{12,14},{14,12},{16,18},{18,... | collective-permute-start | bytes 294920 | tf_op jit(solution)/shard_map/ppermute | solution.py:575
  19.7 4.7 %collective-permute-start.12 = (bf16[384,128]{1,0:T(8,128)(2,1)S(1)}, bf16[384,128]{1,0:T(8,128)(2,1)S(1)}, u32[]{:S(2)}, u32[]{:S(2)}) collective-permute-start(bf16[384,128]{1,0:T(8,128)(2,1)S(1)} %collective-permute-done.8.refs_1_), channel_id=1, source_target_pairs={{0,4},{2,6},{4,0},{6,2},{8,12},{10,14},{12,8},{14,10},{16,20},{18,... | collective-permute-start | bytes 294920 | tf_op jit(solution)/shard_map/ppermute | solution.py:575
  21.2 4.6 %collective-permute-start.2 = (bf16[384,128]{1,0:T(8,128)(2,1)S(1)}, bf16[384,128]{1,0:T(8,128)(2,1)S(1)}, u32[]{:S(2)}, u32[]{:S(2)}) collective-permute-start(bf16[384,128]{1,0:T(8,128)(2,1)S(1)} %collective-permute-done.1.refs_4_), channel_id=1, source_target_pairs={{0,4},{2,6},{4,0},{6,2},{8,12},{10,14},{12,8},{14,10},{16,20},{18,... | collective-permute-start | bytes 294920 | tf_op jit(solution)/shard_map/ppermute | solution.py:575
  22.8 4.6 %collective-permute-start.4 = (bf16[384,128]{1,0:T(8,128)(2,1)S(1)}, bf16[384,128]{1,0:T(8,128)(2,1)S(1)}, u32[]{:S(2)}, u32[]{:S(2)}) collective-permute-start(bf16[384,128]{1,0:T(8,128)(2,1)S(1)} %collective-permute-done.3.refs_5_), channel_id=1, source_target_pairs={{0,4},{2,6},{4,0},{6,2},{8,12},{10,14},{12,8},{14,10},{16,20},{18,... | collective-permute-start | bytes 294920 | tf_op jit(solution)/shard_map/ppermute | solution.py:575
  23.3 7.9 %copy-start.3 = (bf16[128,512]{1,0:T(8,128)(2,1)S(1)}, bf16[128,512]{1,0:T(8,128)(2,1)}, u32[]{:S(2)}) copy-start(bf16[128,512]{1,0:T(8,128)(2,1)} %up_ref.1) | copy-start | bytes 393220
  23.3 9.7 %collective-permute-start.10 = (bf16[384,128]{1,0:T(8,128)(2,1)S(1)}, bf16[384,128]{1,0:T(8,128)(2,1)S(1)}, u32[]{:S(2)}, u32[]{:S(2)}) collective-permute-start(bf16[384,128]{1,0:T(8,128)(2,1)S(1)} %collective-permute-done.8.refs_1_), channel_id=1, source_target_pairs={{0,2},{2,0},{4,6},{6,4},{8,10},{10,8},{12,14},{14,12},{16,18},{18,... | collective-permute-start | bytes 294920 | tf_op jit(solution)/shard_map/ppermute | solution.py:575
  24.4 8.7 %collective-permute-start.13 = (bf16[384,128]{1,0:T(8,128)(2,1)S(1)}, bf16[384,128]{1,0:T(8,128)(2,1)S(1)}, u32[]{:S(2)}, u32[]{:S(2)}) collective-permute-start(bf16[384,128]{1,0:T(8,128)(2,1)S(1)} %collective-permute-done.1.refs_4_), channel_id=1, source_target_pairs={{0,2},{2,0},{4,6},{6,4},{8,10},{10,8},{12,14},{14,12},{16,18},{18,... | collective-permute-start | bytes 294920 | tf_op jit(solution)/shard_map/ppermute | solution.py:575
  25.9 7.8 %collective-permute-start.14 = (bf16[384,128]{1,0:T(8,128)(2,1)S(1)}, bf16[384,128]{1,0:T(8,128)(2,1)S(1)}, u32[]{:S(2)}, u32[]{:S(2)}) collective-permute-start(bf16[384,128]{1,0:T(8,128)(2,1)S(1)} %collective-permute-done.3.refs_5_), channel_id=1, source_target_pairs={{0,2},{2,0},{4,6},{6,4},{8,10},{10,8},{12,14},{14,12},{16,18},{18,... | collective-permute-start | bytes 294920 | tf_op jit(solution)/shard_map/ppermute | solution.py:575
  27.4 7.1 %collective-permute-start.15 = (bf16[384,128]{1,0:T(8,128)(2,1)S(1)}, bf16[384,128]{1,0:T(8,128)(2,1)S(1)}, u32[]{:S(2)}, u32[]{:S(2)}) collective-permute-start(bf16[384,128]{1,0:T(8,128)(2,1)S(1)} %collective-permute-done.11.refs_6_), channel_id=1, source_target_pairs={{0,2},{2,0},{4,6},{6,4},{8,10},{10,8},{12,14},{14,12},{16,18},{18,... | collective-permute-start | bytes 294920 | tf_op jit(solution)/shard_map/ppermute | solution.py:575
  27.4 9.6 %collective-permute-start.16 = (bf16[384,128]{1,0:T(8,128)(2,1)S(1)}, bf16[384,128]{1,0:T(8,128)(2,1)S(1)}, u32[]{:S(2)}, u32[]{:S(2)}) collective-permute-start(bf16[384,128]{1,0:T(8,128)(2,1)S(1)} %collective-permute-done.12.refs_7_), channel_id=1, source_target_pairs={{0,2},{2,0},{4,6},{6,4},{8,10},{10,8},{12,14},{14,12},{16,18},{18,... | collective-permute-start | bytes 294920 | tf_op jit(solution)/shard_map/ppermute | solution.py:575
  33.0 6.2 %collective-permute-start.5 = (bf16[384,128]{1,0:T(8,128)(2,1)S(1)}, bf16[384,128]{1,0:T(8,128)(2,1)S(1)}, u32[]{:S(2)}, u32[]{:S(2)}) collective-permute-start(bf16[384,128]{1,0:T(8,128)(2,1)S(1)} %collective-permute-done.2.refs_0_.refs_12_), channel_id=1, source_target_pairs={{0,2},{2,0},{4,6},{6,4},{8,10},{10,8},{12,14},{14,12},{16,18},{18,... | collective-permute-start | bytes 294920 | tf_op jit(solution)/shard_map/ppermute | solution.py:575
  33.1 6.1 %collective-permute-start.6 = (bf16[384,128]{1,0:T(8,128)(2,1)S(1)}, bf16[384,128]{1,0:T(8,128)(2,1)S(1)}, u32[]{:S(2)}, u32[]{:S(2)}) collective-permute-start(bf16[384,128]{1,0:T(8,128)(2,1)S(1)} %collective-permute-done.4.refs_1_.refs_13_), channel_id=1, source_target_pairs={{0,2},{2,0},{4,6},{6,4},{8,10},{10,8},{12,14},{14,12},{16,18},{18,... | collective-permute-start | bytes 294920 | tf_op jit(solution)/shard_map/ppermute | solution.py:575
  33.6 12.3 %collective-permute-start.19 = (bf16[128,512]{1,0:T(8,128)(2,1)S(1)}, bf16[128,512]{1,0:T(8,128)(2,1)S(1)}, u32[]{:S(2)}, u32[]{:S(2)}) collective-permute-start(bf16[128,512]{1,0:T(8,128)(2,1)S(1)} %get-tuple-element.56), channel_id=1, source_target_pairs={{0,0},{2,4},{4,2},{6,8},{8,6},{10,12},{12,10},{14,16},{16,14},{18,... | collective-permute-start | bytes 393224 | tf_op jit(solution)/shard_map/ppermute | solution.py:684
  34.5 7.5 %collective-permute-start.17 = (bf16[128,512]{1,0:T(8,128)(2,1)S(1)}, bf16[128,512]{1,0:T(8,128)(2,1)S(1)}, u32[]{:S(2)}, u32[]{:S(2)}) collective-permute-start(bf16[128,512]{1,0:T(8,128)(2,1)S(1)} %get-tuple-element.50), channel_id=1, source_target_pairs={{0,2},{2,0},{4,6},{6,4},{8,10},{10,8},{12,14},{14,12},{16,18},{18,... | collective-permute-start | bytes 393224 | tf_op jit(solution)/shard_map/ppermute | solution.py:678
  39.2 2.9 %copy-start = (bf16[512,2048]{1,0:T(8,128)(2,1)S(1)}, bf16[512,2048]{1,0:T(8,128)(2,1)}, u32[]{:S(2)}) copy-start(bf16[512,2048]{1,0:T(8,128)(2,1)} %refs_9_.1) | copy-start | bytes 6291460
  39.2 2.9 %copy-start.1 = (bf16[512,2048]{1,0:T(8,128)(2,1)S(1)}, bf16[512,2048]{1,0:T(8,128)(2,1)}, u32[]{:S(2)}) copy-start(bf16[512,2048]{1,0:T(8,128)(2,1)} %refs_10_.1) | copy-start | bytes 6291460
  39.2 2.9 %copy-start.2 = (bf16[128,512]{1,0:T(8,128)(2,1)S(1)}, bf16[128,512]{1,0:T(8,128)(2,1)}, u32[]{:S(2)}) copy-start(bf16[128,512]{1,0:T(8,128)(2,1)} %refs_8_.1) | copy-start | bytes 393220
  44.4 9.2 %collective-permute-start.18 = (bf16[128,1024]{1,0:T(8,128)(2,1)S(1)}, bf16[128,1024]{1,0:T(8,128)(2,1)S(1)}, u32[]{:S(2)}, u32[]{:S(2)}) collective-permute-start(bf16[128,1024]{1,0:T(8,128)(2,1)S(1)} %get-tuple-element.53), channel_id=1, source_target_pairs={{0,1},{1,0},{2,3},{3,2},{4,5},{5,4},{6,7},{7,6},{8,9},{9,8},{10,11... | collective-permute-start | bytes 786440 | tf_op jit(solution)/shard_map/ppermute | solution.py:575
  47.4 10.9 %collective-permute-start.20 = (bf16[128,1024]{1,0:T(8,128)(2,1)S(1)}, bf16[128,1024]{1,0:T(8,128)(2,1)S(1)}, u32[]{:S(2)}, u32[]{:S(2)}) collective-permute-start(bf16[128,1024]{1,0:T(8,128)(2,1)S(1)} %get-tuple-element.58), channel_id=1, source_target_pairs={{0,1},{1,0},{2,3},{3,2},{4,5},{5,4},{6,7},{7,6},{8,9},{9,8},{10,11... | collective-permute-start | bytes 786440 | tf_op jit(solution)/shard_map/ppermute | solution.py:575

commit v5 on v4

--- a/solution.py
+++ b/solution.py
@@ -2,6 +2,7 @@
 
 import jax
 import jax.numpy as jnp
+import numpy as np
 from jax import lax
 from jax.experimental import pallas as pl
 from jax.experimental.pallas import tpu as pltpu
@@ -290,16 +291,28 @@
     compressed = dot(normalized, down_ref[...])
     copies[3].wait()
     rope = dot(normalized, rope_ref[...], ((1,), (1,)))
-    high = squares.astype(BF16).astype(F32)
-    lane = lax.broadcasted_iota(jnp.int32, (rows, LANES), 1)
-    rope = jnp.concatenate([rope, jnp.zeros((rows, LANES - rope.shape[1]), F32)], axis=1)
-    width = compressed.shape[1]
-    own_ref[:, :width] = compressed
-    own_ref[:, width:] = jnp.where(lane == LANES - 1, squares, jnp.where(lane == LANES - 2, 0.0, rope))
-    send_ref[:, :width] = compressed.astype(BF16)
-    send_ref[:, width:] = jnp.where(
-        lane == LANES - 1, high, jnp.where(lane == LANES - 2, squares - high, rope)
-    ).astype(BF16)
+    middle = rows // 2
+    packed = jnp.concatenate([rope[:middle], rope[middle:]], axis=1)
+    line = jnp.broadcast_to(squares, (rows, LANES)).T[:1]
+    high = line.astype(BF16).astype(F32)
+    own_ref[:rows] = compressed
+    own_ref[rows : rows + middle] = packed
+    own_ref[rows + middle :] = stacked(own_ref.shape[0] - rows - middle, [line])
+    send_ref[:rows] = compressed.astype(BF16)
+    send_ref[rows : rows + middle] = packed.astype(BF16)
+    tail = stacked(own_ref.shape[0] - rows - middle, [high, line - high])
+    send_ref[rows + middle :] = tail.astype(BF16)
+
+
+def stacked(height, lines):
+    row = lax.broadcasted_iota(jnp.int32, (height, LANES), 0)
+    out = jnp.zeros((height, LANES), F32)
+    count = 0
+    for line in lines:
+        for at in range(0, line.shape[1], LANES):
+            out = jnp.where(row == count, line[:, at : at + LANES], out)
+            count += 1
+    return out
 
 
 def turn(vectors, cosines, sines):
@@ -309,28 +322,40 @@
 
 
 def latent_body(own_ref, got_ref, table_ref, gain_ref, block_ref, scale_ref, *, features):
-    rows = own_ref.shape[0]
+    rows = scale_ref.shape[0]
+    middle = rows // 2
     total = own_ref[...] + got_ref[...].astype(F32)
-    width = gain_ref.shape[1]
-    compressed = total[:, :width]
-    rest = total[:, width:]
-    squares = rest[:, LANES - 1 :] + rest[:, LANES - 2 : LANES - 1]
-    row_scale = lax.rsqrt(squares / features + EPSILON)
-    scale_ref[...] = jnp.broadcast_to(row_scale, scale_ref.shape)
+    compressed = total[:rows]
+    packed = total[rows : rows + middle]
+    tail = total[rows + middle :]
+    count = rows // LANES
+    squares = jnp.concatenate(
+        [tail[k : k + 1] + tail[count + k : count + k + 1] for k in range(count)], axis=1
+    )
+    scale = jnp.broadcast_to(lax.rsqrt(squares / features + EPSILON), (LANES, rows)).T
+    scale_ref[...] = scale
     mean = jnp.mean(compressed * compressed, axis=1, keepdims=True)
     block_ref[:rows] = (compressed * lax.rsqrt(mean + EPSILON) * gain_ref[...]).astype(BF16)
-    rope = turn(rest[:, :D_ROPE] * row_scale, table_ref[:, :D_ROPE], table_ref[:, D_ROPE:])
-    packed = jnp.concatenate([rope[: rows // 2], rope[rows // 2 :]], axis=1)
-    block_ref[rows:] = packed.astype(BF16)
-
-
-def own_body(part_ref, *refs, count):
+    rope = jnp.concatenate([packed[:, :D_ROPE], packed[:, D_ROPE:]], axis=0)
+    rope = turn(rope * scale[:, :D_ROPE], table_ref[:, :D_ROPE], table_ref[:, D_ROPE:])
+    block_ref[rows:] = jnp.concatenate([rope[:middle], rope[middle:]], axis=1).astype(BF16)
+
+
+def stage_body(part_ref, w_ref, rest_ref, sem):
+    half = rest_ref.shape[0]
+    theirs = pl.multiple_of((1 - part_ref[0]) * half, half)
+    copy = pltpu.make_async_copy(w_ref.at[pl.ds(theirs, half), :], rest_ref, sem)
+    copy.start()
+    copy.wait()
+
+
+def own_body(offset_ref, part_ref, *refs, count):
+    *refs, sems = refs
     weights = refs[:count]
-    own_ref = refs[count]
-    sums = refs[count + 1 : 2 * count + 1]
-    rests = refs[2 * count + 1 : 3 * count + 1]
-    mines = refs[3 * count + 1 : 4 * count + 1]
-    sems = refs[-1]
+    own_ref, table_ref = refs[count : count + 2]
+    sums = refs[count + 2 : 2 * count + 2]
+    rests = refs[2 * count + 2 : 3 * count + 1]
+    mines = refs[3 * count + 1 :]
     half = own_ref.shape[1]
     part = part_ref[0]
     mine = pl.multiple_of(part * half, half)
@@ -345,6 +370,14 @@
     ]
     for copy in first + second:
         copy.start()
+    row = lax.broadcasted_iota(jnp.int32, table_ref.shape, 0) + offset_ref[0]
+    lane = lax.broadcasted_iota(jnp.int32, table_ref.shape, 1)
+    turn_of = lane % (D_ROPE // 2)
+    rate = jnp.exp2(turn_of.astype(F32) * (-2.0 / D_ROPE * np.log2(ROPE_BASE)))
+    angle = row.astype(F32) * rate
+    sine = jnp.sin(angle)
+    sine = jnp.where(lane < D_ROPE + D_ROPE // 2, -sine, sine)
+    table_ref[...] = jnp.where(lane < D_ROPE, jnp.cos(angle), sine)
     own = own_ref[...]
     for copy, mine_ref, sum_ref in zip(first, mines, sums):
         copy.wait()
@@ -618,15 +651,11 @@
     parity = lax.axis_index("sp").astype(jnp.int32) % 2
     flip = 1 - parity
 
-    places = (offset + jnp.arange(rows, dtype=jnp.int32)).astype(F32)
-    angles = rotary_angles(places, D_ROPE)
-    cosines, sines = jnp.cos(angles), jnp.sin(angles)
-    table = jnp.concatenate([cosines, cosines, -sines, sines], axis=1)
-
     lat = key_value_down_weight.shape[1]
+    height = rows + rows // 2 + 16
     normalized, own, send = call(
         compress_body,
-        [shape((rows, half), BF16), shape((rows, lat + LANES), F32), shape((rows, lat + LANES), BF16)],
+        [shape((rows, half), BF16), shape((height, lat), F32), shape((height, lat), BF16)],
         [offset[None], part[None], parity[None], flip[None]], [activations, norm_gain[None], key_value_down_weight, rope_key.T], [],
         2 * rows * half * 192, 8,
         [
@@ -640,14 +669,18 @@
     got = swap(send, "tp", 1)
     other = swap(normalized, "tp", 1)
     weights = [win_key, win_value, win_query, lat_query]
-    partial_sums = call(
+    table, *partial_sums = call(
         partial(own_body, count=len(weights)),
-        [shape((rows, w.shape[1]), F32) for w in weights]
-        + [shape((half, w.shape[1]), BF16) for w in weights],
-        [part[None]], weights, [normalized],
+        [shape((rows, LANES), F32)] + [shape((rows, w.shape[1]), F32) for w in weights]
+        + [shape((half, w.shape[1]), BF16) for w in weights[:-1]],
+        [offset[None], part[None]], weights, [normalized],
         2 * rows * half * 1792, 16,
         [pltpu.VMEM((half, w.shape[1]), BF16) for w in weights]
         + [pltpu.SemaphoreType.DMA((2, len(weights)))],
+    )
+    staged = call(
+        stage_body, shape((half, weights[-1].shape[1]), BF16),
+        [part[None]], weights[-1:], [], 1e6, 4, [pltpu.SemaphoreType.DMA],
     )
     block, row_scale = call(
         partial(latent_body, features=features),
@@ -672,7 +705,7 @@
             shape((chunks, lat + LANES, columns), BF16),
         ],
         [parity[None]], [],
-        [other, row_scale, table, *partial_sums, key_up_weight],
+        [other, row_scale, table, *partial_sums, staged, key_up_weight],
         2 * rows * half * 1792, 16,
     )
     inner = lax.ppermute(inward, "sp", [(i, i ^ 1) for i in range(count) if i ^ 1 < count])

time: 59.4 us -> 68.7 us (1.16)
  waiting for transfers between devices: 20.3 us -> 29.4 us
  Pallas kernels: 18 us -> 19.3 us
  other arithmetic: 0.73 us -> 0.01 us
    ppermute x19, waiting for transfers between devices: 20.3 us -> 29.4 us  [swap(): return lax.ppermute(cells, axis, [(i, i ^ bit) for i in range(count)])]
    pallas_call x8 -> x9, Pallas kernels: 16.4 us -> 17.7 us  [call(): pl.pallas_call(body, out_shape=outs, in_specs=scalars(len(smem)) + [pl.Bl...]
  transfers between devices with their start and end apart: 21 -> 21, of which waited for: 8 -> 7; matrix products, arithmetic and copies ran while one was open for 1% -> 0% of each run, Pallas kernels for 25% -> 24%
where the time goes in v5:
time: 68.7 us; the launch traced here: 68.5 us
  waiting for transfers between devices  29.4 us (43%)
  starting transfers between devices  19.5 us (28%)
  Pallas kernels  19.3 us (28%)
    ppermute x19, waiting for transfers between devices, swap(): return lax.ppermute(cells, axis, [(i, i ^ bit) for i in range(count)])  29.4 us
    pallas_call x9, Pallas kernels, call(): pl.pallas_call(body, out_shape=outs, in_specs=scalars(len(smem)) + [pl.Bl...  17.7 us
    ppermute x19, starting transfers between devices, swap(): return lax.ppermute(cells, axis, [(i, i ^ bit) for i in range(count)])  16.2 us
    ppermute x1, starting transfers between devices, per_device(): lax.ppermute(inward, 'sp', [(i, i ^ 1) for i in range(count) if i ^ 1 < c...  2.46 us
    pallas_call x2, Pallas kernels, store(): pl.pallas_call(partial(store_body, fresh=fresh), out_shape=jax.ShapeDtype...  1.55 us
  transfers between devices with their start and end apart: 21, of which 7 were waited for; matrix products, arithmetic and copies ran while one was open for 0% of the time, Pallas kernels for 24%

profile of v5, /device:TPU:0, one launch (start us, length us, event | category | flops | bytes accessed | tf_op | source)
XLA Modules:
  0.0 68.5 jit_solution(14449590081270366224)
XLA Ops:
  0.0 2.2 %shard_map.136 = (bf16[256,1024]{1,0:T(8,128)(2,1)S(1)}, f32[400,128]{1,0:T(8,128)S(1)}, bf16[400,128]{1,0:T(8,128)(2,1)S(1)}) custom-call(s32[1]{0:T(128)} %bitcast.2.offset_ref, s32[1]{0:T(128)} %bitcast.3.part_ref, s32[1]{0:T(128)} %bitcast.parity_ref.chunk_ref, s32[1]{0:T(128)} %bitcast.1.other_ref.chunk_ref, bf16[256,1024]{1,0:T(8,128)(2,1)} %x_hbm.1, ...), custom_call_target="tpu_custom_call" | custom-call | flops 100663296 | bytes 1318912 | tf_op jit(solution)/shard_map/pallas_call | solution.py:251
  2.2 3.0 %collective-permute-start.7 = (bf16[256,1024]{1,0:T(8,128)(2,1)S(1)}, bf16[256,1024]{1,0:T(8,128)(2,1)S(1)}, u32[]{:S(2)}, u32[]{:S(2)}) collective-permute-start(bf16[256,1024]{1,0:T(8,128)(2,1)S(1)} %get-tuple-element.34.refs_4_), channel_id=1, source_target_pairs={{0,1},{1,0},{2,3},{3,2},{4,5},{5,4},{6,7},{7,6},{8,9},{9,8},{10,11... | collective-permute-start | bytes 1572872 | tf_op jit(solution)/shard_map/ppermute | solution.py:608
  5.3 0.0 copy-start.4
  5.3 0.1 collective-permute-start
  5.4 3.0 %shard_map.137 = (f32[256,128]{1,0:T(8,128)S(1)}, f32[256,256]{1,0:T(8,128)S(1)}, f32[256,256]{1,0:T(8,128)S(1)}, f32[256,512]{1,0:T(8,128)S(1)}, f32[256,768]{1...) custom-call(s32[1]{0:T(128)} %bitcast.2.offset_ref, ...), custom_call_target="tpu_custom_call" | custom-call | flops 939524096 | bytes 7864320 | tf_op jit(solution)/shard_map/pallas_call | solution.py:251
  8.4 11.0 %collective-permute-done.got_ref = bf16[400,128]{1,0:T(8,128)(2,1)S(1)} collective-permute-done((bf16[400,128]{1,0:T(8,128)(2,1)S(1)}, bf16[400,128]{1,0:T(8,128)(2,1)S(1)}, u32[]{:S(2)}, u32[]{:S(2)}) %collective-permute-start) | collective-permute-done | bytes 102432 | tf_op jit(solution)/shard_map/ppermute | solution.py:608
  19.4 0.0 copy-done.4
  19.4 0.4 shard_map.138
  19.8 1.9 %collective-permute-start.8 = (bf16[384,128]{1,0:T(8,128)(2,1)S(1)}, bf16[384,128]{1,0:T(8,128)(2,1)S(1)}, u32[]{:S(2)}, u32[]{:S(2)}) collective-permute-start(bf16[384,128]{1,0:T(8,128)(2,1)S(1)} %get-tuple-element.36.refs_0_), channel_id=1, source_target_pairs={{0,8},{2,10},{4,12},{6,14},{8,0},{10,2},{12,4},{14,6},{16,24},{18,... | collective-permute-start | bytes 294920 | tf_op jit(solution)/shard_map/ppermute | solution.py:608
  21.7 2.6 %collective-permute-start.1 = (bf16[384,128]{1,0:T(8,128)(2,1)S(1)}, bf16[384,128]{1,0:T(8,128)(2,1)S(1)}, u32[]{:S(2)}, u32[]{:S(2)}) collective-permute-start(bf16[384,128]{1,0:T(8,128)(2,1)S(1)} %get-tuple-element.36.refs_0_), channel_id=1, source_target_pairs={{0,16},{2,18},{4,20},{6,22},{8,24},{10,26},{12,28},{14,30},{16,0},... | collective-permute-start | bytes 294920 | tf_op jit(solution)/shard_map/ppermute | solution.py:608
  24.3 0.0 collective-permute-start.3
  24.3 1.7 %collective-permute-start.11 = (bf16[384,128]{1,0:T(8,128)(2,1)S(1)}, bf16[384,128]{1,0:T(8,128)(2,1)S(1)}, u32[]{:S(2)}, u32[]{:S(2)}) collective-permute-start(bf16[384,128]{1,0:T(8,128)(2,1)S(1)} %get-tuple-element.36.refs_0_), channel_id=1, source_target_pairs={{0,4},{2,6},{4,0},{6,2},{8,12},{10,14},{12,8},{14,10},{16,20},{18,... | collective-permute-start | bytes 294920 | tf_op jit(solution)/shard_map/ppermute | solution.py:608
  26.0 0.0 collective-permute-done.8.refs_1_
  26.0 0.0 collective-permute-start.9
  26.0 5.2 %collective-permute-done.1.refs_4_ = bf16[384,128]{1,0:T(8,128)(2,1)S(1)} collective-permute-done((bf16[384,128]{1,0:T(8,128)(2,1)S(1)}, bf16[384,128]{1,0:T(8,128)(2,1)S(1)}, u32[]{:S(2)}, u32[]{:S(2)}) %collective-permute-start.1) | collective-permute-done | bytes 98336 | tf_op jit(solution)/shard_map/ppermute | solution.py:608
  31.2 1.5 %collective-permute-start.12 = (bf16[384,128]{1,0:T(8,128)(2,1)S(1)}, bf16[384,128]{1,0:T(8,128)(2,1)S(1)}, u32[]{:S(2)}, u32[]{:S(2)}) collective-permute-start(bf16[384,128]{1,0:T(8,128)(2,1)S(1)} %collective-permute-done.8.refs_1_), channel_id=1, source_target_pairs={{0,4},{2,6},{4,0},{6,2},{8,12},{10,14},{12,8},{14,10},{16,20},{18,... | collective-permute-start | bytes 294920 | tf_op jit(solution)/shard_map/ppermute | solution.py:608
  32.8 0.0 collective-permute-done.3.refs_5_
  32.8 0.5 collective-permute-start.2
  33.3 0.0 collective-permute-done.11.refs_6_
  33.3 1.5 %collective-permute-start.4 = (bf16[384,128]{1,0:T(8,128)(2,1)S(1)}, bf16[384,128]{1,0:T(8,128)(2,1)S(1)}, u32[]{:S(2)}, u32[]{:S(2)}) collective-permute-start(bf16[384,128]{1,0:T(8,128)(2,1)S(1)} %collective-permute-done.3.refs_5_), channel_id=1, source_target_pairs={{0,4},{2,6},{4,0},{6,2},{8,12},{10,14},{12,8},{14,10},{16,20},{18,... | collective-permute-start | bytes 294920 | tf_op jit(solution)/shard_map/ppermute | solution.py:608
  34.8 0.0 collective-permute-done.9.refs_2_
  34.8 0.0 collective-permute-start.10
  34.8 1.0 %collective-permute-done.12.refs_7_ = bf16[384,128]{1,0:T(8,128)(2,1)S(1)} collective-permute-done((bf16[384,128]{1,0:T(8,128)(2,1)S(1)}, bf16[384,128]{1,0:T(8,128)(2,1)S(1)}, u32[]{:S(2)}, u32[]{:S(2)}) %collective-permute-start.12) | collective-permute-done | bytes 98336 | tf_op jit(solution)/shard_map/ppermute | solution.py:608
  35.9 0.0 collective-permute-start.13
  35.9 1.5 %collective-permute-done.2.refs_0_.refs_12_ = bf16[384,128]{1,0:T(8,128)(2,1)S(1)} collective-permute-done((bf16[384,128]{1,0:T(8,128)(2,1)S(1)}, bf16[384,128]{1,0:T(8,128)(2,1)S(1)}, u32[]{:S(2)}, u32[]{:S(2)}) %collective-permute-start.2) | collective-permute-done | bytes 98336 | tf_op jit(solution)/shard_map/ppermute | solution.py:608
  37.4 0.0 collective-permute-start.14
  37.4 1.0 %collective-permute-done.4.refs_1_.refs_13_ = bf16[384,128]{1,0:T(8,128)(2,1)S(1)} collective-permute-done((bf16[384,128]{1,0:T(8,128)(2,1)S(1)}, bf16[384,128]{1,0:T(8,128)(2,1)S(1)}, u32[]{:S(2)}, u32[]{:S(2)}) %collective-permute-start.4) | collective-permute-done | bytes 98336 | tf_op jit(solution)/shard_map/ppermute | solution.py:608
  38.4 0.0 collective-permute-start.15
  38.4 0.0 collective-permute-done.7.got_ref
  38.4 0.5 collective-permute-start.16
  38.9 0.0 copy-done.5
  39.0 1.5 %shard_map.139.wl_ref = bf16[1024,768]{1,0:T(8,128)(2,1)S(1)} custom-call(s32[1]{0:T(128)} %bitcast.3.part_ref, bf16[2048,768]{1,0:T(8,128)(2,1)} %w_ref.1), custom_call_target="tpu_custom_call" | custom-call | flops 1000000 | bytes 3145728 | tf_op jit(solution)/shard_map/pallas_call | solution.py:251
  40.4 0.0 copy-done.3
  40.4 1.9 %shard_map.140 = (bf16[2,4,128,256]{3,2,1,0:T(8,128)(2,1)S(1)}, bf16[256,512]{1,0:T(8,128)(2,1)S(1)}, bf16[128,512]{1,0:T(8,128)(2,1)S(1)}, bf16[128,512]{1,0:T(...) custom-call(s32[1]{0:T(128)} %bitcast.parity_ref.chunk_ref, ...), custom_call_target="tpu_custom_call" | custom-call | flops 939524096 | bytes 6422528 | tf_op jit(solution)/shard_map/pallas_call | solution.py:251
  42.3 0.0 collective-permute-done.10.refs_3_
  42.3 0.1 collective-permute-start.5
  42.4 0.0 collective-permute-done.13.refs_8_
  42.4 0.5 collective-permute-start.6
  42.9 0.0 collective-permute-done.14.refs_9_
  42.9 0.8 %collective-permute-start.19 = (bf16[128,512]{1,0:T(8,128)(2,1)S(1)}, bf16[128,512]{1,0:T(8,128)(2,1)S(1)}, u32[]{:S(2)}, u32[]{:S(2)}) collective-permute-start(bf16[128,512]{1,0:T(8,128)(2,1)S(1)} %get-tuple-element.56), channel_id=1, source_target_pairs={{0,0},{2,4},{4,2},{6,8},{8,6},{10,12},{12,10},{14,16},{16,14},{18,... | collective-permute-start | bytes 393224 | tf_op jit(solution)/shard_map/ppermute | solution.py:717
  43.8 0.0 collective-permute-done.15.refs_10_
  43.8 2.5 %collective-permute-start.17 = (bf16[128,512]{1,0:T(8,128)(2,1)S(1)}, bf16[128,512]{1,0:T(8,128)(2,1)S(1)}, u32[]{:S(2)}, u32[]{:S(2)}) collective-permute-start(bf16[128,512]{1,0:T(8,128)(2,1)S(1)} %get-tuple-element.50), channel_id=1, source_target_pairs={{0,2},{2,0},{4,6},{6,4},{8,10},{10,8},{12,14},{14,12},{16,18},{18,... | collective-permute-start | bytes 393224 | tf_op jit(solution)/shard_map/ppermute | solution.py:711
  46.2 0.0 collective-permute-done.16.refs_11_
  46.2 2.2 %shard_map.141 = (f32[16,512]{1,0:T(8,128)S(1)}, f32[128,512]{1,0:T(8,128)S(1)}) custom-call(s32[1]{0:T(128)} %bitcast.1.other_ref.chunk_ref, bf16[384,128]{1,0:T(8,128)(2,1)S(1)} %get-tuple-element.36.refs_0_, bf16[384,128]{1,0:T(8,128)(2,1)S(1)} %collective-permute-done.8.refs_1_, bf16[384,128]{1,0:T(8,128)(2,1)S(1)} %collective-permute-done.9.refs_2_, ...), custom_call_target="tpu_custom_call" | custom-call | flops 3000000000 | bytes 2228224 | tf_op jit(solution)/shard_map/pallas_call | solution.py:251
  48.4 0.0 copy-start
  48.5 0.0 copy-start.1
  48.5 0.0 copy-start.2
  48.5 0.0 collective-permute-done.5.refs_2_.refs_14_
  48.5 0.0 collective-permute-done.6.refs_3_.refs_15_
  48.5 2.8 %shard_map.143 = (f32[16,512]{1,0:T(8,128)S(1)}, f32[128,512]{1,0:T(8,128)S(1)}) custom-call(s32[1]{0:T(128)} %bitcast.parity_ref.chunk_ref, bf16[384,128]{1,0:T(8,128)(2,1)S(1)} %get-tuple-element.36.refs_0_, bf16[384,128]{1,0:T(8,128)(2,1)S(1)} %collective-permute-done.8.refs_1_, bf16[384,128]{1,0:T(8,128)(2,1)S(1)} %collective-permute-done.9.refs_2_, ...), custom_call_target="tpu_custom_call" | custom-call | flops 3000000000 | bytes 2621440 | tf_op jit(solution)/shard_map/pallas_call | solution.py:251
  51.3 0.0 collective-permute-done.17.refs_10_
  51.3 0.1 broadcast_in_dim.20.refs_8_.refs_4_
  51.4 0.0 copy-done
  51.4 0.0 copy-done.1
  51.4 0.0 copy-done.2
  51.4 2.3 %shard_map.142 = (bf16[128,1024]{1,0:T(8,128)(2,1)S(1)}, f32[128,1024]{1,0:T(8,128)S(1)}) custom-call(s32[1]{0:T(128)} %bitcast.2.offset_ref, s32[1]{0:T(128)} %bitcast.3.part_ref, s32[1]{0:T(128)} %bitcast.1.other_ref.chunk_ref, bf16[384,128]{1,0:T(8,128)(2,1)S(1)} %collective-permute-done.2.refs_0_.refs_12_, ...), custom_call_target="tpu_custom_call" | custom-call | flops 1000000000 | bytes 6983680 | tf_op jit(solution)/shard_map/pallas_call | solution.py:251
  53.7 1.6 %collective-permute-start.18 = (bf16[128,1024]{1,0:T(8,128)(2,1)S(1)}, bf16[128,1024]{1,0:T(8,128)(2,1)S(1)}, u32[]{:S(2)}, u32[]{:S(2)}) collective-permute-start(bf16[128,1024]{1,0:T(8,128)(2,1)S(1)} %get-tuple-element.53), channel_id=1, source_target_pairs={{0,1},{1,0},{2,3},{3,2},{4,5},{5,4},{6,7},{7,6},{8,9},{9,8},{10,11... | collective-permute-start | bytes 786440 | tf_op jit(solution)/shard_map/ppermute | solution.py:608
  55.3 0.0 collective-permute-done.19.refs_6_
  55.3 1.5 %shard_map.144 = (bf16[128,1024]{1,0:T(8,128)(2,1)S(1)}, f32[128,1024]{1,0:T(8,128)S(1)}) custom-call(s32[1]{0:T(128)} %bitcast.2.offset_ref, s32[1]{0:T(128)} %bitcast.3.part_ref, s32[1]{0:T(128)} %bitcast.parity_ref.chunk_ref, bf16[2,256,512]{2,1,0:T(8,128)(2,1)S(1)} %get-tuple-element.45.refs_12_.refs_4_.refs_16_.refs_0_, ...), custom_call_target="tpu_custom_call" | custom-call | flops 1000000000 | bytes 6590464 | tf_op jit(solution)/shard_map/pallas_call | solution.py:251
  56.8 0.6 collective-permute-start.20
  57.3 5.6 %collective-permute-done.18.refs_1_ = bf16[128,1024]{1,0:T(8,128)(2,1)S(1)} collective-permute-done((bf16[128,1024]{1,0:T(8,128)(2,1)S(1)}, bf16[128,1024]{1,0:T(8,128)(2,1)S(1)}, u32[]{:S(2)}, u32[]{:S(2)}) %collective-permute-start.18) | collective-permute-done | bytes 262176 | tf_op jit(solution)/shard_map/ppermute | solution.py:608
  62.9 0.8 %store.1.refs_0_ = bf16[256,1024]{1,0:T(8,128)(2,1)} custom-call(s32[1]{0:T(128)} %bitcast.1.other_ref.chunk_ref, f32[128,1024]{1,0:T(8,128)S(1)} %get-tuple-element.52.refs_0_, bf16[128,1024]{1,0:T(8,128)(2,1)S(1)} %collective-permute-done.18.refs_1_), custom_call_target="tpu_custom_call" | custom-call | tf_op jit(solution)/shard_map/store/pallas_call | solution.py:594
  63.7 3.9 %collective-permute-done.20.refs_2_ = bf16[128,1024]{1,0:T(8,128)(2,1)S(1)} collective-permute-done((bf16[128,1024]{1,0:T(8,128)(2,1)S(1)}, bf16[128,1024]{1,0:T(8,128)(2,1)S(1)}, u32[]{:S(2)}, u32[]{:S(2)}) %collective-permute-start.20) | collective-permute-done | bytes 262176 | tf_op jit(solution)/shard_map/ppermute | solution.py:608
  67.6 0.8 %store_rest.1 = bf16[256,1024]{1,0:T(8,128)(2,1)} custom-call(s32[1]{0:T(128)} %bitcast.parity_ref.chunk_ref, bf16[256,1024]{1,0:T(8,128)(2,1)} %store.1.refs_0_, f32[128,1024]{1,0:T(8,128)S(1)} %get-tuple-element.57.refs_1_, bf16[128,1024]{1,0:T(8,128)(2,1)S(1)} %collective-permute-done.20.refs_2_), custom_call_target="tpu_custom_call", output_to_operand_aliasing={{}: (1, {})} | custom-call | tf_op jit(solution)/shard_map/store_rest/pallas_call | solution.py:594
  (3 shorter events, 0.0 us)
Async XLA Ops:
  2.2 36.2 %collective-permute-start.7 = (bf16[256,1024]{1,0:T(8,128)(2,1)S(1)}, bf16[256,1024]{1,0:T(8,128)(2,1)S(1)}, u32[]{:S(2)}, u32[]{:S(2)}) collective-permute-start(bf16[256,1024]{1,0:T(8,128)(2,1)S(1)} %get-tuple-element.34.refs_4_), channel_id=1, source_target_pairs={{0,1},{1,0},{2,3},{3,2},{4,5},{5,4},{6,7},{7,6},{8,9},{9,8},{10,11... | collective-permute-start | bytes 1572872 | tf_op jit(solution)/shard_map/ppermute | solution.py:608
  5.3 14.1 %copy-start.4 = (f32[128]{0:T(128)S(1)}, f32[128]{0:T(128)}, u32[]{:S(2)}) copy-start(f32[128]{0:T(128)} %param.23) | copy-start | bytes 1540
  5.3 33.7 %copy-start.5 = (f32[8]{0:T(128)S(1)}, f32[8]{0:T(128)}, u32[]{:S(2)}) copy-start(f32[8]{0:T(128)} %param.19) | copy-start | bytes 100
  5.3 14.1 %collective-permute-start = (bf16[400,128]{1,0:T(8,128)(2,1)S(1)}, bf16[400,128]{1,0:T(8,128)(2,1)S(1)}, u32[]{:S(2)}, u32[]{:S(2)}) collective-permute-start(bf16[400,128]{1,0:T(8,128)(2,1)S(1)} %get-tuple-element.33), channel_id=1, source_target_pairs={{0,1},{1,0},{2,3},{3,2},{4,5},{5,4},{6,7},{7,6},{8,9},{9,8},{10,11... | collective-permute-start | bytes 307208 | tf_op jit(solution)/shard_map/ppermute | solution.py:608
  19.8 6.2 %collective-permute-start.8 = (bf16[384,128]{1,0:T(8,128)(2,1)S(1)}, bf16[384,128]{1,0:T(8,128)(2,1)S(1)}, u32[]{:S(2)}, u32[]{:S(2)}) collective-permute-start(bf16[384,128]{1,0:T(8,128)(2,1)S(1)} %get-tuple-element.36.refs_0_), channel_id=1, source_target_pairs={{0,8},{2,10},{4,12},{6,14},{8,0},{10,2},{12,4},{14,6},{16,24},{18,... | collective-permute-start | bytes 294920 | tf_op jit(solution)/shard_map/ppermute | solution.py:608
  21.7 9.6 %collective-permute-start.1 = (bf16[384,128]{1,0:T(8,128)(2,1)S(1)}, bf16[384,128]{1,0:T(8,128)(2,1)S(1)}, u32[]{:S(2)}, u32[]{:S(2)}) collective-permute-start(bf16[384,128]{1,0:T(8,128)(2,1)S(1)} %get-tuple-element.36.refs_0_), channel_id=1, source_target_pairs={{0,16},{2,18},{4,20},{6,22},{8,24},{10,26},{12,28},{14,30},{16,0},... | collective-permute-start | bytes 294920 | tf_op jit(solution)/shard_map/ppermute | solution.py:608
  24.3 8.5 %collective-permute-start.3 = (bf16[384,128]{1,0:T(8,128)(2,1)S(1)}, bf16[384,128]{1,0:T(8,128)(2,1)S(1)}, u32[]{:S(2)}, u32[]{:S(2)}) collective-permute-start(bf16[384,128]{1,0:T(8,128)(2,1)S(1)} %get-tuple-element.36.refs_0_), channel_id=1, source_target_pairs={{0,24},{2,26},{4,28},{6,30},{8,16},{10,18},{12,20},{14,22},{16,8},... | collective-permute-start | bytes 294920 | tf_op jit(solution)/shard_map/ppermute | solution.py:608
  24.3 9.0 %collective-permute-start.11 = (bf16[384,128]{1,0:T(8,128)(2,1)S(1)}, bf16[384,128]{1,0:T(8,128)(2,1)S(1)}, u32[]{:S(2)}, u32[]{:S(2)}) collective-permute-start(bf16[384,128]{1,0:T(8,128)(2,1)S(1)} %get-tuple-element.36.refs_0_), channel_id=1, source_target_pairs={{0,4},{2,6},{4,0},{6,2},{8,12},{10,14},{12,8},{14,10},{16,20},{18,... | collective-permute-start | bytes 294920 | tf_op jit(solution)/shard_map/ppermute | solution.py:608
  26.0 8.8 %collective-permute-start.9 = (bf16[384,128]{1,0:T(8,128)(2,1)S(1)}, bf16[384,128]{1,0:T(8,128)(2,1)S(1)}, u32[]{:S(2)}, u32[]{:S(2)}) collective-permute-start(bf16[384,128]{1,0:T(8,128)(2,1)S(1)} %get-tuple-element.36.refs_0_), channel_id=1, source_target_pairs={{0,2},{2,0},{4,6},{6,4},{8,10},{10,8},{12,14},{14,12},{16,18},{18,... | collective-permute-start | bytes 294920 | tf_op jit(solution)/shard_map/ppermute | solution.py:608
  31.2 4.6 %collective-permute-start.12 = (bf16[384,128]{1,0:T(8,128)(2,1)S(1)}, bf16[384,128]{1,0:T(8,128)(2,1)S(1)}, u32[]{:S(2)}, u32[]{:S(2)}) collective-permute-start(bf16[384,128]{1,0:T(8,128)(2,1)S(1)} %collective-permute-done.8.refs_1_), channel_id=1, source_target_pairs={{0,4},{2,6},{4,0},{6,2},{8,12},{10,14},{12,8},{14,10},{16,20},{18,... | collective-permute-start | bytes 294920 | tf_op jit(solution)/shard_map/ppermute | solution.py:608
  32.8 4.6 %collective-permute-start.2 = (bf16[384,128]{1,0:T(8,128)(2,1)S(1)}, bf16[384,128]{1,0:T(8,128)(2,1)S(1)}, u32[]{:S(2)}, u32[]{:S(2)}) collective-permute-start(bf16[384,128]{1,0:T(8,128)(2,1)S(1)} %collective-permute-done.1.refs_4_), channel_id=1, source_target_pairs={{0,4},{2,6},{4,0},{6,2},{8,12},{10,14},{12,8},{14,10},{16,20},{18,... | collective-permute-start | bytes 294920 | tf_op jit(solution)/shard_map/ppermute | solution.py:608
  33.3 5.2 %collective-permute-start.4 = (bf16[384,128]{1,0:T(8,128)(2,1)S(1)}, bf16[384,128]{1,0:T(8,128)(2,1)S(1)}, u32[]{:S(2)}, u32[]{:S(2)}) collective-permute-start(bf16[384,128]{1,0:T(8,128)(2,1)S(1)} %collective-permute-done.3.refs_5_), channel_id=1, source_target_pairs={{0,4},{2,6},{4,0},{6,2},{8,12},{10,14},{12,8},{14,10},{16,20},{18,... | collective-permute-start | bytes 294920 | tf_op jit(solution)/shard_map/ppermute | solution.py:608
  34.8 7.5 %collective-permute-start.10 = (bf16[384,128]{1,0:T(8,128)(2,1)S(1)}, bf16[384,128]{1,0:T(8,128)(2,1)S(1)}, u32[]{:S(2)}, u32[]{:S(2)}) collective-permute-start(bf16[384,128]{1,0:T(8,128)(2,1)S(1)} %collective-permute-done.8.refs_1_), channel_id=1, source_target_pairs={{0,2},{2,0},{4,6},{6,4},{8,10},{10,8},{12,14},{14,12},{16,18},{18,... | collective-permute-start | bytes 294920 | tf_op jit(solution)/shard_map/ppermute | solution.py:608
  35.9 6.6 %collective-permute-start.13 = (bf16[384,128]{1,0:T(8,128)(2,1)S(1)}, bf16[384,128]{1,0:T(8,128)(2,1)S(1)}, u32[]{:S(2)}, u32[]{:S(2)}) collective-permute-start(bf16[384,128]{1,0:T(8,128)(2,1)S(1)} %collective-permute-done.1.refs_4_), channel_id=1, source_target_pairs={{0,2},{2,0},{4,6},{6,4},{8,10},{10,8},{12,14},{14,12},{16,18},{18,... | collective-permute-start | bytes 294920 | tf_op jit(solution)/shard_map/ppermute | solution.py:608
  37.4 5.5 %collective-permute-start.14 = (bf16[384,128]{1,0:T(8,128)(2,1)S(1)}, bf16[384,128]{1,0:T(8,128)(2,1)S(1)}, u32[]{:S(2)}, u32[]{:S(2)}) collective-permute-start(bf16[384,128]{1,0:T(8,128)(2,1)S(1)} %collective-permute-done.3.refs_5_), channel_id=1, source_target_pairs={{0,2},{2,0},{4,6},{6,4},{8,10},{10,8},{12,14},{14,12},{16,18},{18,... | collective-permute-start | bytes 294920 | tf_op jit(solution)/shard_map/ppermute | solution.py:608
  38.4 5.3 %collective-permute-start.15 = (bf16[384,128]{1,0:T(8,128)(2,1)S(1)}, bf16[384,128]{1,0:T(8,128)(2,1)S(1)}, u32[]{:S(2)}, u32[]{:S(2)}) collective-permute-start(bf16[384,128]{1,0:T(8,128)(2,1)S(1)} %collective-permute-done.11.refs_6_), channel_id=1, source_target_pairs={{0,2},{2,0},{4,6},{6,4},{8,10},{10,8},{12,14},{14,12},{16,18},{18,... | collective-permute-start | bytes 294920 | tf_op jit(solution)/shard_map/ppermute | solution.py:608
  38.4 7.8 %collective-permute-start.16 = (bf16[384,128]{1,0:T(8,128)(2,1)S(1)}, bf16[384,128]{1,0:T(8,128)(2,1)S(1)}, u32[]{:S(2)}, u32[]{:S(2)}) collective-permute-start(bf16[384,128]{1,0:T(8,128)(2,1)S(1)} %collective-permute-done.12.refs_7_), channel_id=1, source_target_pairs={{0,2},{2,0},{4,6},{6,4},{8,10},{10,8},{12,14},{14,12},{16,18},{18,... | collective-permute-start | bytes 294920 | tf_op jit(solution)/shard_map/ppermute | solution.py:608
  39.0 1.5 %copy-start.3 = (bf16[128,512]{1,0:T(8,128)(2,1)S(1)}, bf16[128,512]{1,0:T(8,128)(2,1)}, u32[]{:S(2)}) copy-start(bf16[128,512]{1,0:T(8,128)(2,1)} %up_ref.1) | copy-start | bytes 393220
  42.3 6.1 %collective-permute-start.5 = (bf16[384,128]{1,0:T(8,128)(2,1)S(1)}, bf16[384,128]{1,0:T(8,128)(2,1)S(1)}, u32[]{:S(2)}, u32[]{:S(2)}) collective-permute-start(bf16[384,128]{1,0:T(8,128)(2,1)S(1)} %collective-permute-done.2.refs_0_.refs_12_), channel_id=1, source_target_pairs={{0,2},{2,0},{4,6},{6,4},{8,10},{10,8},{12,14},{14,12},{16,18},{18,... | collective-permute-start | bytes 294920 | tf_op jit(solution)/shard_map/ppermute | solution.py:608
  42.4 6.1 %collective-permute-start.6 = (bf16[384,128]{1,0:T(8,128)(2,1)S(1)}, bf16[384,128]{1,0:T(8,128)(2,1)S(1)}, u32[]{:S(2)}, u32[]{:S(2)}) collective-permute-start(bf16[384,128]{1,0:T(8,128)(2,1)S(1)} %collective-permute-done.4.refs_1_.refs_13_), channel_id=1, source_target_pairs={{0,2},{2,0},{4,6},{6,4},{8,10},{10,8},{12,14},{14,12},{16,18},{18,... | collective-permute-start | bytes 294920 | tf_op jit(solution)/shard_map/ppermute | solution.py:608
  42.9 12.3 %collective-permute-start.19 = (bf16[128,512]{1,0:T(8,128)(2,1)S(1)}, bf16[128,512]{1,0:T(8,128)(2,1)S(1)}, u32[]{:S(2)}, u32[]{:S(2)}) collective-permute-start(bf16[128,512]{1,0:T(8,128)(2,1)S(1)} %get-tuple-element.56), channel_id=1, source_target_pairs={{0,0},{2,4},{4,2},{6,8},{8,6},{10,12},{12,10},{14,16},{16,14},{18,... | collective-permute-start | bytes 393224 | tf_op jit(solution)/shard_map/ppermute | solution.py:717
  43.8 7.5 %collective-permute-start.17 = (bf16[128,512]{1,0:T(8,128)(2,1)S(1)}, bf16[128,512]{1,0:T(8,128)(2,1)S(1)}, u32[]{:S(2)}, u32[]{:S(2)}) collective-permute-start(bf16[128,512]{1,0:T(8,128)(2,1)S(1)} %get-tuple-element.50), channel_id=1, source_target_pairs={{0,2},{2,0},{4,6},{6,4},{8,10},{10,8},{12,14},{14,12},{16,18},{18,... | collective-permute-start | bytes 393224 | tf_op jit(solution)/shard_map/ppermute | solution.py:711
  48.4 2.9 %copy-start = (bf16[512,2048]{1,0:T(8,128)(2,1)S(1)}, bf16[512,2048]{1,0:T(8,128)(2,1)}, u32[]{:S(2)}) copy-start(bf16[512,2048]{1,0:T(8,128)(2,1)} %refs_9_.1) | copy-start | bytes 6291460
  48.5 2.9 %copy-start.1 = (bf16[512,2048]{1,0:T(8,128)(2,1)S(1)}, bf16[512,2048]{1,0:T(8,128)(2,1)}, u32[]{:S(2)}) copy-start(bf16[512,2048]{1,0:T(8,128)(2,1)} %refs_10_.1) | copy-start | bytes 6291460
  48.5 2.9 %copy-start.2 = (bf16[128,512]{1,0:T(8,128)(2,1)S(1)}, bf16[128,512]{1,0:T(8,128)(2,1)}, u32[]{:S(2)}) copy-start(bf16[128,512]{1,0:T(8,128)(2,1)} %refs_8_.1) | copy-start | bytes 393220
  53.7 9.2 %collective-permute-start.18 = (bf16[128,1024]{1,0:T(8,128)(2,1)S(1)}, bf16[128,1024]{1,0:T(8,128)(2,1)S(1)}, u32[]{:S(2)}, u32[]{:S(2)}) collective-permute-start(bf16[128,1024]{1,0:T(8,128)(2,1)S(1)} %get-tuple-element.53), channel_id=1, source_target_pairs={{0,1},{1,0},{2,3},{3,2},{4,5},{5,4},{6,7},{7,6},{8,9},{9,8},{10,11... | collective-permute-start | bytes 786440 | tf_op jit(solution)/shard_map/ppermute | solution.py:608
  56.8 10.8 %collective-permute-start.20 = (bf16[128,1024]{1,0:T(8,128)(2,1)S(1)}, bf16[128,1024]{1,0:T(8,128)(2,1)S(1)}, u32[]{:S(2)}, u32[]{:S(2)}) collective-permute-start(bf16[128,1024]{1,0:T(8,128)(2,1)S(1)} %get-tuple-element.58), channel_id=1, source_target_pairs={{0,1},{1,0},{2,3},{3,2},{4,5},{5,4},{6,7},{7,6},{8,9},{9,8},{10,11... | collective-permute-start | bytes 786440 | tf_op jit(solution)/shard_map/ppermute | solution.py:608

commit v6 on v5

--- a/solution.py
+++ b/solution.py
@@ -273,25 +273,30 @@
     rows, half = x_hbm.shape
     del offset_ref, parity_ref, other_ref
     start = pl.multiple_of(part_ref[0] * half, half)
+    middle = rows // 2
     copies = [
-        pltpu.make_async_copy(x_hbm, x_ref, sems.at[0]),
+        pltpu.make_async_copy(x_hbm.at[:middle], x_ref.at[:middle], sems.at[0]),
         pltpu.make_async_copy(gain_hbm.at[:, pl.ds(start, half)], gain_ref, sems.at[3]),
         pltpu.make_async_copy(down_hbm.at[pl.ds(start, half), :], down_ref, sems.at[1]),
         pltpu.make_async_copy(rope_hbm.at[:, pl.ds(start, half)], rope_ref, sems.at[2]),
     ]
+    copies.append(pltpu.make_async_copy(x_hbm.at[middle:], x_ref.at[middle:], sems.at[4]))
     for copy in copies:
         copy.start()
-    copies[0].wait()
     copies[1].wait()
-    wide = x_ref[...].astype(F32)
-    normalized = (wide * gain_ref[...]).astype(BF16)
-    norm_ref[...] = normalized
-    squares = jnp.sum(wide * wide, axis=1, keepdims=True)
-    copies[2].wait()
-    compressed = dot(normalized, down_ref[...])
-    copies[3].wait()
-    rope = dot(normalized, rope_ref[...], ((1,), (1,)))
-    middle = rows // 2
+    parts = []
+    for at, copy in ((0, copies[0]), (middle, copies[4])):
+        copy.wait()
+        wide = x_ref[at : at + middle].astype(F32)
+        normalized = (wide * gain_ref[...]).astype(BF16)
+        norm_ref[at : at + middle] = normalized
+        squares = jnp.sum(wide * wide, axis=1, keepdims=True)
+        if at == 0:
+            copies[2].wait()
+            copies[3].wait()
+        compressed = dot(normalized, down_ref[...])
+        parts.append((squares, compressed, dot(normalized, rope_ref[...], ((1,), (1,)))))
+    squares, compressed, rope = (jnp.concatenate(p, axis=0) for p in zip(*parts))
     packed = jnp.concatenate([rope[:middle], rope[middle:]], axis=1)
     line = jnp.broadcast_to(squares, (rows, LANES)).T[:1]
     high = line.astype(BF16).astype(F32)
@@ -663,7 +668,7 @@
             pltpu.VMEM((1, half), F32),
             pltpu.VMEM((half, lat), BF16),
             pltpu.VMEM((rope_key.shape[1], half), BF16),
-            pltpu.SemaphoreType.DMA((4,)),
+            pltpu.SemaphoreType.DMA((5,)),
         ],
     )
     got = swap(send, "tp", 1)

time: 68.7 us -> 68.4 us (level)
  no operation moved by 1% of the time
where the time goes in v6:
time: 68.4 us; the launch traced here: 68.2 us
  waiting for transfers between devices  29.4 us (43%)
  starting transfers between devices  19.5 us (29%)
  Pallas kernels  18.9 us (28%)
    ppermute x19, waiting for transfers between devices, swap(): return lax.ppermute(cells, axis, [(i, i ^ bit) for i in range(count)])  29.4 us
    pallas_call x9, Pallas kernels, call(): pl.pallas_call(body, out_shape=outs, in_specs=scalars(len(smem)) + [pl.Bl...  17.4 us
    ppermute x19, starting transfers between devices, swap(): return lax.ppermute(cells, axis, [(i, i ^ bit) for i in range(count)])  16.2 us
    ppermute x1, starting transfers between devices, per_device(): lax.ppermute(inward, 'sp', [(i, i ^ 1) for i in range(count) if i ^ 1 < c...  2.48 us
    pallas_call x2, Pallas kernels, store(): pl.pallas_call(partial(store_body, fresh=fresh), out_shape=jax.ShapeDtype...  1.55 us
  transfers between devices with their start and end apart: 21, of which 7 were waited for; matrix products, arithmetic and copies ran while one was open for 0% of the time, Pallas kernels for 24%

profile of v6, /device:TPU:0, one launch (start us, length us, event | category | flops | bytes accessed | tf_op | source)
XLA Modules:
  0.0 68.2 jit_solution(9039008380670798119)
XLA Ops:
  0.0 1.9 %shard_map.136 = (bf16[256,1024]{1,0:T(8,128)(2,1)S(1)}, f32[400,128]{1,0:T(8,128)S(1)}, bf16[400,128]{1,0:T(8,128)(2,1)S(1)}) custom-call(s32[1]{0:T(128)} %bitcast.2.offset_ref, s32[1]{0:T(128)} %bitcast.3.part_ref, s32[1]{0:T(128)} %bitcast.parity_ref.chunk_ref, s32[1]{0:T(128)} %bitcast.1.other_ref.chunk_ref, bf16[256,1024]{1,0:T(8,128)(2,1)} %x_hbm.1, ...), custom_call_target="tpu_custom_call" | custom-call | flops 100663296 | bytes 1318912 | tf_op jit(solution)/shard_map/pallas_call | solution.py:251
  1.9 3.0 %collective-permute-start.7 = (bf16[256,1024]{1,0:T(8,128)(2,1)S(1)}, bf16[256,1024]{1,0:T(8,128)(2,1)S(1)}, u32[]{:S(2)}, u32[]{:S(2)}) collective-permute-start(bf16[256,1024]{1,0:T(8,128)(2,1)S(1)} %get-tuple-element.34.refs_4_), channel_id=1, source_target_pairs={{0,1},{1,0},{2,3},{3,2},{4,5},{5,4},{6,7},{7,6},{8,9},{9,8},{10,11... | collective-permute-start | bytes 1572872 | tf_op jit(solution)/shard_map/ppermute | solution.py:613
  4.9 0.0 copy-start.5
  4.9 0.1 collective-permute-start
  5.0 3.0 %shard_map.137 = (f32[256,128]{1,0:T(8,128)S(1)}, f32[256,256]{1,0:T(8,128)S(1)}, f32[256,256]{1,0:T(8,128)S(1)}, f32[256,512]{1,0:T(8,128)S(1)}, f32[256,768]{1...) custom-call(s32[1]{0:T(128)} %bitcast.2.offset_ref, ...), custom_call_target="tpu_custom_call" | custom-call | flops 939524096 | bytes 7864320 | tf_op jit(solution)/shard_map/pallas_call | solution.py:251
  8.0 11.0 %collective-permute-done.got_ref = bf16[400,128]{1,0:T(8,128)(2,1)S(1)} collective-permute-done((bf16[400,128]{1,0:T(8,128)(2,1)S(1)}, bf16[400,128]{1,0:T(8,128)(2,1)S(1)}, u32[]{:S(2)}, u32[]{:S(2)}) %collective-permute-start) | collective-permute-done | bytes 102432 | tf_op jit(solution)/shard_map/ppermute | solution.py:613
  19.0 0.0 copy-done.4
  19.0 0.4 shard_map.138
  19.4 1.9 %collective-permute-start.8 = (bf16[384,128]{1,0:T(8,128)(2,1)S(1)}, bf16[384,128]{1,0:T(8,128)(2,1)S(1)}, u32[]{:S(2)}, u32[]{:S(2)}) collective-permute-start(bf16[384,128]{1,0:T(8,128)(2,1)S(1)} %get-tuple-element.36.refs_0_), channel_id=1, source_target_pairs={{0,8},{2,10},{4,12},{6,14},{8,0},{10,2},{12,4},{14,6},{16,24},{18,... | collective-permute-start | bytes 294920 | tf_op jit(solution)/shard_map/ppermute | solution.py:613
  21.3 2.6 %collective-permute-start.1 = (bf16[384,128]{1,0:T(8,128)(2,1)S(1)}, bf16[384,128]{1,0:T(8,128)(2,1)S(1)}, u32[]{:S(2)}, u32[]{:S(2)}) collective-permute-start(bf16[384,128]{1,0:T(8,128)(2,1)S(1)} %get-tuple-element.36.refs_0_), channel_id=1, source_target_pairs={{0,16},{2,18},{4,20},{6,22},{8,24},{10,26},{12,28},{14,30},{16,0},... | collective-permute-start | bytes 294920 | tf_op jit(solution)/shard_map/ppermute | solution.py:613
  23.9 0.0 collective-permute-start.3
  23.9 1.7 %collective-permute-start.11 = (bf16[384,128]{1,0:T(8,128)(2,1)S(1)}, bf16[384,128]{1,0:T(8,128)(2,1)S(1)}, u32[]{:S(2)}, u32[]{:S(2)}) collective-permute-start(bf16[384,128]{1,0:T(8,128)(2,1)S(1)} %get-tuple-element.36.refs_0_), channel_id=1, source_target_pairs={{0,4},{2,6},{4,0},{6,2},{8,12},{10,14},{12,8},{14,10},{16,20},{18,... | collective-permute-start | bytes 294920 | tf_op jit(solution)/shard_map/ppermute | solution.py:613
  25.6 0.0 collective-permute-done.8.refs_1_
  25.7 0.0 collective-permute-start.9
  25.7 5.2 %collective-permute-done.1.refs_4_ = bf16[384,128]{1,0:T(8,128)(2,1)S(1)} collective-permute-done((bf16[384,128]{1,0:T(8,128)(2,1)S(1)}, bf16[384,128]{1,0:T(8,128)(2,1)S(1)}, u32[]{:S(2)}, u32[]{:S(2)}) %collective-permute-start.1) | collective-permute-done | bytes 98336 | tf_op jit(solution)/shard_map/ppermute | solution.py:613
  30.9 1.5 %collective-permute-start.12 = (bf16[384,128]{1,0:T(8,128)(2,1)S(1)}, bf16[384,128]{1,0:T(8,128)(2,1)S(1)}, u32[]{:S(2)}, u32[]{:S(2)}) collective-permute-start(bf16[384,128]{1,0:T(8,128)(2,1)S(1)} %collective-permute-done.8.refs_1_), channel_id=1, source_target_pairs={{0,4},{2,6},{4,0},{6,2},{8,12},{10,14},{12,8},{14,10},{16,20},{18,... | collective-permute-start | bytes 294920 | tf_op jit(solution)/shard_map/ppermute | solution.py:613
  32.4 0.0 collective-permute-done.3.refs_5_
  32.4 0.5 collective-permute-start.2
  32.9 0.0 collective-permute-done.11.refs_6_
  32.9 1.5 %collective-permute-start.4 = (bf16[384,128]{1,0:T(8,128)(2,1)S(1)}, bf16[384,128]{1,0:T(8,128)(2,1)S(1)}, u32[]{:S(2)}, u32[]{:S(2)}) collective-permute-start(bf16[384,128]{1,0:T(8,128)(2,1)S(1)} %collective-permute-done.3.refs_5_), channel_id=1, source_target_pairs={{0,4},{2,6},{4,0},{6,2},{8,12},{10,14},{12,8},{14,10},{16,20},{18,... | collective-permute-start | bytes 294920 | tf_op jit(solution)/shard_map/ppermute | solution.py:613
  34.4 0.0 collective-permute-done.9.refs_2_
  34.4 0.0 collective-permute-start.10
  34.4 1.1 %collective-permute-done.12.refs_7_ = bf16[384,128]{1,0:T(8,128)(2,1)S(1)} collective-permute-done((bf16[384,128]{1,0:T(8,128)(2,1)S(1)}, bf16[384,128]{1,0:T(8,128)(2,1)S(1)}, u32[]{:S(2)}, u32[]{:S(2)}) %collective-permute-start.12) | collective-permute-done | bytes 98336 | tf_op jit(solution)/shard_map/ppermute | solution.py:613
  35.5 0.0 collective-permute-start.13
  35.5 1.5 %collective-permute-done.2.refs_0_.refs_12_ = bf16[384,128]{1,0:T(8,128)(2,1)S(1)} collective-permute-done((bf16[384,128]{1,0:T(8,128)(2,1)S(1)}, bf16[384,128]{1,0:T(8,128)(2,1)S(1)}, u32[]{:S(2)}, u32[]{:S(2)}) %collective-permute-start.2) | collective-permute-done | bytes 98336 | tf_op jit(solution)/shard_map/ppermute | solution.py:613
  37.0 0.0 collective-permute-start.14
  37.0 1.0 %collective-permute-done.4.refs_1_.refs_13_ = bf16[384,128]{1,0:T(8,128)(2,1)S(1)} collective-permute-done((bf16[384,128]{1,0:T(8,128)(2,1)S(1)}, bf16[384,128]{1,0:T(8,128)(2,1)S(1)}, u32[]{:S(2)}, u32[]{:S(2)}) %collective-permute-start.4) | collective-permute-done | bytes 98336 | tf_op jit(solution)/shard_map/ppermute | solution.py:613
  38.1 0.0 collective-permute-start.15
  38.1 0.0 collective-permute-done.7.got_ref
  38.1 0.5 collective-permute-start.16
  38.6 0.0 copy-done.5
  38.6 1.5 %shard_map.139.wl_ref = bf16[1024,768]{1,0:T(8,128)(2,1)S(1)} custom-call(s32[1]{0:T(128)} %bitcast.3.part_ref, bf16[2048,768]{1,0:T(8,128)(2,1)} %w_ref.1), custom_call_target="tpu_custom_call" | custom-call | flops 1000000 | bytes 3145728 | tf_op jit(solution)/shard_map/pallas_call | solution.py:251
  40.1 0.0 copy-done.3
  40.1 1.9 %shard_map.140 = (bf16[2,4,128,256]{3,2,1,0:T(8,128)(2,1)S(1)}, bf16[256,512]{1,0:T(8,128)(2,1)S(1)}, bf16[128,512]{1,0:T(8,128)(2,1)S(1)}, bf16[128,512]{1,0:T(...) custom-call(s32[1]{0:T(128)} %bitcast.parity_ref.chunk_ref, ...), custom_call_target="tpu_custom_call" | custom-call | flops 939524096 | bytes 6422528 | tf_op jit(solution)/shard_map/pallas_call | solution.py:251
  42.0 0.0 collective-permute-done.10.refs_3_
  42.0 0.1 collective-permute-start.5
  42.1 0.0 collective-permute-done.13.refs_8_
  42.1 0.5 collective-permute-start.6
  42.6 0.0 collective-permute-done.14.refs_9_
  42.6 0.8 %collective-permute-start.19 = (bf16[128,512]{1,0:T(8,128)(2,1)S(1)}, bf16[128,512]{1,0:T(8,128)(2,1)S(1)}, u32[]{:S(2)}, u32[]{:S(2)}) collective-permute-start(bf16[128,512]{1,0:T(8,128)(2,1)S(1)} %get-tuple-element.56), channel_id=1, source_target_pairs={{0,0},{2,4},{4,2},{6,8},{8,6},{10,12},{12,10},{14,16},{16,14},{18,... | collective-permute-start | bytes 393224 | tf_op jit(solution)/shard_map/ppermute | solution.py:722
  43.4 0.0 collective-permute-done.15.refs_10_
  43.4 2.5 %collective-permute-start.17 = (bf16[128,512]{1,0:T(8,128)(2,1)S(1)}, bf16[128,512]{1,0:T(8,128)(2,1)S(1)}, u32[]{:S(2)}, u32[]{:S(2)}) collective-permute-start(bf16[128,512]{1,0:T(8,128)(2,1)S(1)} %get-tuple-element.50), channel_id=1, source_target_pairs={{0,2},{2,0},{4,6},{6,4},{8,10},{10,8},{12,14},{14,12},{16,18},{18,... | collective-permute-start | bytes 393224 | tf_op jit(solution)/shard_map/ppermute | solution.py:716
  45.9 0.0 collective-permute-done.16.refs_11_
  45.9 2.2 %shard_map.141 = (f32[16,512]{1,0:T(8,128)S(1)}, f32[128,512]{1,0:T(8,128)S(1)}) custom-call(s32[1]{0:T(128)} %bitcast.1.other_ref.chunk_ref, bf16[384,128]{1,0:T(8,128)(2,1)S(1)} %get-tuple-element.36.refs_0_, bf16[384,128]{1,0:T(8,128)(2,1)S(1)} %collective-permute-done.8.refs_1_, bf16[384,128]{1,0:T(8,128)(2,1)S(1)} %collective-permute-done.9.refs_2_, ...), custom_call_target="tpu_custom_call" | custom-call | flops 3000000000 | bytes 2228224 | tf_op jit(solution)/shard_map/pallas_call | solution.py:251
  48.1 0.0 copy-start
  48.1 0.0 copy-start.1
  48.1 0.0 copy-start.2
  48.1 0.0 collective-permute-done.5.refs_2_.refs_14_
  48.2 0.0 collective-permute-done.6.refs_3_.refs_15_
  48.2 2.8 %shard_map.143 = (f32[16,512]{1,0:T(8,128)S(1)}, f32[128,512]{1,0:T(8,128)S(1)}) custom-call(s32[1]{0:T(128)} %bitcast.parity_ref.chunk_ref, bf16[384,128]{1,0:T(8,128)(2,1)S(1)} %get-tuple-element.36.refs_0_, bf16[384,128]{1,0:T(8,128)(2,1)S(1)} %collective-permute-done.8.refs_1_, bf16[384,128]{1,0:T(8,128)(2,1)S(1)} %collective-permute-done.9.refs_2_, ...), custom_call_target="tpu_custom_call" | custom-call | flops 3000000000 | bytes 2621440 | tf_op jit(solution)/shard_map/pallas_call | solution.py:251
  51.0 0.0 collective-permute-done.17.refs_10_
  51.0 0.1 broadcast_in_dim.20.refs_8_.refs_4_
  51.0 0.0 copy-done
  51.0 0.0 copy-done.1
  51.0 0.0 copy-done.2
  51.0 2.3 %shard_map.142 = (bf16[128,1024]{1,0:T(8,128)(2,1)S(1)}, f32[128,1024]{1,0:T(8,128)S(1)}) custom-call(s32[1]{0:T(128)} %bitcast.2.offset_ref, s32[1]{0:T(128)} %bitcast.3.part_ref, s32[1]{0:T(128)} %bitcast.1.other_ref.chunk_ref, bf16[384,128]{1,0:T(8,128)(2,1)S(1)} %collective-permute-done.2.refs_0_.refs_12_, ...), custom_call_target="tpu_custom_call" | custom-call | flops 1000000000 | bytes 6983680 | tf_op jit(solution)/shard_map/pallas_call | solution.py:251
  53.3 1.5 %collective-permute-start.18 = (bf16[128,1024]{1,0:T(8,128)(2,1)S(1)}, bf16[128,1024]{1,0:T(8,128)(2,1)S(1)}, u32[]{:S(2)}, u32[]{:S(2)}) collective-permute-start(bf16[128,1024]{1,0:T(8,128)(2,1)S(1)} %get-tuple-element.53), channel_id=1, source_target_pairs={{0,1},{1,0},{2,3},{3,2},{4,5},{5,4},{6,7},{7,6},{8,9},{9,8},{10,11... | collective-permute-start | bytes 786440 | tf_op jit(solution)/shard_map/ppermute | solution.py:613
  54.9 0.0 collective-permute-done.19.refs_6_
  54.9 1.5 %shard_map.144 = (bf16[128,1024]{1,0:T(8,128)(2,1)S(1)}, f32[128,1024]{1,0:T(8,128)S(1)}) custom-call(s32[1]{0:T(128)} %bitcast.2.offset_ref, s32[1]{0:T(128)} %bitcast.3.part_ref, s32[1]{0:T(128)} %bitcast.parity_ref.chunk_ref, bf16[2,256,512]{2,1,0:T(8,128)(2,1)S(1)} %get-tuple-element.45.refs_12_.refs_4_.refs_16_.refs_0_, ...), custom_call_target="tpu_custom_call" | custom-call | flops 1000000000 | bytes 6590464 | tf_op jit(solution)/shard_map/pallas_call | solution.py:251
  56.4 0.6 collective-permute-start.20
  57.0 5.6 %collective-permute-done.18.refs_1_ = bf16[128,1024]{1,0:T(8,128)(2,1)S(1)} collective-permute-done((bf16[128,1024]{1,0:T(8,128)(2,1)S(1)}, bf16[128,1024]{1,0:T(8,128)(2,1)S(1)}, u32[]{:S(2)}, u32[]{:S(2)}) %collective-permute-start.18) | collective-permute-done | bytes 262176 | tf_op jit(solution)/shard_map/ppermute | solution.py:613
  62.6 0.8 %store.1.refs_0_ = bf16[256,1024]{1,0:T(8,128)(2,1)} custom-call(s32[1]{0:T(128)} %bitcast.1.other_ref.chunk_ref, f32[128,1024]{1,0:T(8,128)S(1)} %get-tuple-element.52.refs_0_, bf16[128,1024]{1,0:T(8,128)(2,1)S(1)} %collective-permute-done.18.refs_1_), custom_call_target="tpu_custom_call" | custom-call | tf_op jit(solution)/shard_map/store/pallas_call | solution.py:599
  63.4 3.9 %collective-permute-done.20.refs_2_ = bf16[128,1024]{1,0:T(8,128)(2,1)S(1)} collective-permute-done((bf16[128,1024]{1,0:T(8,128)(2,1)S(1)}, bf16[128,1024]{1,0:T(8,128)(2,1)S(1)}, u32[]{:S(2)}, u32[]{:S(2)}) %collective-permute-start.20) | collective-permute-done | bytes 262176 | tf_op jit(solution)/shard_map/ppermute | solution.py:613
  67.3 0.8 %store_rest.1 = bf16[256,1024]{1,0:T(8,128)(2,1)} custom-call(s32[1]{0:T(128)} %bitcast.parity_ref.chunk_ref, bf16[256,1024]{1,0:T(8,128)(2,1)} %store.1.refs_0_, f32[128,1024]{1,0:T(8,128)S(1)} %get-tuple-element.57.refs_1_, bf16[128,1024]{1,0:T(8,128)(2,1)S(1)} %collective-permute-done.20.refs_2_), custom_call_target="tpu_custom_call", output_to_operand_aliasing={{}: (1, {})} | custom-call | tf_op jit(solution)/shard_map/store_rest/pallas_call | solution.py:599
  (3 shorter events, 0.0 us)
Async XLA Ops:
  1.9 36.2 %collective-permute-start.7 = (bf16[256,1024]{1,0:T(8,128)(2,1)S(1)}, bf16[256,1024]{1,0:T(8,128)(2,1)S(1)}, u32[]{:S(2)}, u32[]{:S(2)}) collective-permute-start(bf16[256,1024]{1,0:T(8,128)(2,1)S(1)} %get-tuple-element.34.refs_4_), channel_id=1, source_target_pairs={{0,1},{1,0},{2,3},{3,2},{4,5},{5,4},{6,7},{7,6},{8,9},{9,8},{10,11... | collective-permute-start | bytes 1572872 | tf_op jit(solution)/shard_map/ppermute | solution.py:613
  4.9 14.1 %copy-start.4 = (f32[128]{0:T(128)S(1)}, f32[128]{0:T(128)}, u32[]{:S(2)}) copy-start(f32[128]{0:T(128)} %param.23) | copy-start | bytes 1540
  4.9 33.7 %copy-start.5 = (f32[8]{0:T(128)S(1)}, f32[8]{0:T(128)}, u32[]{:S(2)}) copy-start(f32[8]{0:T(128)} %param.19) | copy-start | bytes 100
  4.9 14.1 %collective-permute-start = (bf16[400,128]{1,0:T(8,128)(2,1)S(1)}, bf16[400,128]{1,0:T(8,128)(2,1)S(1)}, u32[]{:S(2)}, u32[]{:S(2)}) collective-permute-start(bf16[400,128]{1,0:T(8,128)(2,1)S(1)} %get-tuple-element.33), channel_id=1, source_target_pairs={{0,1},{1,0},{2,3},{3,2},{4,5},{5,4},{6,7},{7,6},{8,9},{9,8},{10,11... | collective-permute-start | bytes 307208 | tf_op jit(solution)/shard_map/ppermute | solution.py:613
  19.4 6.2 %collective-permute-start.8 = (bf16[384,128]{1,0:T(8,128)(2,1)S(1)}, bf16[384,128]{1,0:T(8,128)(2,1)S(1)}, u32[]{:S(2)}, u32[]{:S(2)}) collective-permute-start(bf16[384,128]{1,0:T(8,128)(2,1)S(1)} %get-tuple-element.36.refs_0_), channel_id=1, source_target_pairs={{0,8},{2,10},{4,12},{6,14},{8,0},{10,2},{12,4},{14,6},{16,24},{18,... | collective-permute-start | bytes 294920 | tf_op jit(solution)/shard_map/ppermute | solution.py:613
  21.3 9.6 %collective-permute-start.1 = (bf16[384,128]{1,0:T(8,128)(2,1)S(1)}, bf16[384,128]{1,0:T(8,128)(2,1)S(1)}, u32[]{:S(2)}, u32[]{:S(2)}) collective-permute-start(bf16[384,128]{1,0:T(8,128)(2,1)S(1)} %get-tuple-element.36.refs_0_), channel_id=1, source_target_pairs={{0,16},{2,18},{4,20},{6,22},{8,24},{10,26},{12,28},{14,30},{16,0},... | collective-permute-start | bytes 294920 | tf_op jit(solution)/shard_map/ppermute | solution.py:613
  23.9 8.5 %collective-permute-start.3 = (bf16[384,128]{1,0:T(8,128)(2,1)S(1)}, bf16[384,128]{1,0:T(8,128)(2,1)S(1)}, u32[]{:S(2)}, u32[]{:S(2)}) collective-permute-start(bf16[384,128]{1,0:T(8,128)(2,1)S(1)} %get-tuple-element.36.refs_0_), channel_id=1, source_target_pairs={{0,24},{2,26},{4,28},{6,30},{8,16},{10,18},{12,20},{14,22},{16,8},... | collective-permute-start | bytes 294920 | tf_op jit(solution)/shard_map/ppermute | solution.py:613
  23.9 9.0 %collective-permute-start.11 = (bf16[384,128]{1,0:T(8,128)(2,1)S(1)}, bf16[384,128]{1,0:T(8,128)(2,1)S(1)}, u32[]{:S(2)}, u32[]{:S(2)}) collective-permute-start(bf16[384,128]{1,0:T(8,128)(2,1)S(1)} %get-tuple-element.36.refs_0_), channel_id=1, source_target_pairs={{0,4},{2,6},{4,0},{6,2},{8,12},{10,14},{12,8},{14,10},{16,20},{18,... | collective-permute-start | bytes 294920 | tf_op jit(solution)/shard_map/ppermute | solution.py:613
  25.7 8.8 %collective-permute-start.9 = (bf16[384,128]{1,0:T(8,128)(2,1)S(1)}, bf16[384,128]{1,0:T(8,128)(2,1)S(1)}, u32[]{:S(2)}, u32[]{:S(2)}) collective-permute-start(bf16[384,128]{1,0:T(8,128)(2,1)S(1)} %get-tuple-element.36.refs_0_), channel_id=1, source_target_pairs={{0,2},{2,0},{4,6},{6,4},{8,10},{10,8},{12,14},{14,12},{16,18},{18,... | collective-permute-start | bytes 294920 | tf_op jit(solution)/shard_map/ppermute | solution.py:613
  30.9 4.6 %collective-permute-start.12 = (bf16[384,128]{1,0:T(8,128)(2,1)S(1)}, bf16[384,128]{1,0:T(8,128)(2,1)S(1)}, u32[]{:S(2)}, u32[]{:S(2)}) collective-permute-start(bf16[384,128]{1,0:T(8,128)(2,1)S(1)} %collective-permute-done.8.refs_1_), channel_id=1, source_target_pairs={{0,4},{2,6},{4,0},{6,2},{8,12},{10,14},{12,8},{14,10},{16,20},{18,... | collective-permute-start | bytes 294920 | tf_op jit(solution)/shard_map/ppermute | solution.py:613
  32.4 4.6 %collective-permute-start.2 = (bf16[384,128]{1,0:T(8,128)(2,1)S(1)}, bf16[384,128]{1,0:T(8,128)(2,1)S(1)}, u32[]{:S(2)}, u32[]{:S(2)}) collective-permute-start(bf16[384,128]{1,0:T(8,128)(2,1)S(1)} %collective-permute-done.1.refs_4_), channel_id=1, source_target_pairs={{0,4},{2,6},{4,0},{6,2},{8,12},{10,14},{12,8},{14,10},{16,20},{18,... | collective-permute-start | bytes 294920 | tf_op jit(solution)/shard_map/ppermute | solution.py:613
  32.9 5.2 %collective-permute-start.4 = (bf16[384,128]{1,0:T(8,128)(2,1)S(1)}, bf16[384,128]{1,0:T(8,128)(2,1)S(1)}, u32[]{:S(2)}, u32[]{:S(2)}) collective-permute-start(bf16[384,128]{1,0:T(8,128)(2,1)S(1)} %collective-permute-done.3.refs_5_), channel_id=1, source_target_pairs={{0,4},{2,6},{4,0},{6,2},{8,12},{10,14},{12,8},{14,10},{16,20},{18,... | collective-permute-start | bytes 294920 | tf_op jit(solution)/shard_map/ppermute | solution.py:613
  34.4 7.5 %collective-permute-start.10 = (bf16[384,128]{1,0:T(8,128)(2,1)S(1)}, bf16[384,128]{1,0:T(8,128)(2,1)S(1)}, u32[]{:S(2)}, u32[]{:S(2)}) collective-permute-start(bf16[384,128]{1,0:T(8,128)(2,1)S(1)} %collective-permute-done.8.refs_1_), channel_id=1, source_target_pairs={{0,2},{2,0},{4,6},{6,4},{8,10},{10,8},{12,14},{14,12},{16,18},{18,... | collective-permute-start | bytes 294920 | tf_op jit(solution)/shard_map/ppermute | solution.py:613
  35.5 6.6 %collective-permute-start.13 = (bf16[384,128]{1,0:T(8,128)(2,1)S(1)}, bf16[384,128]{1,0:T(8,128)(2,1)S(1)}, u32[]{:S(2)}, u32[]{:S(2)}) collective-permute-start(bf16[384,128]{1,0:T(8,128)(2,1)S(1)} %collective-permute-done.1.refs_4_), channel_id=1, source_target_pairs={{0,2},{2,0},{4,6},{6,4},{8,10},{10,8},{12,14},{14,12},{16,18},{18,... | collective-permute-start | bytes 294920 | tf_op jit(solution)/shard_map/ppermute | solution.py:613
  37.0 5.5 %collective-permute-start.14 = (bf16[384,128]{1,0:T(8,128)(2,1)S(1)}, bf16[384,128]{1,0:T(8,128)(2,1)S(1)}, u32[]{:S(2)}, u32[]{:S(2)}) collective-permute-start(bf16[384,128]{1,0:T(8,128)(2,1)S(1)} %collective-permute-done.3.refs_5_), channel_id=1, source_target_pairs={{0,2},{2,0},{4,6},{6,4},{8,10},{10,8},{12,14},{14,12},{16,18},{18,... | collective-permute-start | bytes 294920 | tf_op jit(solution)/shard_map/ppermute | solution.py:613
  38.1 5.3 %collective-permute-start.15 = (bf16[384,128]{1,0:T(8,128)(2,1)S(1)}, bf16[384,128]{1,0:T(8,128)(2,1)S(1)}, u32[]{:S(2)}, u32[]{:S(2)}) collective-permute-start(bf16[384,128]{1,0:T(8,128)(2,1)S(1)} %collective-permute-done.11.refs_6_), channel_id=1, source_target_pairs={{0,2},{2,0},{4,6},{6,4},{8,10},{10,8},{12,14},{14,12},{16,18},{18,... | collective-permute-start | bytes 294920 | tf_op jit(solution)/shard_map/ppermute | solution.py:613
  38.1 7.8 %collective-permute-start.16 = (bf16[384,128]{1,0:T(8,128)(2,1)S(1)}, bf16[384,128]{1,0:T(8,128)(2,1)S(1)}, u32[]{:S(2)}, u32[]{:S(2)}) collective-permute-start(bf16[384,128]{1,0:T(8,128)(2,1)S(1)} %collective-permute-done.12.refs_7_), channel_id=1, source_target_pairs={{0,2},{2,0},{4,6},{6,4},{8,10},{10,8},{12,14},{14,12},{16,18},{18,... | collective-permute-start | bytes 294920 | tf_op jit(solution)/shard_map/ppermute | solution.py:613
  38.6 1.5 %copy-start.3 = (bf16[128,512]{1,0:T(8,128)(2,1)S(1)}, bf16[128,512]{1,0:T(8,128)(2,1)}, u32[]{:S(2)}) copy-start(bf16[128,512]{1,0:T(8,128)(2,1)} %up_ref.1) | copy-start | bytes 393220
  42.0 6.2 %collective-permute-start.5 = (bf16[384,128]{1,0:T(8,128)(2,1)S(1)}, bf16[384,128]{1,0:T(8,128)(2,1)S(1)}, u32[]{:S(2)}, u32[]{:S(2)}) collective-permute-start(bf16[384,128]{1,0:T(8,128)(2,1)S(1)} %collective-permute-done.2.refs_0_.refs_12_), channel_id=1, source_target_pairs={{0,2},{2,0},{4,6},{6,4},{8,10},{10,8},{12,14},{14,12},{16,18},{18,... | collective-permute-start | bytes 294920 | tf_op jit(solution)/shard_map/ppermute | solution.py:613
  42.1 6.1 %collective-permute-start.6 = (bf16[384,128]{1,0:T(8,128)(2,1)S(1)}, bf16[384,128]{1,0:T(8,128)(2,1)S(1)}, u32[]{:S(2)}, u32[]{:S(2)}) collective-permute-start(bf16[384,128]{1,0:T(8,128)(2,1)S(1)} %collective-permute-done.4.refs_1_.refs_13_), channel_id=1, source_target_pairs={{0,2},{2,0},{4,6},{6,4},{8,10},{10,8},{12,14},{14,12},{16,18},{18,... | collective-permute-start | bytes 294920 | tf_op jit(solution)/shard_map/ppermute | solution.py:613
  42.6 12.3 %collective-permute-start.19 = (bf16[128,512]{1,0:T(8,128)(2,1)S(1)}, bf16[128,512]{1,0:T(8,128)(2,1)S(1)}, u32[]{:S(2)}, u32[]{:S(2)}) collective-permute-start(bf16[128,512]{1,0:T(8,128)(2,1)S(1)} %get-tuple-element.56), channel_id=1, source_target_pairs={{0,0},{2,4},{4,2},{6,8},{8,6},{10,12},{12,10},{14,16},{16,14},{18,... | collective-permute-start | bytes 393224 | tf_op jit(solution)/shard_map/ppermute | solution.py:722
  43.4 7.6 %collective-permute-start.17 = (bf16[128,512]{1,0:T(8,128)(2,1)S(1)}, bf16[128,512]{1,0:T(8,128)(2,1)S(1)}, u32[]{:S(2)}, u32[]{:S(2)}) collective-permute-start(bf16[128,512]{1,0:T(8,128)(2,1)S(1)} %get-tuple-element.50), channel_id=1, source_target_pairs={{0,2},{2,0},{4,6},{6,4},{8,10},{10,8},{12,14},{14,12},{16,18},{18,... | collective-permute-start | bytes 393224 | tf_op jit(solution)/shard_map/ppermute | solution.py:716
  48.1 2.9 %copy-start = (bf16[512,2048]{1,0:T(8,128)(2,1)S(1)}, bf16[512,2048]{1,0:T(8,128)(2,1)}, u32[]{:S(2)}) copy-start(bf16[512,2048]{1,0:T(8,128)(2,1)} %refs_9_.1) | copy-start | bytes 6291460
  48.1 2.9 %copy-start.1 = (bf16[512,2048]{1,0:T(8,128)(2,1)S(1)}, bf16[512,2048]{1,0:T(8,128)(2,1)}, u32[]{:S(2)}) copy-start(bf16[512,2048]{1,0:T(8,128)(2,1)} %refs_10_.1) | copy-start | bytes 6291460
  48.1 2.9 %copy-start.2 = (bf16[128,512]{1,0:T(8,128)(2,1)S(1)}, bf16[128,512]{1,0:T(8,128)(2,1)}, u32[]{:S(2)}) copy-start(bf16[128,512]{1,0:T(8,128)(2,1)} %refs_8_.1) | copy-start | bytes 393220
  53.3 9.2 %collective-permute-start.18 = (bf16[128,1024]{1,0:T(8,128)(2,1)S(1)}, bf16[128,1024]{1,0:T(8,128)(2,1)S(1)}, u32[]{:S(2)}, u32[]{:S(2)}) collective-permute-start(bf16[128,1024]{1,0:T(8,128)(2,1)S(1)} %get-tuple-element.53), channel_id=1, source_target_pairs={{0,1},{1,0},{2,3},{3,2},{4,5},{5,4},{6,7},{7,6},{8,9},{9,8},{10,11... | collective-permute-start | bytes 786440 | tf_op jit(solution)/shard_map/ppermute | solution.py:613
  56.4 10.9 %collective-permute-start.20 = (bf16[128,1024]{1,0:T(8,128)(2,1)S(1)}, bf16[128,1024]{1,0:T(8,128)(2,1)S(1)}, u32[]{:S(2)}, u32[]{:S(2)}) collective-permute-start(bf16[128,1024]{1,0:T(8,128)(2,1)S(1)} %get-tuple-element.58), channel_id=1, source_target_pairs={{0,1},{1,0},{2,3},{3,2},{4,5},{5,4},{6,7},{7,6},{8,9},{9,8},{10,11... | collective-permute-start | bytes 786440 | tf_op jit(solution)/shard_map/ppermute | solution.py:613
